TPU v7x, 512 devices: a whole 4x8x8 slice. The times are simulated.
512 devices in a mesh: ep: 32 (over z, x), tp: 16 (over y, core).
Axes of the slice: x: 4, y: 8, z: 8, core: 2. Of those that a mesh axis runs over, the one named last changes fastest.
Arguments:
- blender_incoming_features: bfloat16 [8192, 4096], P('ep', 'tp'), may hold values from -6 to 6
- entry_latent_matrix: bfloat16 [8192, 2048], P('ep', 'tp'), may hold values from -6 to 6
- exit_latent_matrix: bfloat16 [8192, 2048], P('ep', 'tp'), may hold values from -6 to 6
- unactivated_valve: bfloat16 [8192, 4096], P('ep', 'tp'), may hold values from -6 to 6
- presoftplus_strides: float32 [8192, 64], P('ep', 'tp'), may hold values from -7 to 7
- extra_attenuation: float32 [8192, 64], P('ep', 'tp'), may hold values from -1 to 0
- incoming_feature_kernel: bfloat16 [4, 4096], P(None, 'tp'), may hold values from -3 to 3
- entry_latent_kernel: bfloat16 [4, 2048], P(None, 'tp'), may hold values from -3 to 3
- exit_latent_kernel: bfloat16 [4, 2048], P(None, 'tp'), may hold values from -3 to 3
- stride_offset_vector: float32 [64], P('tp'), may hold values from -1 to 1
- attenuation_speed_exponent: float32 [64], P('tp'), may hold values from -16 to -3
- bypass_coef_vector: float32 [64], P('tp'), may hold values from 0.5 to 4
- cluster_rescale_coefs: bfloat16 [4096], P('tp'), may hold values from 0.099609375 to 1.8984375
- blender_result_matrix: bfloat16 [4096, 2048], P('tp'), may hold values from -0.09375 to 0.09375
- latter_microbatch_activations: bfloat16 [8192, 2048], P('ep'), may hold values from -6 to 6
- specialist_rescale_coefs: bfloat16 [2048], replicated, may hold values from 0.099609375 to 1.8984375
- specialist_valve_matrix: bfloat16 [32, 2048, 4096], P('ep', None, 'tp'), may hold values from -0.125 to 0.125
- specialist_expand_matrix: bfloat16 [32, 2048, 4096], P('ep', None, 'tp'), may hold values from -0.125 to 0.125
- specialist_contract_matrix: bfloat16 [32, 4096, 2048], P('ep', 'tp'), may hold values from -0.125 to 0.125
- specialist_picks: int32 [8192, 2], P('ep'), may hold values from 0 to 31, all different within a row; in each aligned block of 256 rows (0 to 255, 256 to 511, ...) at most 24 rows name the same one
- selected_specialist_coefs: float32 [8192, 2], P('ep'), may hold values from 0.1 to 1
Outputs:
- mixed_a: bfloat16 [8192, 2048], P(('ep', 'tp'))
- mixed_b: bfloat16 [8192, 2048], P('ep', 'tp')
Inputs may be any that keep to these rules, and one draw needn't show every extreme that they name: `specialist_picks`: in each aligned block of 256 rows, the rows of one index of ep, no expert is named by more than 24 rows, a bound that some block reaches.
All inputs are finite; a program needn't handle non-finite values.
Results may differ from a plain program's by a relative error of at most 0.019.
Values may be sent and summed in bfloat16 or wider, within the bound.
No kernel may reach another device: no remote copies, remote signals or barrier semaphores. Data moves between devices by JAX's collectives and lax.ppermute only.
A program may use at most 64 MiB of HBM per device.

v0:
```python
import jax
import jax.numpy as jnp
from jax import lax
from jax.sharding import Mesh
from jax.sharding import PartitionSpec as P

HEADS = 64
HEAD_DIM = 64
SHARING_CLUSTERS = 16
STATE = 128
BLOCK = 64
TOPK = 2
EP = ("ep_0", "ep_1")
TP = ("tp_0", "tp_1")
EP_TP = ("ep_0", "ep_1", "tp_0", "tp_1")


NORM_EPS = 1e-06


def from_behind(block, axis, distance):
    devices = range(lax.axis_size(axis))
    route = [(i - distance, i) for i in devices if i - distance in devices]
    return lax.ppermute(block, axis, route)


def filled_with(x, identity):
    return jax.tree.map(
        lambda part, zero: jnp.zeros_like(part) + jnp.asarray(zero, part.dtype), x, identity
    )


def carried_in(x, axes, combine, identity):
    before = start = filled_with(x, identity)
    running = x
    for axis in reversed(axes):
        count, place = (lax.axis_size(axis), lax.axis_index(axis))
        pieces = jax.tree.map(
            lambda part, kind: lax.all_gather(part.astype(kind), axis),
            running,
            (jnp.bfloat16, jnp.bfloat16),
        )
        inside, running = (start, start)
        for k in range(count):
            passed = k < place
            running = combine(
                running, jax.tree.map(lambda part, own: part[k].astype(own.dtype), pieces, x)
            )
            inside = jax.tree.map(lambda new, old: jnp.where(passed, new, old), running, inside)
        before = combine(inside, before)
    return before


def in_blocks(x, dim, count):
    before, after = (x.shape[:dim], x.shape[dim + 1 :])
    return jnp.moveaxis(x.reshape(*before, count, -1, *after), dim, 0)


def summed_on_arrival(x, axis, dim):
    tiles = in_blocks(x, dim, lax.axis_size(axis))
    arrived = lax.all_to_all(tiles, axis, split_axis=0, concat_axis=0, tiled=True)
    return arrived.astype(jnp.float32).sum(axis=0)


def summed_rows(x, axes, dim):
    for axis in axes:
        x = lax.psum_scatter(x, axis, scatter_dimension=dim, tiled=True)
    return x


def conv_silu(inputs, rim_rows, weight):
    tap_count = weight.shape[0]
    context_span = inputs.shape[0]
    joined = jnp.concatenate([rim_rows, inputs], axis=0).astype(jnp.float32)
    kernel = weight.astype(jnp.float32)
    running_total = kernel[0] * joined[0:context_span]
    for offset in range(1, tap_count):
        running_total = running_total + kernel[offset] * joined[offset : offset + context_span]
    return jax.nn.silu(running_total)


def block_step(carry_state, inputs):
    scaled_x, b_block, c_block, log_block = inputs
    context_span = log_block.shape[0]
    running = jnp.cumsum(log_block, axis=0)
    causal = (jnp.arange(context_span)[:, None] >= jnp.arange(context_span)[None, :])[
        :, :, None, None
    ]
    log_gap = running[:, None] - running[None, :]
    weights = jnp.where(causal, jnp.exp(jnp.where(causal, log_gap, 0.0)), 0.0)
    scores = jnp.einsum("lgn,sgn->lsg", c_block, b_block, preferred_element_type=jnp.float32)
    inside = jnp.einsum("lsgj,sgjp->lgjp", scores[..., None] * weights, scaled_x)
    c_wide = c_block.astype(jnp.float32)
    b_wide = b_block.astype(jnp.float32)
    before = jnp.einsum("lgn,gjpn->lgjp", c_wide, carry_state) * jnp.exp(running)[..., None]
    to_end = jnp.exp(running[-1] - running)
    carry_state = carry_state * jnp.exp(running[-1])[..., None, None] + jnp.einsum(
        "sgn,sgjp->gjpn", b_wide, scaled_x * to_end[..., None]
    )
    return (carry_state, inside + before)


def combine_states(earlier, later):
    early_state, early_log = earlier
    late_state, late_log = later
    return (early_state * jnp.exp(late_log)[..., None, None] + late_state, early_log + late_log)


def local(
    blender_incoming_features,
    entry_latent_matrix,
    exit_latent_matrix,
    unactivated_valve,
    presoftplus_strides,
    extra_attenuation,
    incoming_feature_kernel,
    entry_latent_kernel,
    exit_latent_kernel,
    stride_offset_vector,
    attenuation_speed_exponent,
    bypass_coef_vector,
    cluster_rescale_coefs,
    blender_result_matrix,
    latter_microbatch_activations,
    specialist_rescale_coefs,
    specialist_valve_matrix,
    specialist_expand_matrix,
    specialist_contract_matrix,
    specialist_picks,
    selected_specialist_coefs,
):
    tap_count = incoming_feature_kernel.shape[0]
    tok_rows = blender_incoming_features.shape[0]
    groups_local = entry_latent_matrix.shape[1] // STATE
    members_within_cluster = HEADS // SHARING_CLUSTERS
    tail_start = tok_rows - tap_count + 1
    rim_x, rim_b, rim_c = from_behind(
        (
            blender_incoming_features[tail_start:],
            entry_latent_matrix[tail_start:],
            exit_latent_matrix[tail_start:],
        ),
        EP,
        1,
    )
    conv_x_out = conv_silu(blender_incoming_features, rim_x, incoming_feature_kernel).reshape(
        tok_rows, groups_local, members_within_cluster, HEAD_DIM
    )
    conv_b_out = (
        conv_silu(entry_latent_matrix, rim_b, entry_latent_kernel)
        .astype(jnp.bfloat16)
        .reshape(tok_rows, groups_local, STATE)
    )
    conv_c_out = (
        conv_silu(exit_latent_matrix, rim_c, exit_latent_kernel)
        .astype(jnp.bfloat16)
        .reshape(tok_rows, groups_local, STATE)
    )
    stride_amount = jax.nn.softplus(presoftplus_strides + stride_offset_vector[None, :])
    attenuation_exponent = (
        -jnp.exp(attenuation_speed_exponent)[None, :] * stride_amount + extra_attenuation
    ).reshape(tok_rows, groups_local, members_within_cluster)
    scaled_x = (
        conv_x_out
        * stride_amount.reshape(tok_rows, groups_local, members_within_cluster)[..., None]
    )
    blocks = tok_rows // BLOCK

    def as_blocks(array_value):
        return array_value.reshape((blocks, BLOCK) + array_value.shape[1:])

    start_state = jnp.zeros((groups_local, members_within_cluster, HEAD_DIM, STATE), jnp.float32)
    end_state, block_out = lax.scan(
        block_step,
        start_state,
        (
            as_blocks(scaled_x),
            as_blocks(conv_b_out),
            as_blocks(conv_c_out),
            as_blocks(attenuation_exponent),
        ),
    )
    running = jnp.cumsum(attenuation_exponent, axis=0)
    enter_state = carried_in(
        (end_state, running[-1]),
        EP,
        combine_states,
        (jnp.zeros_like(end_state), jnp.zeros_like(running[-1])),
    )[0]
    carried = (
        jnp.einsum("lgn,gjpn->lgjp", conv_c_out.astype(jnp.float32), enter_state)
        * jnp.exp(running)[..., None]
    )
    ssd_out = (
        block_out.reshape(tok_rows, groups_local, members_within_cluster, HEAD_DIM)
        + carried
        + bypass_coef_vector.reshape(groups_local, members_within_cluster)[None, :, :, None]
        * conv_x_out
    )
    gated_out = ssd_out.reshape(tok_rows, -1) * jax.nn.silu(unactivated_valve.astype(jnp.float32))
    grouped = gated_out.reshape(tok_rows, groups_local, -1)
    grouped = grouped * lax.rsqrt(jnp.mean(grouped * grouped, axis=-1, keepdims=True) + NORM_EPS)
    normed = (grouped.reshape(tok_rows, -1) * cluster_rescale_coefs.astype(jnp.float32)).astype(
        jnp.bfloat16
    )
    mixed_a = summed_on_arrival(
        jnp.dot(normed, blender_result_matrix, preferred_element_type=jnp.float32).astype(
            jnp.bfloat16
        ),
        TP,
        0,
    ).astype(jnp.bfloat16)
    ep_count = lax.axis_size(EP)
    token_count = latter_microbatch_activations.shape[0]
    model_width = latter_microbatch_activations.shape[1]
    local_experts = specialist_valve_matrix.shape[0]
    expert_count = ep_count * local_experts
    capacity = 3 * token_count * TOPK // (2 * expert_count)
    slot_total = expert_count * capacity
    widened = latter_microbatch_activations.astype(jnp.float32)
    normed_b = (
        widened
        * lax.rsqrt(jnp.mean(widened * widened, axis=-1, keepdims=True) + NORM_EPS)
        * specialist_rescale_coefs.astype(jnp.float32)
    ).astype(jnp.bfloat16)
    flat_routes = specialist_picks.reshape(-1)
    assigned = flat_routes.shape[0]
    positions = jnp.arange(assigned, dtype=jnp.int32)
    earlier_same = (flat_routes[:, None] == flat_routes[None, :]) & (
        positions[None, :] < positions[:, None]
    )
    slot_rank = jnp.sum(earlier_same.astype(jnp.int32), axis=1)
    slot_of = flat_routes * capacity + slot_rank
    slot_ids = jnp.arange(slot_total, dtype=jnp.int32)
    placing = (slot_ids[:, None] == slot_of[None, :]).astype(jnp.bfloat16)
    placing = jnp.sum(placing.reshape(slot_total, token_count, TOPK), axis=2)
    outgoing = jnp.dot(placing, normed_b, preferred_element_type=jnp.float32).astype(jnp.bfloat16)
    outgoing = outgoing.reshape(ep_count, local_experts, capacity, model_width)
    slice_width = model_width // lax.axis_size(TP)
    my_columns = lax.dynamic_slice_in_dim(
        outgoing, lax.axis_index(TP) * slice_width, slice_width, 3
    )
    arrived = lax.all_to_all(my_columns, EP, split_axis=0, concat_axis=0, tiled=True)
    gathered_piece = lax.all_gather(arrived, TP, axis=3, tiled=True)
    gate_sum = jnp.einsum(
        "sejd,edf->sejf",
        gathered_piece,
        specialist_valve_matrix,
        preferred_element_type=jnp.float32,
    )
    up_sum = jnp.einsum(
        "sejd,edf->sejf",
        gathered_piece,
        specialist_expand_matrix,
        preferred_element_type=jnp.float32,
    )
    hidden = (jax.nn.silu(gate_sum) * up_sum).astype(jnp.bfloat16)
    partial_out = jnp.einsum(
        "sejf,efd->sejd", hidden, specialist_contract_matrix, preferred_element_type=jnp.float32
    )
    summed = (
        summed_rows(partial_out.astype(jnp.bfloat16), TP, 3)
        .astype(jnp.float32)
        .astype(jnp.bfloat16)
    )
    returned = lax.all_to_all(summed, EP, split_axis=0, concat_axis=0, tiled=True)
    returned = returned.reshape(slot_total, -1)
    token_slots = slot_of.reshape(token_count, TOPK)
    combined = jnp.zeros((token_count, returned.shape[1]), jnp.float32)
    for pick_index in range(TOPK):
        selecting = (token_slots[:, pick_index][:, None] == slot_ids[None, :]).astype(jnp.bfloat16)
        chosen_rows = jnp.dot(selecting, returned, preferred_element_type=jnp.float32)
        combined = combined + chosen_rows * selected_specialist_coefs[:, pick_index][:, None]
    mixed_b = combined.astype(jnp.bfloat16)
    return (mixed_a, mixed_b)


def solution(mesh):
    split = Mesh(mesh.devices.reshape(8, 4, 8, 2), ("ep_0", "ep_1", "tp_0", "tp_1"))
    in_specs = (
        P(EP, TP),
        P(EP, TP),
        P(EP, TP),
        P(EP, TP),
        P(EP, TP),
        P(EP, TP),
        P(None, TP),
        P(None, TP),
        P(None, TP),
        P(TP),
        P(TP),
        P(TP),
        P(TP),
        P(TP, None),
        P(EP, None),
        P(),
        P(EP, None, TP),
        P(EP, None, TP),
        P(EP, TP, None),
        P(EP, None),
        P(EP, None),
    )
    out_specs = (P(EP_TP, None), P(EP, TP))
    return jax.shard_map(local, mesh=split, in_specs=in_specs, out_specs=out_specs, check_vma=False)
```

profile of v0, /device:TPU:1, one launch (start us, length us, event | category | flops | bytes accessed | tf_op | source)
XLA Modules:
  0.0 217.2 jit_solution(4881775239269224496)
XLA Ops:
  7.2 0.9 copy.135
  10.5 1.5 fusion.40
  12.1 2.5 %convolution_convert_fusion.1 = bf16[768,2048]{1,0:T(8,128)(2,1)S(1)} fusion(bf16[768,256]{1,0:T(8,128)(2,1)S(1)} %fusion.71, bf16[256,2048]{1,0:T(8,128)(2,1)} %param.37, f32[2048]{0:T(1024)S(1)} %convert_element_type.381, f32[256]{0:T(256)S(1)} %add_rsqrt_fusion), kind=kOutput, calls=%fused_computation.46 | convolution fusion | flops 808976384 | bytes 4596736 | tf_op jit(solution)/shard_map/dot_general | solution.py:237
  14.7 23.6 %all_to_all.15 = bf16[32,1,24,128]{3,2,1,0:T(8,128)(2,1)} all-to-all(bf16[32,1,24,128]{3,2,1,0:T(8,128)(2,1)S(1)} %constant_dynamic-slice_fusion.2), channel_id=1, replica_groups=mesh['ep_0'=8,'ep_1'=4,'tp_0'=8,'tp_1'=2] {'ep_0','ep_1'}, dimensions={0} | all-to-all | bytes 393216 | tf_op jit(solution)/shard_map/all_to_all | solution.py:243
  38.3 2.1 collective-permute-start
  40.5 3.1 %collective-permute-start.2 = (bf16[3,128]{1,0:T(4,128)(2,1)S(1)}, bf16[3,128]{1,0:T(4,128)(2,1)S(1)}, u32[]{:S(2)}, u32[]{:S(2)}) collective-permute-start(bf16[3,128]{1,0:T(4,128)(2,1)S(1)} %slice.198), channel_id=1, source_target_pairs={{0,16},{16,32},{32,48},{48,64},{64,80},{80,96},{96,112},{112,128},... | collective-permute-start | bytes 2312 | tf_op jit(solution)/shard_map/ppermute | solution.py:24
  43.8 1.2 reduce-window.6
  45.6 2.4 %collective-permute-start.1 = (bf16[3,128]{1,0:T(4,128)(2,1)S(1)}, bf16[3,128]{1,0:T(4,128)(2,1)S(1)}, u32[]{:S(2)}, u32[]{:S(2)}) collective-permute-start(bf16[3,128]{1,0:T(4,128)(2,1)S(1)} %slice.189), channel_id=1, source_target_pairs={{0,16},{16,32},{32,48},{48,64},{64,80},{80,96},{96,112},{112,128},... | collective-permute-start | bytes 2312 | tf_op jit(solution)/shard_map/ppermute | solution.py:24
  48.0 7.6 %all_gather.21 = bf16[4,1,4]{2,1,0:T(2,128)(2,1)S(1)} all-gather(bf16[1,1,4]{2,1,0:T(2,128)(2,1)S(1)} %slice.260), channel_id=1, replica_groups=mesh['ep_0'=8,'ep_1'=4,'tp_0'=8,'tp_1'=2] {'ep_1'}, dimensions={0}, use_global_device_ids=true | all-gather | bytes 40 | tf_op jit(solution)/shard_map/all_gather | solution.py:39
  55.7 10.8 %all_gather.22 = bf16[8,1,4]{2,1,0:T(2,128)(2,1)S(1)} all-gather(bf16[1,1,4]{2,1,0:T(2,128)(2,1)S(1)} %get-tuple-element.133), channel_id=1, replica_groups=mesh['ep_0'=8,'ep_1'=4,'tp_0'=8,'tp_1'=2] {'ep_0'}, dimensions={0}, use_global_device_ids=true | all-gather | bytes 72 | tf_op jit(solution)/shard_map/all_gather | solution.py:39
  68.2 15.7 %all-gather.3.cloned.1.call-done = bf16[32,1,24,2048]{3,2,0,1:T(8,128)(2,1)} async-done(((bf16[32,1,24,128]{3,2,0,1:T(8,128)(2,1)}), bf16[32,1,24,2048]{3,2,0,1:T(8,128)(2,1)}) %all-gather.3.cloned.1.call-update) | async-done | bytes 3145744 | tf_op jit(solution)/shard_map/all_gather | solution.py:244
  83.9 4.1 %fusion.44 = f32[32,1,24,256]{3,2,0,1:T(8,128)} fusion(bf16[32,1,24,2048]{3,2,0,1:T(8,128)(2,1)} %all-gather.3.cloned.1.call-done, bf16[1,2048,256]{2,1,0:T(8,128)(2,1)} %param.39), kind=kOutput, calls=%fused_computation.60 | convolution fusion | flops 805306368 | bytes 4980736 | tf_op jit(solution)/shard_map/sejd,edf->sejf/dot_general | solution.py:245
  87.9 7.5 %fusion.39 = bf16[32,1,24,2048]{3,2,0,1:T(8,128)(2,1)} fusion(bf16[1,256,2048]{2,1,0:T(8,128)(2,1)S(1)} %copy-done, bf16[32,1,24,2048]{3,2,0,1:T(8,128)(2,1)} %all-gather.3.cloned.1.call-done, bf16[1,2048,256]{2,1,0:T(8,128)(2,1)} %param.40, f32[32,1,24,256]{3,2,0,1:T(8,128)} %fusion.44), kind=kOutput, calls=%fused_computation.51 | convolution fusion | flops 1613365248 | bytes 9175040 | tf_op jit(solution)/shard_map/sejf,efd->sejd/dot_general | solution.py:258
  95.4 1.0 copy-done.1
  96.4 16.0 %while.13 = (s32[]{:T(128)}, f32[1,4,64,128]{3,2,1,0:T(8,128)S(1)}, f32[4,64,1,4,64]{1,0,4,3,2:T(4,128)S(1)}, f32[4,64,1,4]{3,1,2,0:T(8,128)S(1)}, f32[4,64,1,4,...) while((s32[]{:T(128)}, f32[1,4,64,128]{3,2,1,0:T(8,128)S(1)}, ...), condition=%wide.region_2.3_spmd.clone, body=%wide.region_0.2_spmd.clone.sunk | while | flops 11800579 | bytes 1400524 | solution.py:173
  97.4 2.8 %dynamic_update_slice.6 = f32[4,64,1,4,64]{1,0,4,3,2:T(4,128)S(1)} dynamic-update-slice(f32[4,64,1,4,64]{1,0,4,3,2:T(4,128)S(1)} %get-tuple-element.209, f32[1,64,1,4,64]{1,0,4,3,2:T(1,128)S(1)} %bitcast.305, s32[]{:T(128)} %get-tuple-element.207, s32[]{:T(128)} %constant.33.clone.1..sunk, s32[]{:T(128)} %constant.33.clone.1..sunk, s32[]{:T(128)} %constant.33.clone.1..sunk, s32[]{:T(128)} %constant.33.clone.1..sunk) | dynamic-update-slice | bytes 131076 | tf_op jit(solution)/shard_map/while/body/jit(dynamic_update_index_in_dim)/dynamic_update_slice | solution.py:173
  101.4 2.8 %dynamic_update_slice.6 = f32[4,64,1,4,64]{1,0,4,3,2:T(4,128)S(1)} dynamic-update-slice(f32[4,64,1,4,64]{1,0,4,3,2:T(4,128)S(1)} %get-tuple-element.209, f32[1,64,1,4,64]{1,0,4,3,2:T(1,128)S(1)} %bitcast.305, s32[]{:T(128)} %get-tuple-element.207, s32[]{:T(128)} %constant.33.clone.1..sunk, s32[]{:T(128)} %constant.33.clone.1..sunk, s32[]{:T(128)} %constant.33.clone.1..sunk, s32[]{:T(128)} %constant.33.clone.1..sunk) | dynamic-update-slice | bytes 131076 | tf_op jit(solution)/shard_map/while/body/jit(dynamic_update_index_in_dim)/dynamic_update_slice | solution.py:173
  105.4 2.8 %dynamic_update_slice.6 = f32[4,64,1,4,64]{1,0,4,3,2:T(4,128)S(1)} dynamic-update-slice(f32[4,64,1,4,64]{1,0,4,3,2:T(4,128)S(1)} %get-tuple-element.209, f32[1,64,1,4,64]{1,0,4,3,2:T(1,128)S(1)} %bitcast.305, s32[]{:T(128)} %get-tuple-element.207, s32[]{:T(128)} %constant.33.clone.1..sunk, s32[]{:T(128)} %constant.33.clone.1..sunk, s32[]{:T(128)} %constant.33.clone.1..sunk, s32[]{:T(128)} %constant.33.clone.1..sunk) | dynamic-update-slice | bytes 131076 | tf_op jit(solution)/shard_map/while/body/jit(dynamic_update_index_in_dim)/dynamic_update_slice | solution.py:173
  109.4 2.8 %dynamic_update_slice.6 = f32[4,64,1,4,64]{1,0,4,3,2:T(4,128)S(1)} dynamic-update-slice(f32[4,64,1,4,64]{1,0,4,3,2:T(4,128)S(1)} %get-tuple-element.209, f32[1,64,1,4,64]{1,0,4,3,2:T(1,128)S(1)} %bitcast.305, s32[]{:T(128)} %get-tuple-element.207, s32[]{:T(128)} %constant.33.clone.1..sunk, s32[]{:T(128)} %constant.33.clone.1..sunk, s32[]{:T(128)} %constant.33.clone.1..sunk, s32[]{:T(128)} %constant.33.clone.1..sunk) | dynamic-update-slice | bytes 131076 | tf_op jit(solution)/shard_map/while/body/jit(dynamic_update_index_in_dim)/dynamic_update_slice | solution.py:173
  112.9 10.6 %all-gather = bf16[4,4,64,128]{3,2,1,0:T(8,128)(2,1)S(1)} all-gather(bf16[1,4,64,128]{3,2,1,0:T(8,128)(2,1)S(1)} %convert_element_type.353), channel_id=2, replica_groups=mesh['ep_0'=8,'ep_1'=4,'tp_0'=8,'tp_1'=2] {'ep_1'}, dimensions={0}, use_global_device_ids=true | all-gather | bytes 327680 | tf_op jit(solution)/shard_map/all_gather | solution.py:39
  123.6 22.6 %all_gather.25 = bf16[8,1,4,64,128]{4,3,2,1,0:T(8,128)(2,1)S(1)} all-gather(bf16[1,1,4,64,128]{4,3,2,1,0:T(8,128)(2,1)S(1)} %fusion.134), channel_id=1, replica_groups=mesh['ep_0'=8,'ep_1'=4,'tp_0'=8,'tp_1'=2] {'ep_0'}, dimensions={0}, use_global_device_ids=true | all-gather | bytes 589824 | tf_op jit(solution)/shard_map/all_gather | solution.py:39
  147.0 2.7 %convolution_convert_fusion.2 = bf16[256,2048]{1,0:T(8,128)(2,1)} fusion(bf16[256,2048]{1,0:T(8,128)(2,1)} %param.36, f32[256]{0:T(256)S(1)} %convert_element_type.375, f32[256]{0:T(256)S(1)} %add_rsqrt_fusion.1, f32[256,256]{1,0:T(8,128)S(1)} %copy.134, bf16[256,256]{1,0:T(8,128)(2,1)S(1)} %copy-done.3), kind=kOutput, calls=%fused_computation.54 | convolution fusion | flops 269549568 | bytes 2492416 | tf_op jit(solution)/shard_map/dot_general | solution.py:207
  149.7 11.0 %all-to-all-start = ((bf16[16,16,2048]{2,1,0:T(8,128)(2,1)}), bf16[16,16,2048]{2,1,0:T(8,128)(2,1)}, u32[]{:S(2)}, u32[]{:S(2)}) async-start(bf16[16,16,2048]{2,1,0:T(8,128)(2,1)} %bitcast.49), calls=%async_computation | async-start | bytes 2097152 | tf_op jit(solution)/shard_map/all_to_all | solution.py:61
  161.0 3.8 %copy.143 = bf16[32,1,24,256]{2,0,1,3:T(8,128)(2,1)S(1)} copy(bf16[32,1,24,256]{3,2,0,1:T(8,128)(2,1)} %reduce-scatter.5.cloned.1.call-done) | data formatting | bytes 786432
  164.8 4.2 %reshape.641 = bf16[256,768]{1,0:T(8,128)(2,1)} reshape(bf16[256,1,32,24]{3,2,1,0:T(8,128)(2,1)S(1)} %bitcast.307) | data formatting | bytes 786432
  169.0 16.5 %reduce-scatter.7.cloned.1.call-done = bf16[128,768]{1,0:T(8,128)(2,1)} async-done(((bf16[256,768]{1,0:T(8,128)(2,1)}), bf16[128,768]{1,0:T(8,128)(2,1)}) %reduce-scatter.7.cloned.1.call-update) | async-done | bytes 196624
  185.5 2.6 %reshape.642 = bf16[128,1,32,24]{3,2,1,0:T(8,128)(2,1)S(1)} reshape(bf16[128,768]{1,0:T(8,128)(2,1)} %reduce-scatter.7.cloned.1.call-done) | data formatting | bytes 393216
  188.2 1.7 copy.144
  189.9 8.9 %all-to-all-start.2 = ((bf16[32,1,24,128]{3,2,1,0:T(8,128)(2,1)}), bf16[32,1,24,128]{3,2,1,0:T(8,128)(2,1)S(1)}, u32[]{:S(2)}, u32[]{:S(2)}) async-start(bf16[32,1,24,128]{3,2,1,0:T(8,128)(2,1)} %bitcast.73), calls=%async_computation.3 | async-start | bytes 393216 | tf_op jit(solution)/shard_map/all_to_all | solution.py:266
  198.8 2.0 reduce_sum.54
  200.9 8.6 %all-to-all-done.2 = bf16[32,1,24,128]{3,2,1,0:T(8,128)(2,1)S(1)} async-done(((bf16[32,1,24,128]{3,2,1,0:T(8,128)(2,1)}), bf16[32,1,24,128]{3,2,1,0:T(8,128)(2,1)S(1)}, u32[]{:S(2)}, u32[]{:S(2)}) %all-to-all-start.2) | async-done | bytes 196640 | tf_op jit(solution)/shard_map/all_to_all | solution.py:266
  209.8 0.9 fusion.63
  (153 shorter events, 11.1 us)
Async XLA Ops:
  7.2 80.8 %copy-start = (bf16[1,256,2048]{2,1,0:T(8,128)(2,1)S(1)}, bf16[1,256,2048]{2,1,0:T(8,128)(2,1)}, u32[]{:S(2)}) copy-start(bf16[1,256,2048]{2,1,0:T(8,128)(2,1)} %param.41) | copy-start | bytes 3145732
  7.2 76.7 %all-gather.3.cloned.1.call-start = ((), (), s32[]{:S(2)}) async-start(), calls=%async_computation.5 | async-start | bytes 3342336 | tf_op jit(solution)/shard_map/all_gather | solution.py:244
  12.0 26.3 %copy-start.2 = (bf16[256,256]{1,0:T(8,128)(2,1)S(1)}, bf16[256,256]{1,0:T(8,128)(2,1)}, u32[]{:S(2)}) copy-start(bf16[256,256]{1,0:T(8,128)(2,1)} %param.23) | copy-start | bytes 393220
  12.0 28.4 %copy-start.4 = (bf16[256,128]{1,0:T(8,128)(2,1)S(1)}, bf16[256,128]{1,0:T(8,128)(2,1)}, u32[]{:S(2)}) copy-start(bf16[256,128]{1,0:T(8,128)(2,1)} %param.25) | copy-start | bytes 196612
  12.0 31.6 %copy-start.13 = (f32[4]{0:T(128)S(1)}, f32[4]{0:T(128)}, u32[]{:S(2)}) copy-start(f32[4]{0:T(128)} %param.33) | copy-start | bytes 52
  12.0 31.6 %copy-start.7 = (f32[256,4]{0,1:T(4,128)S(1)}, f32[256,4]{0,1:T(4,128)}, u32[]{:S(2)}) copy-start(f32[256,4]{0,1:T(4,128)} %param.28) | copy-start | bytes 12292
  12.0 31.6 %copy-start.8 = (f32[256,4]{0,1:T(4,128)S(1)}, f32[256,4]{0,1:T(4,128)}, u32[]{:S(2)}) copy-start(f32[256,4]{0,1:T(4,128)} %param.27) | copy-start | bytes 12292
  12.1 31.6 %copy-start.12 = (f32[4]{0:T(128)S(1)}, f32[4]{0:T(128)}, u32[]{:S(2)}) copy-start(f32[4]{0:T(128)} %param.32) | copy-start | bytes 52
  12.1 33.1 %copy-start.5 = (bf16[256,128]{1,0:T(8,128)(2,1)S(1)}, bf16[256,128]{1,0:T(8,128)(2,1)}, u32[]{:S(2)}) copy-start(bf16[256,128]{1,0:T(8,128)(2,1)} %param.24) | copy-start | bytes 196612
  12.1 54.6 %copy-start.10 = (bf16[4,128]{1,0:T(4,128)(2,1)S(1)}, bf16[4,128]{1,0:T(4,128)(2,1)}, u32[]{:S(2)}) copy-start(bf16[4,128]{1,0:T(4,128)(2,1)} %param.31) | copy-start | bytes 3076
  12.1 54.6 %copy-start.11 = (bf16[4,128]{1,0:T(4,128)(2,1)S(1)}, bf16[4,128]{1,0:T(4,128)(2,1)}, u32[]{:S(2)}) copy-start(bf16[4,128]{1,0:T(4,128)(2,1)} %param.30) | copy-start | bytes 3076
  12.1 54.7 %copy-start.6 = (bf16[4,256]{1,0:T(4,128)(2,1)S(1)}, bf16[4,256]{1,0:T(4,128)(2,1)}, u32[]{:S(2)}) copy-start(bf16[4,256]{1,0:T(4,128)(2,1)} %param.29) | copy-start | bytes 6148
  12.1 54.9 %copy-start.14 = (bf16[256]{0:T(256)(128)(2,1)S(1)}, bf16[256]{0:T(256)(128)(2,1)}, u32[]{:S(2)}) copy-start(bf16[256]{0:T(256)(128)(2,1)} %param.35) | copy-start | bytes 1540
  38.3 122.7 %reduce-scatter.5.cloned.1.call-start = ((), (), s32[]{:S(2)}) async-start(), calls=%async_computation.6 | async-start | bytes 3538944 | tf_op jit(solution)/shard_map/reduce_scatter | solution.py:67
  38.3 29.0 %collective-permute-start = (bf16[3,256]{1,0:T(4,128)(2,1)S(1)}, bf16[3,256]{1,0:T(4,128)(2,1)S(1)}, u32[]{:S(2)}, u32[]{:S(2)}) collective-permute-start(bf16[3,256]{1,0:T(4,128)(2,1)S(1)} %slice.180), channel_id=1, source_target_pairs={{0,16},{16,32},{32,48},{48,64},{64,80},{80,96},{96,112},{112,128},... | collective-permute-start | bytes 4616 | tf_op jit(solution)/shard_map/ppermute | solution.py:24
  40.5 26.6 %collective-permute-start.2 = (bf16[3,128]{1,0:T(4,128)(2,1)S(1)}, bf16[3,128]{1,0:T(4,128)(2,1)S(1)}, u32[]{:S(2)}, u32[]{:S(2)}) collective-permute-start(bf16[3,128]{1,0:T(4,128)(2,1)S(1)} %slice.198), channel_id=1, source_target_pairs={{0,16},{16,32},{32,48},{48,64},{64,80},{80,96},{96,112},{112,128},... | collective-permute-start | bytes 2312 | tf_op jit(solution)/shard_map/ppermute | solution.py:24
  45.6 21.5 %collective-permute-start.1 = (bf16[3,128]{1,0:T(4,128)(2,1)S(1)}, bf16[3,128]{1,0:T(4,128)(2,1)S(1)}, u32[]{:S(2)}, u32[]{:S(2)}) collective-permute-start(bf16[3,128]{1,0:T(4,128)(2,1)S(1)} %slice.189), channel_id=1, source_target_pairs={{0,16},{16,32},{32,48},{48,64},{64,80},{80,96},{96,112},{112,128},... | collective-permute-start | bytes 2312 | tf_op jit(solution)/shard_map/ppermute | solution.py:24
  95.4 1.0 copy-start.1
  96.4 49.8 %copy-start.15 = (f32[4]{0:T(128)S(1)}, f32[4]{0:T(128)}, u32[]{:S(2)}) copy-start(f32[4]{0:T(128)} %param.34) | copy-start | bytes 52
  112.4 34.4 %copy-start.3 = (bf16[256,256]{1,0:T(8,128)(2,1)S(1)}, bf16[256,256]{1,0:T(8,128)(2,1)}, u32[]{:S(2)}) copy-start(bf16[256,256]{1,0:T(8,128)(2,1)} %param.26) | copy-start | bytes 393220
  149.7 40.2 %all-to-all-start = ((bf16[16,16,2048]{2,1,0:T(8,128)(2,1)}), bf16[16,16,2048]{2,1,0:T(8,128)(2,1)}, u32[]{:S(2)}, u32[]{:S(2)}) async-start(bf16[16,16,2048]{2,1,0:T(8,128)(2,1)} %bitcast.49), calls=%async_computation | async-start | bytes 2097152 | tf_op jit(solution)/shard_map/all_to_all | solution.py:61
  160.7 24.8 %reduce-scatter.7.cloned.1.call-start = ((), (), s32[]{:S(2)}) async-start(), calls=%async_computation.7 | async-start | bytes 589824
  164.8 34.1 %copy-start.9 = (f32[256,2]{0,1:T(2,128)S(1)}, f32[256,2]{0,1:T(2,128)}, u32[]{:S(2)}) copy-start(f32[256,2]{0,1:T(2,128)} %param.43) | copy-start | bytes 6148
  189.9 19.5 %all-to-all-start.2 = ((bf16[32,1,24,128]{3,2,1,0:T(8,128)(2,1)}), bf16[32,1,24,128]{3,2,1,0:T(8,128)(2,1)S(1)}, u32[]{:S(2)}, u32[]{:S(2)}) async-start(bf16[32,1,24,128]{3,2,1,0:T(8,128)(2,1)} %bitcast.73), calls=%async_computation.3 | async-start | bytes 393216 | tf_op jit(solution)/shard_map/all_to_all | solution.py:266
Sparse Core Ops, SparseCore 0:
  38.4 45.4 all-gather.2
  95.5 44.1 reduce-scatter.4
  169.2 16.3 reduce-scatter.6
where the time goes:
time: 218 us; the launch traced here: 217 us
  blocking collectives  75.3 us (35%)
  waiting for transfers between devices  40.9 us (19%)
  local copies, waits for them, and re-layouts  28.7 us (13%)
  starting transfers between devices  27.9 us (13%)
  matrix products  21 us (10%)
  between operations  14.4 us (7%)
  other arithmetic  8.82 us (4%)
    all_gather x4, blocking collectives, carried_in(): lax.all_gather(part.astype(kind), axis)  51.7 us
    all_to_all x1, blocking collectives, local(): lax.all_to_all(my_columns, EP, split_axis=0, concat_axis=0, tiled=True)  23.6 us
    unnamed x4, waiting for transfers between devices  16.6 us
    all_gather x1, waiting for transfers between devices, local(): gathered_piece = lax.all_gather(arrived, TP, axis=3, tiled=True)  15.7 us
    unnamed x37, local copies, waits for them, and re-layouts  14.4 us
    dynamic_update_slice x4, local copies, waits for them, and re-layouts, local(): lax.scan(block_step, start_state, (as_blocks(scaled_x), as_blocks(conv_b_...  11.2 us
    all_to_all x1, starting transfers between devices, summed_on_arrival(): lax.all_to_all(tiles, axis, split_axis=0, concat_axis=0, tiled=True)  11 us
    all_to_all x1, starting transfers between devices, local(): lax.all_to_all(summed, EP, split_axis=0, concat_axis=0, tiled=True)  8.89 us
  transfers between devices with their start and end apart: 8, of which 3 were waited for; matrix products, arithmetic and copies ran while one was open for 17% of the time, Pallas kernels for 0%

commit v1 on v0

v1 whole, which is shorter than its diff:
```python
import jax
import jax.numpy as jnp
from jax import lax
from jax.experimental import pallas as pl
from jax.experimental.pallas import tpu as pltpu
from jax.sharding import Mesh
from jax.sharding import PartitionSpec as P

HEADS = 64
HEAD_DIM = 64
SHARING_CLUSTERS = 16
STATE = 128
TOPK = 2
EP = ("ep_0", "ep_1")
TP = ("tp_0", "tp_1")
EP_TP = ("ep_0", "ep_1", "tp_0", "tp_1")
RIM = 8
PIECE = 8

NORM_EPS = 1e-06
F32 = jnp.float32
BF16 = jnp.bfloat16
VMEM = pl.BlockSpec(memory_space=pltpu.VMEM)
SMEM = pl.BlockSpec(memory_space=pltpu.SMEM)


def call(body, outs, ins, flops, scratch=(), smem=0):
    return pl.pallas_call(
        body,
        out_shape=outs,
        in_specs=[SMEM] * smem + [VMEM] * (len(ins) - smem),
        out_specs=jax.tree.map(lambda _: VMEM, outs),
        scratch_shapes=scratch,
        cost_estimate=pl.CostEstimate(flops=flops, bytes_accessed=1 << 20, transcendentals=0),
    )(*ins)


def shaped(*shape, dtype=BF16):
    return jax.ShapeDtypeStruct(shape, dtype)


def iota(shape, dim):
    return lax.broadcasted_iota(jnp.int32, shape, dim)


def silu(v):
    return v * jax.nn.sigmoid(v)


def dot(a, b, contract=(1, 0)):
    return lax.dot_general(
        a, b, (((contract[0],), (contract[1],)), ((), ())), preferred_element_type=F32
    )


def spread(columns, width):
    lane_head = iota((columns.shape[0], 4 * width), 1) // width
    wide = columns[:, 0:1]
    for head in range(1, 4):
        wide = jnp.where(lane_head == head, columns[:, head : head + 1], wide)
    return wide


def front_body(
    place,
    tokens,
    token_gain,
    picks,
    x_in,
    b_in,
    c_in,
    rim,
    x_taps,
    b_taps,
    c_taps,
    strides,
    extra,
    offset,
    speed,
    send,
    x_out,
    b_out,
    c_out,
    columns_out,
    rows_out,
    slots_out,
    joined,
):
    count, width = x_in.shape
    state = b_in.shape[1]
    experts, rows, lanes = send.shape
    capacity = rows - 2 * PIECE

    joined[0:RIM, :] = rim[...].astype(F32)
    joined[RIM:, 0:width] = x_in[...].astype(F32)
    joined[RIM:, width : width + state] = b_in[...].astype(F32)
    joined[RIM:, width + state :] = c_in[...].astype(F32)

    def filtered(first, size, taps_ref):
        taps = taps_ref[...].astype(F32)
        total = None
        for j in range(taps.shape[0]):
            start = RIM - taps.shape[0] + 1 + j
            term = taps[j : j + 1] * joined[start : start + count, first : first + size]
            total = term if total is None else total + term
        return silu(total)

    x = filtered(0, width, x_taps)
    b = filtered(width, state, b_taps).astype(BF16)
    c = filtered(width + state, state, c_taps).astype(BF16)
    x_out[...] = x
    b_out[...] = b
    c_out[...] = c

    raw = strides[...] + offset[...]
    step = jnp.maximum(raw, 0.0) + jnp.log1p(jnp.exp(-jnp.abs(raw)))
    total = -jnp.exp(speed[...]) * step + extra[...]
    both = jnp.concatenate([total, step], axis=0)
    lane = iota(both.shape, 1)
    shift = 1
    while shift < count:
        moved = jnp.where((lane >= shift), pltpu.roll(both, shift, axis=1), 0.0)
        both = jnp.where(iota(both.shape, 0) < 4, both + moved, both)
        shift *= 2
    columns = both.T
    rows_out[...] = both
    columns_out[...] = columns
    running, step_column = columns[:, 0:4], columns[:, 4:8]
    last = columns[count - 1 : count, 0:4]
    weight = step_column * jnp.exp(last - running)
    weighted = (x * spread(weight, HEAD_DIM)).astype(BF16)
    end_state = dot(weighted, b, (0, 0)).astype(BF16)
    high = last.astype(BF16).astype(F32)
    low = last - high
    half = iota((PIECE, lanes), 1) < lanes // 2

    data = tokens[...].astype(F32)
    scale = lax.rsqrt(jnp.mean(data * data, axis=1, keepdims=True) + NORM_EPS)
    first = pl.multiple_of(place[0] * lanes, lanes)
    chosen = tokens[:, pl.ds(first, lanes)].astype(F32)
    gain = token_gain[:, pl.ds(first, lanes)].astype(F32)
    chosen = (chosen * scale * gain).astype(BF16)
    token_count = tokens.shape[0]
    expert = iota((experts, token_count), 0)
    earlier = (
        iota((token_count, token_count), 0) < iota((token_count, token_count), 1)
    ).astype(BF16)
    base = jnp.zeros((experts, 1), F32)
    slot_ids = iota((experts * capacity, token_count), 0)
    placing = None
    for k in range(TOPK):
        pick = picks[k : k + 1, :]
        named = (expert == pick).astype(F32)
        rank = base + dot(named.astype(BF16), earlier)
        rank = jnp.sum(named * rank, axis=0, keepdims=True)
        slot = pick * capacity + rank.astype(jnp.int32)
        slots_out[k : k + 1, :] = slot
        base = base + jnp.sum(named, axis=1, keepdims=True)
        hit = slot_ids == slot
        placing = hit if placing is None else placing | hit
    routed = dot(placing.astype(F32).astype(BF16), chosen).astype(BF16)
    for e in range(experts):
        head = e * PIECE // HEAD_DIM
        send[e, 0:capacity, :] = routed[e * capacity : (e + 1) * capacity]
        send[e, capacity : capacity + PIECE, :] = end_state[e * PIECE : (e + 1) * PIECE]
        send[e, capacity + PIECE :, :] = jnp.where(
            half, high[:, head : head + 1], low[:, head : head + 1]
        ).astype(BF16)


def enter_body(got, enter, tokens):
    sources, rows, lanes = got.shape
    capacity = rows - 2 * PIECE
    tokens[...] = got[:, 0:capacity, :].reshape(sources * capacity, lanes)
    size = sources * PIECE
    piece = got[:, capacity : capacity + PIECE, :].reshape(size, lanes)
    logs = got[:, capacity + PIECE :, :].reshape(size, lanes).astype(F32)
    logs = logs[:, 0:1] + logs[:, lanes // 2 : lanes // 2 + 1]
    row, column = iota((size, size), 0), iota((size, size), 1)
    before = column // PIECE < row // PIECE
    mean = jnp.where(before, 1.0 / PIECE, 0.0).astype(BF16)
    wide = jnp.broadcast_to(logs, (size, lanes))
    high = wide.astype(BF16)
    mid = (wide - high.astype(F32)).astype(BF16)
    low = (wide - high.astype(F32) - mid.astype(F32)).astype(BF16)
    earlier = dot(mean, high) + dot(mean, mid) + dot(mean, low)
    through = (earlier + wide).T[0:1, :]
    keep = before & (column % PIECE == row % PIECE)
    gap = jnp.where(keep, earlier[:, 0:1] - through, 0.0)
    decay = jnp.where(keep, jnp.exp(gap), 0.0)
    decay_high = decay.astype(BF16)
    decay_low = (decay - decay_high.astype(F32)).astype(BF16)
    result = dot(decay_high, piece) + dot(decay_low, piece)
    enter[...] = result.astype(BF16).reshape(sources, PIECE, lanes)


def inside_body(x_ref, b_ref, c_ref, columns, rows, bypass, out):
    count = x_ref.shape[0]
    scores = dot(c_ref[...], b_ref[...], (1, 1))
    causal = iota((count, count), 0) >= iota((count, count), 1)
    for head in range(4):
        part = slice(head * HEAD_DIM, (head + 1) * HEAD_DIM)
        gap = columns[:, head : head + 1] - rows[head : head + 1, :]
        weights = jnp.where(causal, jnp.exp(jnp.where(causal, gap, 0.0)), 0.0)
        x = x_ref[:, part]
        scaled = (x * columns[:, 4 + head : 5 + head]).astype(BF16)
        inside = dot((scores * weights).astype(BF16), scaled)
        out[:, part] = inside + bypass[head] * x


def finish_body(place, y, c, columns, enter, valve, gain, result, mine, other, normed):
    carried = dot(c[...], enter[...], (1, 1))
    carried = carried * spread(jnp.exp(columns[:, 0:4]), HEAD_DIM)
    gated = (y[...] + carried) * silu(valve[...].astype(F32))
    scale = lax.rsqrt(jnp.mean(gated * gated, axis=1, keepdims=True) + NORM_EPS)
    normed[...] = gated * scale * gain[...].astype(F32)
    chips, rows, width = mine.shape
    for target, core in ((mine, place[0]), (other, 1 - place[0])):
        parts = [
            normed[pl.ds(pl.multiple_of(2 * rows * k + rows * core, 8), rows), :]
            for k in range(chips)
        ]
        left = jnp.concatenate(parts, axis=0).astype(BF16)
        block = 512
        for first in range(0, width, block):
            product = dot(left, result[:, first : first + block]).astype(BF16)
            target[:, :, first : first + block] = product.reshape(chips, rows, block)


def expert_body(place, own, far, valve, expand, contract, mine, other):
    chips, total, lanes = own.shape
    core = place[0]
    half = chips * lanes
    hidden_width = valve.shape[1]
    block = 256
    near_rows = pl.ds(pl.multiple_of(core * half, half), half)
    far_rows = pl.ds(pl.multiple_of((1 - core) * half, half), half)

    def columns_of(which):
        return jnp.concatenate(
            [
                contract[:, pl.ds(pl.multiple_of((2 * k + which) * lanes, lanes), lanes)]
                for k in range(chips)
            ],
            axis=1,
        )

    def step(i, _):
        at = pl.ds(pl.multiple_of(i * block, block), block)
        near_x = jnp.concatenate([own[k, at, :] for k in range(chips)], axis=1)
        far_x = jnp.concatenate([far[k, at, :] for k in range(chips)], axis=1)
        gate = dot(near_x, valve[near_rows, :]) + dot(far_x, valve[far_rows, :])
        up = dot(near_x, expand[near_rows, :]) + dot(far_x, expand[far_rows, :])
        hidden = (silu(gate) * up).astype(BF16)
        for target, which in ((mine, core), (other, 1 - core)):
            product = dot(hidden, columns_of(which)).astype(BF16)
            for k in range(chips):
                target[k, at, :] = product[:, k * lanes : (k + 1) * lanes]
        return 0

    lax.fori_loop(0, total // block, step, 0)


def combine_body(got, slots, coefs, out):
    sources, capacity, lanes = got.shape
    rows = got[...].reshape(sources * capacity, lanes)
    slot_ids = iota((rows.shape[0], slots.shape[1]), 0)
    padded = jnp.concatenate([coefs[...]] * (8 // TOPK), axis=0)
    columns = padded.T
    total = None
    for k in range(TOPK):
        chosen = (slot_ids == slots[k : k + 1, :]).astype(F32).astype(BF16)
        term = dot(chosen, rows, (0, 0)) * columns[:, k : k + 1]
        total = term if total is None else total + term
    out[...] = total.astype(BF16)


def local(
    blender_incoming_features,
    entry_latent_matrix,
    exit_latent_matrix,
    unactivated_valve,
    presoftplus_strides,
    extra_attenuation,
    incoming_feature_kernel,
    entry_latent_kernel,
    exit_latent_kernel,
    stride_offset_vector,
    attenuation_speed_exponent,
    bypass_coef_vector,
    cluster_rescale_coefs,
    blender_result_matrix,
    latter_microbatch_activations,
    specialist_rescale_coefs,
    specialist_valve_matrix,
    specialist_expand_matrix,
    specialist_contract_matrix,
    specialist_picks,
    selected_specialist_coefs,
):
    ep_count, chips = lax.axis_size(EP), lax.axis_size("tp_0")
    chip, core = lax.axis_index("tp_0"), lax.axis_index("tp_1")
    count, width = blender_incoming_features.shape
    state = entry_latent_matrix.shape[1]
    token_count, model_width = latter_microbatch_activations.shape
    capacity = 3 * token_count * TOPK // (2 * ep_count)
    lanes = model_width // lax.axis_size(TP)
    total_rows = ep_count * capacity
    swap = [(0, 1), (1, 0)]
    core_at = core.reshape(1)

    rim = jnp.concatenate(
        [
            blender_incoming_features[count - RIM :],
            entry_latent_matrix[count - RIM :],
            exit_latent_matrix[count - RIM :],
        ],
        axis=1,
    )
    rim = lax.ppermute(rim, EP, [(i, i + 1) for i in range(ep_count - 1)])

    send, x, b, c, columns, rows, slots = call(
        front_body,
        (
            shaped(ep_count, capacity + 2 * PIECE, lanes),
            shaped(count, width, dtype=F32),
            shaped(count, state),
            shaped(count, state),
            shaped(count, 8, dtype=F32),
            shaped(8, count, dtype=F32),
            shaped(TOPK, token_count, dtype=jnp.int32),
        ),
        (
            (core * chips + chip).reshape(1),
            latter_microbatch_activations,
            specialist_rescale_coefs.reshape(1, -1),
            specialist_picks.T,
            blender_incoming_features,
            entry_latent_matrix,
            exit_latent_matrix,
            rim,
            incoming_feature_kernel,
            entry_latent_kernel,
            exit_latent_kernel,
            presoftplus_strides.T,
            extra_attenuation.T,
            stride_offset_vector.reshape(-1, 1),
            attenuation_speed_exponent.reshape(-1, 1),
        ),
        1 << 30,
        scratch=(pltpu.VMEM((RIM + count, width + 2 * state), F32),),
        smem=1,
    )
    got = lax.all_to_all(send, EP, 0, 0, tiled=True)
    enter, tokens = call(
        enter_body,
        (shaped(ep_count, PIECE, lanes), shaped(total_rows, lanes)),
        (got,),
        1 << 28,
    )
    own = lax.all_to_all(
        jnp.broadcast_to(tokens, (chips, total_rows, lanes)), "tp_0", 0, 0, tiled=True
    )
    enter = lax.all_to_all(enter, EP, 0, 0, tiled=True).reshape(width, state)
    y = inside(bypass_coef_vector, x, b, c, columns, rows)
    mine_a, other_a = call(
        finish_body,
        (shaped(chips, count // (2 * chips), model_width),) * 2,
        (
            core_at,
            y,
            c,
            columns,
            enter,
            unactivated_valve,
            cluster_rescale_coefs.reshape(1, -1),
            blender_result_matrix,
        ),
        1 << 31,
        scratch=(pltpu.VMEM((count, width), F32),),
        smem=1,
    )
    other_a = lax.ppermute(other_a, "tp_1", swap)
    parts_a = (mine_a.astype(F32) + other_a.astype(F32)).astype(BF16)
    parts_a = lax.all_to_all(parts_a, "tp_0", 0, 0, tiled=True)
    mixed_a = jnp.sum(parts_a.astype(F32), axis=0).astype(BF16)

    far = lax.ppermute(own, "tp_1", swap)
    mine, other = call(
        expert_body,
        (shaped(chips, total_rows, lanes),) * 2,
        (
            core_at,
            own,
            far,
            specialist_valve_matrix.reshape(model_width, -1),
            specialist_expand_matrix.reshape(model_width, -1),
            specialist_contract_matrix.reshape(-1, model_width),
        ),
        1 << 32,
        smem=1,
    )
    other = lax.ppermute(other, "tp_1", swap)
    parts = (mine.astype(F32) + other.astype(F32)).astype(BF16)
    parts = lax.all_to_all(parts, "tp_0", 0, 0, tiled=True)
    summed = jnp.sum(parts.astype(F32), axis=0).astype(BF16)
    returned = lax.all_to_all(
        summed.reshape(ep_count, capacity, lanes), EP, 0, 0, tiled=True
    )
    mixed_b = call(
        combine_body,
        shaped(token_count, lanes),
        (returned, slots, selected_specialist_coefs.T),
        1 << 28,
    )
    return (mixed_a, mixed_b)


def inside(bypass, x, b, c, columns, rows):
    def body(bypass, x, b, c, columns, rows, out):
        inside_body(x, b, c, columns, rows, bypass, out)

    return call(
        body,
        shaped(*x.shape, dtype=F32),
        (bypass, x, b, c, columns, rows),
        1 << 31,
        smem=1,
    )


def solution(mesh):
    split = Mesh(mesh.devices.reshape(8, 4, 8, 2), ("ep_0", "ep_1", "tp_0", "tp_1"))
    in_specs = (
        P(EP, TP),
        P(EP, TP),
        P(EP, TP),
        P(EP, TP),
        P(EP, TP),
        P(EP, TP),
        P(None, TP),
        P(None, TP),
        P(None, TP),
        P(TP),
        P(TP),
        P(TP),
        P(TP),
        P(TP, None),
        P(EP, None),
        P(),
        P(EP, None, TP),
        P(EP, None, TP),
        P(EP, TP, None),
        P(EP, None),
        P(EP, None),
    )
    out_specs = (P(EP_TP, None), P(EP, TP))
    return jax.shard_map(local, mesh=split, in_specs=in_specs, out_specs=out_specs, check_vma=False)
```

time: 218 us -> 205 us (0.940)
  Pallas kernels: 0 us -> 21.8 us
  matrix products: 21 us -> 0 us
  waiting for transfers between devices: 40.9 us -> 59.1 us
  local copies, waits for them, and re-layouts: 28.7 us -> 10.7 us
  between operations: 14.4 us -> 0.73 us
  starting transfers between devices: 27.9 us -> 35.8 us
  blocking collectives: 75.3 us -> 68.8 us
  other arithmetic: 8.82 us -> 6.61 us
    all_gather x4 -> x0, blocking collectives: 51.7 us -> none  [carried_in(): lax.all_gather(part.astype(kind), axis)]
    all_to_all x2 -> x4, waiting for transfers between devices: 8.57 us -> 54.3 us  [the longest x1 24.6 us: local(): parts = lax.all_to_all(parts, 'tp_0', 0, 0, tiled=True)]
    all_to_all x1 -> x2, blocking collectives: 23.6 us -> 68.8 us  [the longest x1 43.6 us: local(): lax.all_to_all(jnp.broadcast_to(tokens, (chips, total_rows, lanes)), 'tp_...]
    pallas_call x0 -> x6, Pallas kernels: none -> 21.8 us  [call(): pl.pallas_call(body, out_shape=outs, in_specs=[SMEM] * smem + [VMEM] * (l...]
    dot_general x23 -> x0, matrix products: 21 us -> none  [the longest x1 7.46 us: local(): jnp.einsum('sejf,efd->sejd', hidden, specialist_contract_matrix, preferre...]
    unnamed x4 -> x0, waiting for transfers between devices: 16.6 us -> none
    all_gather x1 -> x0, waiting for transfers between devices: 15.7 us -> none  [local(): gathered_piece = lax.all_gather(arrived, TP, axis=3, tiled=True)]
    unnamed x37 -> x12, local copies, waits for them, and re-layouts: 14.4 us -> 3.06 us
  transfers between devices with their start and end apart: 8 -> 8, of which waited for: 3 -> 6; matrix products, arithmetic and copies ran while one was open for 17% -> 5% of each run, Pallas kernels for 0% -> 3%
where the time goes in v1:
time: 205 us; the launch traced here: 204 us
  blocking collectives  68.8 us (34%)
  waiting for transfers between devices  59.1 us (29%)
  starting transfers between devices  35.8 us (17%)
  Pallas kernels  21.8 us (11%)
  local copies, waits for them, and re-layouts  10.7 us (5%)
  other arithmetic  6.61 us (3%)
    all_to_all x1, blocking collectives, local(): lax.all_to_all(jnp.broadcast_to(tokens, (chips, total_rows, lanes)), 'tp_...  43.6 us
    all_to_all x1, blocking collectives, local(): got = lax.all_to_all(send, EP, 0, 0, tiled=True)  25.2 us
    all_to_all x1, waiting for transfers between devices, local(): parts = lax.all_to_all(parts, 'tp_0', 0, 0, tiled=True)  24.6 us
    pallas_call x6, Pallas kernels, call(): pl.pallas_call(body, out_shape=outs, in_specs=[SMEM] * smem + [VMEM] * (l...  21.8 us
    all_to_all x1, waiting for transfers between devices, local(): parts_a = lax.all_to_all(parts_a, 'tp_0', 0, 0, tiled=True)  14.1 us
    all_to_all x1, waiting for transfers between devices, local(): lax.all_to_all(summed.reshape(ep_count, capacity, lanes), EP, 0, 0, tiled...  9.77 us
    all_to_all x1, starting transfers between devices, local(): lax.all_to_all(summed.reshape(ep_count, capacity, lanes), EP, 0, 0, tiled...  8.3 us
    ppermute x1, starting transfers between devices, local(): far = lax.ppermute(own, 'tp_1', swap)  5.85 us
  transfers between devices with their start and end apart: 8, of which 6 were waited for; matrix products, arithmetic and copies ran while one was open for 5% of the time, Pallas kernels for 3%

profile of v1, /device:TPU:1, one launch (start us, length us, event | category | flops | bytes accessed | tf_op | source)
XLA Modules:
  0.0 203.6 jit_solution(10911575924612309016)
XLA Ops:
  2.0 0.7 slice.9
  2.7 3.9 %collective-permute-start = (bf16[8,512]{1,0:T(8,128)(2,1)S(1)}, bf16[8,512]{1,0:T(8,128)(2,1)S(1)}, u32[]{:S(2)}, u32[]{:S(2)}) collective-permute-start(bf16[8,512]{1,0:T(8,128)(2,1)S(1)} %pad_maximum_fusion), channel_id=1, source_target_pairs={{0,16},{16,32},{32,48},{48,64},{64,80},{80,96},{96,112},{112,128},... | collective-permute-start | bytes 24584 | tf_op jit(solution)/shard_map/ppermute | solution.py:320
  6.6 1.3 copy.23.offset
  7.9 1.3 copy.24.speed
  9.2 1.3 reshape.39.token_gain
  11.1 4.2 %shard_map.212 = (bf16[32,40,128]{2,1,0:T(8,128)(2,1)}, f32[256,256]{1,0:T(8,128)}, bf16[256,128]{1,0:T(8,128)(2,1)}, bf16[256,128]{1,0:T(8,128)(2,1)}, f32[256,...) custom-call(s32[1]{0:T(128)} %bitcast.1.place, bf16[256,2048]{1,0:T(8,128)(2,1)} %tokens.1, ...), custom_call_target="tpu_custom_call" | custom-call | flops 1073741824 | bytes 1048576 | tf_op jit(solution)/shard_map/pallas_call | solution.py:28
  15.3 25.2 %all_to_all.30.got = bf16[32,40,128]{2,1,0:T(8,128)(2,1)} all-to-all(bf16[32,40,128]{2,1,0:T(8,128)(2,1)} %get-tuple-element.20), channel_id=1, replica_groups=mesh['ep_0'=8,'ep_1'=4,'tp_0'=8,'tp_1'=2] {'ep_0','ep_1'}, dimensions={0} | all-to-all | bytes 655360 | tf_op jit(solution)/shard_map/all_to_all | solution.py:354
  40.5 2.3 %shard_map.214 = (bf16[32,8,128]{2,1,0:T(8,128)(2,1)}, bf16[768,128]{1,0:T(8,128)(2,1)}) custom-call(bf16[32,40,128]{2,1,0:T(8,128)(2,1)} %all_to_all.30.got), custom_call_target="tpu_custom_call" | custom-call | flops 268435456 | bytes 1048576 | tf_op jit(solution)/shard_map/pallas_call | solution.py:28
  42.8 1.1 broadcast_in_dim.3
  44.0 43.6 %all_to_all.31.own = bf16[8,768,128]{2,1,0:T(8,128)(2,1)S(1)} all-to-all(bf16[8,768,128]{2,1,0:T(8,128)(2,1)S(1)} %broadcast_in_dim.3), channel_id=1, replica_groups=mesh['ep_0'=8,'ep_1'=4,'tp_0'=8,'tp_1'=2] {'tp_0'}, dimensions={0} | all-to-all | bytes 3145728 | tf_op jit(solution)/shard_map/all_to_all | solution.py:361
  87.6 5.9 %collective-permute-start.2 = (bf16[8,768,128]{2,1,0:T(8,128)(2,1)S(1)}, bf16[8,768,128]{2,1,0:T(8,128)(2,1)S(1)}, u32[]{:S(2)}, u32[]{:S(2)}) collective-permute-start(bf16[8,768,128]{2,1,0:T(8,128)(2,1)S(1)} %all_to_all.31.own), channel_id=1, source_target_pairs={{0,1},{1,0},{2,3},{3,2},{4,5},{5,4},{6,7},{7,6},{8,9},{9,8},{10,11... | collective-permute-start | bytes 4718600 | tf_op jit(solution)/shard_map/ppermute | solution.py:388
  93.4 3.0 %collective-permute-done.2.far = bf16[8,768,128]{2,1,0:T(8,128)(2,1)S(1)} collective-permute-done((bf16[8,768,128]{2,1,0:T(8,128)(2,1)S(1)}, bf16[8,768,128]{2,1,0:T(8,128)(2,1)S(1)}, u32[]{:S(2)}, u32[]{:S(2)}) %collective-permute-start.2) | collective-permute-done | bytes 1572896 | tf_op jit(solution)/shard_map/ppermute | solution.py:388
  96.4 1.2 copy-done.3
  97.6 7.6 %shard_map.216 = (bf16[8,768,128]{2,1,0:T(8,128)(2,1)}, bf16[8,768,128]{2,1,0:T(8,128)(2,1)}) custom-call(s32[1]{0:T(128)} %bitcast.place, bf16[8,768,128]{2,1,0:T(8,128)(2,1)} %copy-done, bf16[8,768,128]{2,1,0:T(8,128)(2,1)} %copy-done.3, bf16[2048,256]{1,0:T(8,128)(2,1)} %bitcast.16, bf16[2048,256]{1,0:T(8,128)(2,1)} %bitcast.17, bf16[256,2048]{1,0:T(8,128)(2,1)} %bitcast.18), custom_call_target="tpu_custom_call" | custom-call | flops 4294967296 | bytes 1048576 | tf_op jit(solution)/shard_map/pallas_call | solution.py:28
  105.2 2.3 %collective-permute-start.3 = (bf16[8,768,128]{2,1,0:T(8,128)(2,1)}, bf16[8,768,128]{2,1,0:T(8,128)(2,1)S(1)}, u32[]{:S(2)}, u32[]{:S(2)}) collective-permute-start(bf16[8,768,128]{2,1,0:T(8,128)(2,1)} %get-tuple-element.26), channel_id=1, source_target_pairs={{0,1},{1,0},{2,3},{3,2},{4,5},{5,4},{6,7},{7,6},{8,9},{9,8},{10,11... | collective-permute-start | bytes 4718600 | tf_op jit(solution)/shard_map/ppermute | solution.py:403
  107.5 4.8 %all-to-all-start.1 = ((bf16[32,8,128]{2,1,0:T(8,128)(2,1)}), bf16[32,8,128]{2,1,0:T(8,128)(2,1)S(1)}, u32[]{:S(2)}, u32[]{:S(2)}) async-start(bf16[32,8,128]{2,1,0:T(8,128)(2,1)} %get-tuple-element.21), calls=%async_computation.1 | async-start | bytes 131072 | tf_op jit(solution)/shard_map/all_to_all | solution.py:364
  112.3 3.0 %add_convert_fusion = bf16[8,768,128]{2,1,0:T(8,128)(2,1)} fusion(bf16[8,768,128]{2,1,0:T(8,128)(2,1)S(1)} %collective-permute-done.3, bf16[8,768,128]{2,1,0:T(8,128)(2,1)} %get-tuple-element.25), kind=kLoop, calls=%fused_computation | loop fusion | flops 3145728 | bytes 4718592 | tf_op jit(solution)/shard_map/convert_element_type | solution.py:404
  115.3 5.8 %all-to-all-done.1 = bf16[32,8,128]{2,1,0:T(8,128)(2,1)S(1)} async-done(((bf16[32,8,128]{2,1,0:T(8,128)(2,1)}), bf16[32,8,128]{2,1,0:T(8,128)(2,1)S(1)}, u32[]{:S(2)}, u32[]{:S(2)}) %all-to-all-start.1) | async-done | bytes 65568 | tf_op jit(solution)/shard_map/all_to_all | solution.py:364
  121.7 3.6 %all-to-all-start.4 = ((bf16[8,768,128]{2,1,0:T(8,128)(2,1)}), bf16[8,768,128]{2,1,0:T(8,128)(2,1)S(1)}, u32[]{:S(2)}, u32[]{:S(2)}) async-start(bf16[8,768,128]{2,1,0:T(8,128)(2,1)} %add_convert_fusion), calls=%async_computation.4 | async-start | bytes 3145728 | tf_op jit(solution)/shard_map/all_to_all | solution.py:405
  125.9 2.5 %shard_map.213.y = f32[256,256]{1,0:T(8,128)} custom-call(f32[4]{0:T(128)} %bypass.1, f32[256,256]{1,0:T(8,128)} %get-tuple-element.15.x, bf16[256,128]{1,0:T(8,128)(2,1)} %get-tuple-element.16.b, bf16[256,128]{1,0:T(8,128)(2,1)} %get-tuple-element.17.c, f32[256,8]{1,0:T(8,128)} %get-tuple-element.18.columns, f32[8,256]{1,0:T(8,128)} %get-tuple-element.19.rows), custom_call_target="tpu_custom_call" | custom-call | flops 2147483648 | bytes 1048576 | tf_op jit(solution)/shard_map/pallas_call | solution.py:28
  128.4 3.1 %shard_map.215 = (bf16[8,16,2048]{2,1,0:T(8,128)(2,1)}, bf16[8,16,2048]{2,1,0:T(8,128)(2,1)}) custom-call(s32[1]{0:T(128)} %bitcast.place, f32[256,256]{1,0:T(8,128)} %shard_map.213.y, bf16[256,128]{1,0:T(8,128)(2,1)} %get-tuple-element.17.c, f32[256,8]{1,0:T(8,128)} %get-tuple-element.18.columns, bf16[256,128]{1,0:T(8,128)(2,1)} %bitcast.13, ...), custom_call_target="tpu_custom_call" | custom-call | flops 2147483648 | bytes 1048576 | tf_op jit(solution)/shard_map/pallas_call | solution.py:28
  131.6 3.5 %collective-permute-start.1 = (bf16[8,16,2048]{2,1,0:T(8,128)(2,1)}, bf16[8,16,2048]{2,1,0:T(8,128)(2,1)S(1)}, u32[]{:S(2)}, u32[]{:S(2)}) collective-permute-start(bf16[8,16,2048]{2,1,0:T(8,128)(2,1)} %get-tuple-element.23), channel_id=1, source_target_pairs={{0,1},{1,0},{2,3},{3,2},{4,5},{5,4},{6,7},{7,6},{8,9},{9,8},{10,11... | collective-permute-start | bytes 1572872 | tf_op jit(solution)/shard_map/ppermute | solution.py:383
  135.0 1.7 collective-permute-done.1
  136.8 2.0 add_convert_fusion.1
  138.7 24.6 %all-to-all-done.4 = bf16[8,768,128]{2,1,0:T(8,128)(2,1)S(1)} async-done(((bf16[8,768,128]{2,1,0:T(8,128)(2,1)}), bf16[8,768,128]{2,1,0:T(8,128)(2,1)S(1)}, u32[]{:S(2)}, u32[]{:S(2)}) %all-to-all-start.4) | async-done | bytes 1572896 | tf_op jit(solution)/shard_map/all_to_all | solution.py:405
  163.4 3.7 %all-to-all-start.2 = ((bf16[8,16,2048]{2,1,0:T(8,128)(2,1)}), bf16[8,16,2048]{2,1,0:T(8,128)(2,1)S(1)}, u32[]{:S(2)}, u32[]{:S(2)}) async-start(bf16[8,16,2048]{2,1,0:T(8,128)(2,1)} %add_convert_fusion.1), calls=%async_computation.2 | async-start | bytes 1048576 | tf_op jit(solution)/shard_map/all_to_all | solution.py:385
  167.0 0.9 reduce_sum.25
  168.0 14.1 %all-to-all-done.2 = bf16[8,16,2048]{2,1,0:T(8,128)(2,1)S(1)} async-done(((bf16[8,16,2048]{2,1,0:T(8,128)(2,1)}), bf16[8,16,2048]{2,1,0:T(8,128)(2,1)S(1)}, u32[]{:S(2)}, u32[]{:S(2)}) %all-to-all-start.2) | async-done | bytes 524320 | tf_op jit(solution)/shard_map/all_to_all | solution.py:385
  182.0 8.3 %all-to-all-start.5 = ((bf16[32,24,128]{2,1,0:T(8,128)(2,1)}), bf16[32,24,128]{2,1,0:T(8,128)(2,1)S(1)}, u32[]{:S(2)}, u32[]{:S(2)}) async-start(bf16[32,24,128]{2,1,0:T(8,128)(2,1)} %bitcast.11), calls=%async_computation.5 | async-start | bytes 393216 | tf_op jit(solution)/shard_map/all_to_all | solution.py:407
  190.4 0.7 reduce_sum.24
  191.1 9.8 %all-to-all-done.5.got = bf16[32,24,128]{2,1,0:T(8,128)(2,1)S(1)} async-done(((bf16[32,24,128]{2,1,0:T(8,128)(2,1)}), bf16[32,24,128]{2,1,0:T(8,128)(2,1)S(1)}, u32[]{:S(2)}, u32[]{:S(2)}) %all-to-all-start.5) | async-done | bytes 196640 | tf_op jit(solution)/shard_map/all_to_all | solution.py:407
  201.5 2.1 %shard_map.217 = bf16[256,128]{1,0:T(8,128)(2,1)} custom-call(bf16[32,24,128]{2,1,0:T(8,128)(2,1)} %copy-done.1, s32[2,256]{1,0:T(2,128)} %get-tuple-element.27.slots, f32[2,256]{1,0:T(2,128)} %bitcast.22), custom_call_target="tpu_custom_call" | custom-call | flops 268435456 | bytes 1048576 | tf_op jit(solution)/shard_map/pallas_call | solution.py:28
  (17 shorter events, 3.8 us)
Async XLA Ops:
  2.7 7.8 %collective-permute-start = (bf16[8,512]{1,0:T(8,128)(2,1)S(1)}, bf16[8,512]{1,0:T(8,128)(2,1)S(1)}, u32[]{:S(2)}, u32[]{:S(2)}) collective-permute-start(bf16[8,512]{1,0:T(8,128)(2,1)S(1)} %pad_maximum_fusion), channel_id=1, source_target_pairs={{0,16},{16,32},{32,48},{48,64},{64,80},{80,96},{96,112},{112,128},... | collective-permute-start | bytes 24584 | tf_op jit(solution)/shard_map/ppermute | solution.py:320
  10.5 0.6 copy-start.4
  87.6 8.9 %copy-start = (bf16[8,768,128]{2,1,0:T(8,128)(2,1)}, bf16[8,768,128]{2,1,0:T(8,128)(2,1)S(1)}, u32[]{:S(2)}) copy-start(bf16[8,768,128]{2,1,0:T(8,128)(2,1)S(1)} %all_to_all.31.own) | copy-start | bytes 4718596
  87.6 8.9 %collective-permute-start.2 = (bf16[8,768,128]{2,1,0:T(8,128)(2,1)S(1)}, bf16[8,768,128]{2,1,0:T(8,128)(2,1)S(1)}, u32[]{:S(2)}, u32[]{:S(2)}) collective-permute-start(bf16[8,768,128]{2,1,0:T(8,128)(2,1)S(1)} %all_to_all.31.own), channel_id=1, source_target_pairs={{0,1},{1,0},{2,3},{3,2},{4,5},{5,4},{6,7},{7,6},{8,9},{9,8},{10,11... | collective-permute-start | bytes 4718600 | tf_op jit(solution)/shard_map/ppermute | solution.py:388
  96.4 1.2 copy-start.3
  105.2 7.1 %collective-permute-start.3 = (bf16[8,768,128]{2,1,0:T(8,128)(2,1)}, bf16[8,768,128]{2,1,0:T(8,128)(2,1)S(1)}, u32[]{:S(2)}, u32[]{:S(2)}) collective-permute-start(bf16[8,768,128]{2,1,0:T(8,128)(2,1)} %get-tuple-element.26), channel_id=1, source_target_pairs={{0,1},{1,0},{2,3},{3,2},{4,5},{5,4},{6,7},{7,6},{8,9},{9,8},{10,11... | collective-permute-start | bytes 4718600 | tf_op jit(solution)/shard_map/ppermute | solution.py:403
  107.5 13.6 %all-to-all-start.1 = ((bf16[32,8,128]{2,1,0:T(8,128)(2,1)}), bf16[32,8,128]{2,1,0:T(8,128)(2,1)S(1)}, u32[]{:S(2)}, u32[]{:S(2)}) async-start(bf16[32,8,128]{2,1,0:T(8,128)(2,1)} %get-tuple-element.21), calls=%async_computation.1 | async-start | bytes 131072 | tf_op jit(solution)/shard_map/all_to_all | solution.py:364
  115.3 10.0 %copy-start.5 = (bf16[256]{0:T(256)(128)(2,1)S(1)}, bf16[256]{0:T(256)(128)(2,1)}, u32[]{:S(2)}) copy-start(bf16[256]{0:T(256)(128)(2,1)} %param.33) | copy-start | bytes 1540
  121.1 0.6 copy-start.2
  121.7 41.6 %all-to-all-start.4 = ((bf16[8,768,128]{2,1,0:T(8,128)(2,1)}), bf16[8,768,128]{2,1,0:T(8,128)(2,1)S(1)}, u32[]{:S(2)}, u32[]{:S(2)}) async-start(bf16[8,768,128]{2,1,0:T(8,128)(2,1)} %add_convert_fusion), calls=%async_computation.4 | async-start | bytes 3145728 | tf_op jit(solution)/shard_map/all_to_all | solution.py:405
  131.6 5.2 %collective-permute-start.1 = (bf16[8,16,2048]{2,1,0:T(8,128)(2,1)}, bf16[8,16,2048]{2,1,0:T(8,128)(2,1)S(1)}, u32[]{:S(2)}, u32[]{:S(2)}) collective-permute-start(bf16[8,16,2048]{2,1,0:T(8,128)(2,1)} %get-tuple-element.23), channel_id=1, source_target_pairs={{0,1},{1,0},{2,3},{3,2},{4,5},{5,4},{6,7},{7,6},{8,9},{9,8},{10,11... | collective-permute-start | bytes 1572872 | tf_op jit(solution)/shard_map/ppermute | solution.py:383
  163.4 18.7 %all-to-all-start.2 = ((bf16[8,16,2048]{2,1,0:T(8,128)(2,1)}), bf16[8,16,2048]{2,1,0:T(8,128)(2,1)S(1)}, u32[]{:S(2)}, u32[]{:S(2)}) async-start(bf16[8,16,2048]{2,1,0:T(8,128)(2,1)} %add_convert_fusion.1), calls=%async_computation.2 | async-start | bytes 1048576 | tf_op jit(solution)/shard_map/all_to_all | solution.py:385
  182.0 18.8 %all-to-all-start.5 = ((bf16[32,24,128]{2,1,0:T(8,128)(2,1)}), bf16[32,24,128]{2,1,0:T(8,128)(2,1)S(1)}, u32[]{:S(2)}, u32[]{:S(2)}) async-start(bf16[32,24,128]{2,1,0:T(8,128)(2,1)} %bitcast.11), calls=%async_computation.5 | async-start | bytes 393216 | tf_op jit(solution)/shard_map/all_to_all | solution.py:407
  200.8 0.7 copy-start.1

commit v2 on v1

v2 whole, which is shorter than its diff:
```python
import functools

import jax
import jax.numpy as jnp
from jax import lax
from jax.experimental import pallas as pl
from jax.experimental.pallas import tpu as pltpu
from jax.sharding import Mesh
from jax.sharding import PartitionSpec as P


HEAD_DIM = 64
TOPK = 2
EP = ("ep_0", "ep_1")
TP = ("tp_0", "tp_1")
EP_TP = ("ep_0", "ep_1", "tp_0", "tp_1")
RIM = 8
PIECE = 8

NORM_EPS = 1e-06
F32 = jnp.float32
BF16 = jnp.bfloat16
VMEM = pl.BlockSpec(memory_space=pltpu.VMEM)
SMEM = pl.BlockSpec(memory_space=pltpu.SMEM)


def call(body, outs, ins, flops, room, scratch=(), smem=0):
    return pl.pallas_call(
        body,
        out_shape=outs,
        in_specs=[SMEM] * smem + [VMEM] * (len(ins) - smem),
        out_specs=jax.tree.map(lambda _: VMEM, outs),
        scratch_shapes=scratch,
        cost_estimate=pl.CostEstimate(flops=flops, bytes_accessed=1 << 20, transcendentals=0),
        compiler_params=pltpu.CompilerParams(vmem_limit_bytes=room << 20),
    )(*ins)


def shaped(*shape, dtype=BF16):
    return jax.ShapeDtypeStruct(shape, dtype)


def iota(shape, dim):
    return lax.broadcasted_iota(jnp.int32, shape, dim)


def silu(v):
    return v * jax.nn.sigmoid(v)


def dot(a, b, contract=(1, 0)):
    return lax.dot_general(
        a, b, (((contract[0],), (contract[1],)), ((), ())), preferred_element_type=F32
    )


def spread(columns, width):
    lane_head = iota((columns.shape[0], 4 * width), 1) // width
    wide = columns[:, 0:1]
    for head in range(1, 4):
        wide = jnp.where(lane_head == head, columns[:, head : head + 1], wide)
    return wide


def route_body(experts, place, tokens, token_gain, picks, routed, slots_out):
    lanes = token_gain.shape[1]
    total_rows, token_count = routed.shape[0], tokens.shape[0]
    capacity = total_rows // experts
    data = tokens[...].astype(F32)
    scale = lax.rsqrt(jnp.mean(data * data, axis=1, keepdims=True) + NORM_EPS)
    first = pl.multiple_of(place[0] * lanes, lanes)
    chosen = tokens[:, pl.ds(first, 2 * lanes)].astype(F32)
    gain = jnp.concatenate([token_gain[pl.ds(place[0] + k, 1), :] for k in range(2)], axis=1)
    chosen = (chosen * scale * gain).astype(BF16)
    expert = iota((experts, token_count), 0)
    earlier = (
        iota((token_count, token_count), 0) < iota((token_count, token_count), 1)
    ).astype(BF16)
    base = jnp.zeros((experts, 1), F32)
    slot_ids = iota((total_rows, token_count), 0)
    placing = None
    for k in range(TOPK):
        pick = picks[k : k + 1, :]
        named = (expert == pick).astype(F32)
        rank = base + dot(named.astype(BF16), earlier)
        rank = jnp.sum(named * rank, axis=0, keepdims=True)
        slot = pick * capacity + rank.astype(jnp.int32)
        slots_out[k : k + 1, :] = slot
        base = base + jnp.sum(named, axis=1, keepdims=True)
        hit = slot_ids == slot
        placing = hit if placing is None else placing | hit
    routed[...] = dot(placing.astype(F32).astype(BF16), chosen).astype(BF16)


def filter_body(
    offset,
    speed,
    routed,
    x_in,
    b_in,
    c_in,
    rim,
    x_taps,
    b_taps,
    c_taps,
    strides,
    extra,
    send,
    x_out,
    b_out,
    c_out,
    columns_out,
    rows_out,
    joined,
):
    count, width = x_in.shape
    state = b_in.shape[1]
    experts, rows, lanes = send.shape
    capacity = (rows - 2 * PIECE) // 2

    joined[0:RIM, :] = rim[...].astype(F32)
    joined[RIM:, 0:width] = x_in[...].astype(F32)
    joined[RIM:, width : width + state] = b_in[...].astype(F32)
    joined[RIM:, width + state :] = c_in[...].astype(F32)

    def filtered(first, size, taps_ref):
        taps = taps_ref[...].astype(F32)
        total = None
        for j in range(taps.shape[0]):
            start = RIM - taps.shape[0] + 1 + j
            term = taps[j : j + 1] * joined[start : start + count, first : first + size]
            total = term if total is None else total + term
        return silu(total)

    x = filtered(0, width, x_taps)
    b = filtered(width, state, b_taps).astype(BF16)
    c = filtered(width + state, state, c_taps).astype(BF16)
    x_out[...] = x
    b_out[...] = b
    c_out[...] = c

    def per_head(values):
        head = iota(strides.shape, 0)
        wide = jnp.full(strides.shape, values[0], F32)
        for k in range(1, strides.shape[0]):
            wide = jnp.where(head == k, values[k], wide)
        return wide

    raw = strides[...] + per_head(offset)
    step = jnp.maximum(raw, 0.0) + jnp.log1p(jnp.exp(-jnp.abs(raw)))
    total = -jnp.exp(per_head(speed)) * step + extra[...]
    both = jnp.concatenate([total, step], axis=0)
    lane = iota(both.shape, 1)
    shift = 1
    while shift < count:
        moved = jnp.where((lane >= shift), pltpu.roll(both, shift, axis=1), 0.0)
        both = jnp.where(iota(both.shape, 0) < 4, both + moved, both)
        shift *= 2
    columns = both.T
    rows_out[...] = both
    columns_out[...] = columns
    running, step_column = columns[:, 0:4], columns[:, 4:8]
    last = columns[count - 1 : count, 0:4]
    weight = step_column * jnp.exp(last - running)
    weighted = (x * spread(weight, HEAD_DIM)).astype(BF16)
    end_state = dot(weighted, b, (0, 0)).astype(BF16)
    high = last.astype(BF16).astype(F32)
    low = last - high
    half = iota((PIECE, lanes), 1) < lanes // 2
    for e in range(experts):
        head = e * PIECE // HEAD_DIM
        mine = routed[e * capacity : (e + 1) * capacity, :]
        send[e, 0:capacity, :] = mine[:, 0:lanes]
        send[e, capacity : 2 * capacity, :] = mine[:, lanes:]
        send[e, rows - 2 * PIECE : rows - PIECE, :] = end_state[e * PIECE : (e + 1) * PIECE]
        send[e, rows - PIECE :, :] = jnp.where(
            half, high[:, head : head + 1], low[:, head : head + 1]
        ).astype(BF16)


def enter_body(got, enter):
    sources, rows, lanes = got.shape
    size = sources * PIECE
    piece = got[:, rows - 2 * PIECE : rows - PIECE, :].reshape(size, lanes)
    logs = got[:, rows - PIECE :, :].reshape(size, lanes).astype(F32)
    logs = logs[:, 0:1] + logs[:, lanes // 2 : lanes // 2 + 1]
    row, column = iota((size, size), 0), iota((size, size), 1)
    before = column // PIECE < row // PIECE
    mean = jnp.where(before, 1.0 / PIECE, 0.0).astype(BF16)
    wide = jnp.broadcast_to(logs, (size, lanes))
    high = wide.astype(BF16)
    mid = (wide - high.astype(F32)).astype(BF16)
    low = (wide - high.astype(F32) - mid.astype(F32)).astype(BF16)
    earlier = dot(mean, high) + dot(mean, mid) + dot(mean, low)
    through = (earlier + wide).T[0:1, :]
    keep = before & (column % PIECE == row % PIECE)
    gap = jnp.where(keep, earlier[:, 0:1] - through, 0.0)
    decay = jnp.where(keep, jnp.exp(gap), 0.0)
    decay_high = decay.astype(BF16)
    decay_low = (decay - decay_high.astype(F32)).astype(BF16)
    result = dot(decay_high, piece) + dot(decay_low, piece)
    enter[...] = result.astype(BF16).reshape(sources, PIECE, lanes)


def inside_body(x_ref, b_ref, c_ref, columns, rows, bypass, out):
    count = x_ref.shape[0]
    scores = dot(c_ref[...], b_ref[...], (1, 1))
    causal = iota((count, count), 0) >= iota((count, count), 1)
    for head in range(4):
        part = slice(head * HEAD_DIM, (head + 1) * HEAD_DIM)
        gap = columns[:, head : head + 1] - rows[head : head + 1, :]
        weights = jnp.where(causal, jnp.exp(jnp.where(causal, gap, 0.0)), 0.0)
        x = x_ref[:, part]
        scaled = (x * columns[:, 4 + head : 5 + head]).astype(BF16)
        inside = dot((scores * weights).astype(BF16), scaled)
        out[:, part] = inside + bypass[head] * x


def finish_body(place, y, c, columns, enter, valve, gain, result, mine, other, normed):
    carried = dot(c[...], enter[...], (1, 1))
    carried = carried * spread(jnp.exp(columns[:, 0:4]), HEAD_DIM)
    gated = (y[...] + carried) * silu(valve[...].astype(F32))
    scale = lax.rsqrt(jnp.mean(gated * gated, axis=1, keepdims=True) + NORM_EPS)
    normed[...] = gated * scale * jnp.concatenate([gain[0:1, :], gain[1:2, :]], axis=1)
    chips, size, lanes = mine.shape
    width = result.shape[1]
    rows = size * lanes // width
    for target, core in ((mine, place[0]), (other, 1 - place[0])):
        parts = []
        for k in range(chips):
            at = (2 * ((place[1] + k) % chips) + core) * rows
            parts.append(normed[pl.ds(pl.multiple_of(at, rows), rows), :])
        left = jnp.concatenate(parts, axis=0).astype(BF16)
        block = 512
        for first in range(0, width, block):
            product = dot(left, result[:, first : first + block]).astype(BF16)
            for k in range(chips):
                for j in range(block // lanes):
                    at = (first // lanes + j) * rows
                    target[k, at : at + rows, :] = product[
                        k * rows : (k + 1) * rows, j * lanes : (j + 1) * lanes
                    ]


def joined_rows(piece, at, capacity):
    left = piece[at, 0:capacity, :]
    right = piece[at, capacity : 2 * capacity, :]
    rows, lanes = left.shape[0] * capacity, left.shape[2]
    return jnp.concatenate([left.reshape(rows, lanes), right.reshape(rows, lanes)], axis=1)


SOURCE_BLOCK = 8


def sums_body(which, first, final, place, *refs):
    refs = list(refs)
    before = [] if first else [refs.pop(0), refs.pop(0)]
    pieces = [refs.pop(0) for _ in which]
    valve, expand, *outs = refs
    sources = pieces[0].shape[0]
    capacity, size = pieces[0].shape[1] // 2, 2 * pieces[0].shape[2]
    count = SOURCE_BLOCK * capacity

    def step(i, _):
        at = pl.ds(i * SOURCE_BLOCK, SOURCE_BLOCK)
        out = pl.ds(pl.multiple_of(i * count, count), count)
        total = [ref[out, :] for ref in before]
        for (other, shift), piece in zip(which, pieces):
            core = 1 - place[0] if other else place[0]
            row = core * (4 * size) + (place[1] + shift) % 4 * size
            rows = pl.ds(pl.multiple_of(row, size), size)
            x = joined_rows(piece, at, capacity)
            more = [dot(x, matrix[rows, :]) for matrix in (valve, expand)]
            total = [t + m for t, m in zip(total, more)] if total else more
        if final:
            outs[0][out, :] = (silu(total[0]) * total[1]).astype(BF16)
        else:
            outs[0][out, :], outs[1][out, :] = total
        return 0

    lax.fori_loop(0, sources // SOURCE_BLOCK, step, 0)


def split_body(place, contract, keep, give):
    chips = keep.shape[1] // 128
    for k in range(chips):
        at = slice(k * 128, (k + 1) * 128)
        base = 2 * ((place[1] + k) % chips)
        for target, core in ((keep, place[0]), (give, 1 - place[0])):
            target[:, at] = contract[:, pl.ds(pl.multiple_of((base + core) * 128, 128), 128)]


def down_body(hidden, hidden_far, keep, keep_far, mine, other, right, left, across, stay):
    chips = keep.shape[1] // 128
    total = hidden.shape[0]
    block = total // 2
    homes = {
        0: (stay, 0), 1: (right, 0), 2: (stay, 1), 3: (right, 1),
        4: (across, 0), 5: (left, 1), 6: (stay, 2), 7: (left, 0),
    }

    def step(i, _):
        at = pl.ds(pl.multiple_of(i * block, block), block)
        near, far = hidden[at, :], hidden_far[at, :]
        for k in range(0, chips, 2):
            columns = slice(k * 128, (k + 2) * 128)
            product = dot(near, keep[:, columns]) + dot(far, keep_far[:, columns])
            for j in range(2):
                home, slot = homes[k + j]
                home[slot, at, :] = product[:, j * 128 : (j + 1) * 128].astype(BF16)
        return 0

    for k in range(chips):
        home, slot = homes[k]
        home[slot, total:, :] = (mine[k].astype(F32) + other[k].astype(F32)).astype(BF16)
    lax.fori_loop(0, total // block, step, 0)


def rim_body(x, b, c, out, done):
    first, copies = 0, []
    for k, part in enumerate((x, b, c)):
        size = part.shape[1]
        copy = pltpu.make_async_copy(
            part.at[pl.ds(part.shape[0] - RIM, RIM), :],
            out.at[:, pl.ds(first, size)],
            done.at[k],
        )
        copy.start()
        copies.append(copy)
        first += size
    for copy in copies:
        copy.wait()


def last_rows(*parts):
    width = sum(part.shape[1] for part in parts)
    return pl.pallas_call(
        rim_body,
        out_shape=shaped(RIM, width),
        in_specs=[pl.BlockSpec(memory_space=pltpu.HBM)] * len(parts),
        out_specs=VMEM,
        scratch_shapes=[pltpu.SemaphoreType.DMA((len(parts),))],
        compiler_params=pltpu.CompilerParams(vmem_limit_bytes=1 << 20),
    )(*parts)


def merge_body(place, stay, from_left, from_right, from_across, so_far, up_two, down_two):
    far = from_across[0].astype(F32)
    core = jnp.full((1, 1), place[0])
    so_far[...] = (
        stay[0].astype(F32) + from_left[0].astype(F32) + from_right[0].astype(F32)
    )
    up = stay[1].astype(F32) + from_left[1].astype(F32) + jnp.where(core == 0, far, 0.0)
    down = stay[2].astype(F32) + from_right[1].astype(F32) + jnp.where(core == 1, far, 0.0)
    up_two[...] = up.astype(BF16)
    down_two[...] = down.astype(BF16)


def total_body(so_far, from_up, from_down, out, rows_out):
    total = so_far[...] + from_up[...].astype(F32) + from_down[...].astype(F32)
    total = total.astype(BF16)
    count, lanes = out.shape
    rows, width = rows_out.shape
    out[...] = total[0:count]
    for j in range(width // lanes):
        first = count + j * rows
        rows_out[:, j * lanes : (j + 1) * lanes] = total[first : first + rows]


def combine_body(got, slots, coefs, out):
    sources, capacity, lanes = got.shape
    rows = got[...].reshape(sources * capacity, lanes)
    slot_ids = iota((rows.shape[0], slots.shape[1]), 0)
    padded = jnp.concatenate([coefs[...]] * (8 // TOPK), axis=0)
    columns = padded.T
    total = None
    for k in range(TOPK):
        chosen = (slot_ids == slots[k : k + 1, :]).astype(F32).astype(BF16)
        term = dot(chosen, rows, (0, 0)) * columns[:, k : k + 1]
        total = term if total is None else total + term
    out[...] = total.astype(BF16)


def local(
    blender_incoming_features,
    entry_latent_matrix,
    exit_latent_matrix,
    unactivated_valve,
    presoftplus_strides,
    extra_attenuation,
    incoming_feature_kernel,
    entry_latent_kernel,
    exit_latent_kernel,
    stride_offset_vector,
    attenuation_speed_exponent,
    bypass_coef_vector,
    cluster_rescale_coefs,
    blender_result_matrix,
    latter_microbatch_activations,
    specialist_rescale_coefs,
    specialist_valve_matrix,
    specialist_expand_matrix,
    specialist_contract_matrix,
    specialist_picks,
    selected_specialist_coefs,
):
    ep_count, chips = lax.axis_size(EP), lax.axis_size("tp_0")
    chip, core = lax.axis_index("tp_0"), lax.axis_index("tp_1")
    count, width = blender_incoming_features.shape
    state = entry_latent_matrix.shape[1]
    token_count, model_width = latter_microbatch_activations.shape
    capacity = 3 * token_count * TOPK // (2 * ep_count)
    lanes = model_width // lax.axis_size(TP)
    total_rows = ep_count * capacity
    place = jnp.stack([core, chip])
    valve = specialist_valve_matrix.reshape(model_width, -1)
    expand = specialist_expand_matrix.reshape(model_width, -1)
    contract = specialist_contract_matrix.reshape(-1, model_width)
    hidden_width = valve.shape[1]

    def permuted(x, axis, pairs):
        return lax.ppermute(x, axis, pairs)

    def around(x, distance):
        return permuted(x, "tp_0", [(i, (i + distance) % chips) for i in range(chips)])

    def across(x):
        pairs = []
        for i in range(chips):
            pairs.append((2 * i, 2 * ((i + 2) % chips)))
            pairs.append((2 * i + 1, 2 * ((i - 2) % chips) + 1))
        return permuted(x, TP, pairs)

    def partner(x):
        return permuted(x, "tp_1", [(0, 1), (1, 0)])

    def exchanged(x, axis):
        return lax.all_to_all(x, axis, 0, 0, tiled=True)

    rim = last_rows(blender_incoming_features, entry_latent_matrix, exit_latent_matrix)
    rim = permuted(rim, EP, [(i, i + 1) for i in range(ep_count - 1)])
    keep, give = call(
        split_body,
        (shaped(hidden_width, model_width // 2),) * 2,
        (place, contract),
        1 << 30,
        8,
        smem=1,
    )
    keep_far = partner(give)
    routed, slots = call(
        functools.partial(route_body, ep_count),
        (shaped(total_rows, 2 * lanes), shaped(TOPK, token_count, dtype=jnp.int32)),
        (
            (core * chips + chip % 4 * 2).reshape(1),
            latter_microbatch_activations,
            specialist_rescale_coefs.astype(F32).reshape(-1, lanes),
            specialist_picks.T,
        ),
        1 << 30,
        16,
        smem=1,
    )
    send, x, b, c, columns, rows = call(
        filter_body,
        (
            shaped(ep_count, 2 * capacity + 2 * PIECE, lanes),
            shaped(count, width, dtype=F32),
            shaped(count, state),
            shaped(count, state),
            shaped(count, 8, dtype=F32),
            shaped(8, count, dtype=F32),
        ),
        (
            stride_offset_vector,
            attenuation_speed_exponent,
            routed,
            blender_incoming_features,
            entry_latent_matrix,
            exit_latent_matrix,
            rim,
            incoming_feature_kernel,
            entry_latent_kernel,
            exit_latent_kernel,
            presoftplus_strides.T,
            extra_attenuation.T,
        ),
        1 << 30,
        10,
        scratch=(pltpu.VMEM((RIM + count, width + 2 * state), F32),),
        smem=2,
    )
    got = exchanged(send, EP)
    y = inside(bypass_coef_vector, x, b, c, columns, rows)

    own = got[:, 0 : 2 * capacity, :]
    left, right = around(own, 1), around(own, -1)
    beyond = across(own)
    far_own, far_left = partner(own), partner(left)
    far_right, far_beyond = partner(right), partner(beyond)

    def sums(which, before, pieces, final=False):
        first = before is None
        return call(
            functools.partial(sums_body, which, first, final),
            shaped(total_rows, hidden_width)
            if final
            else (shaped(total_rows, hidden_width, dtype=F32),) * 2,
            (place, *(() if first else before), *pieces, valve, expand),
            1 << 31,
            12,
            smem=1,
        )

    partial = sums(((0, 0), (0, 3), (0, 1)), None, (own, left, right))
    partial = sums(
        ((0, 2), (1, 0), (1, 3), (1, 1)), partial, (beyond, far_own, far_left, far_right)
    )
    hidden = sums(((1, 2),), partial, (far_beyond,), True)
    enter = call(enter_body, shaped(ep_count, PIECE, lanes), (got,), 1 << 30, 8)
    enter = exchanged(enter, EP).reshape(width, state)
    row_block = count * model_width // (2 * chips * lanes)
    mine_a, other_a = call(
        finish_body,
        (shaped(chips, row_block, lanes),) * 2,
        (
            place,
            y,
            c,
            columns,
            enter,
            unactivated_valve,
            cluster_rescale_coefs.astype(F32).reshape(-1, 128),
            blender_result_matrix,
        ),
        1 << 31,
        10,
        scratch=(pltpu.VMEM((count, width), F32),),
        smem=1,
    )
    other_a = partner(other_a)
    hidden_far = partner(hidden)
    all_rows = total_rows + row_block
    to_right, to_left, to_across, stay = call(
        down_body,
        tuple(shaped(k, all_rows, lanes) for k in (2, 2, 1, 3)),
        (hidden, hidden_far, keep, keep_far, mine_a, other_a),
        1 << 31,
        14,
    )
    from_left, from_right = around(to_right, 1), around(to_left, -1)
    from_across = across(to_across)
    so_far, up_two, down_two = call(
        merge_body,
        (
            shaped(all_rows, lanes, dtype=F32),
            shaped(all_rows, lanes),
            shaped(all_rows, lanes),
        ),
        (place, stay, from_left, from_right, from_across),
        1 << 29,
        6,
        smem=1,
    )
    from_up, from_down = around(up_two, 2), around(down_two, -2)
    summed, mixed_a = call(
        total_body,
        (shaped(total_rows, lanes), shaped(count // (2 * chips), model_width)),
        (so_far, from_up, from_down),
        1 << 29,
        4,
    )
    returned = exchanged(summed.reshape(ep_count, capacity, lanes), EP)
    mixed_b = call(
        combine_body,
        shaped(token_count, lanes),
        (returned, slots, selected_specialist_coefs.T),
        1 << 28,
        8,
    )
    return (mixed_a, mixed_b)


def inside(bypass, x, b, c, columns, rows):
    def body(bypass, x, b, c, columns, rows, out):
        inside_body(x, b, c, columns, rows, bypass, out)

    return call(
        body, shaped(*x.shape, dtype=F32), (bypass, x, b, c, columns, rows), 1 << 31, 8, smem=1
    )


def solution(mesh):
    split = Mesh(mesh.devices.reshape(8, 4, 8, 2), ("ep_0", "ep_1", "tp_0", "tp_1"))
    in_specs = (
        P(EP, TP),
        P(EP, TP),
        P(EP, TP),
        P(EP, TP),
        P(EP, TP),
        P(EP, TP),
        P(None, TP),
        P(None, TP),
        P(None, TP),
        P(TP),
        P(TP),
        P(TP),
        P(TP),
        P(TP, None),
        P(EP, None),
        P(),
        P(EP, None, TP),
        P(EP, None, TP),
        P(EP, TP, None),
        P(EP, None),
        P(EP, None),
    )
    out_specs = (P(EP_TP, None), P(EP, TP))

    return jax.shard_map(local, mesh=split, in_specs=in_specs, out_specs=out_specs, check_vma=False)
```

time: 205 us -> 166 us (0.81)
  blocking collectives: 68.8 us -> 19.9 us
  starting transfers between devices: 35.8 us -> 68.2 us
  waiting for transfers between devices: 59.1 us -> 38.6 us
  other arithmetic: 6.61 us -> 0.08 us
  local copies, waits for them, and re-layouts: 10.7 us -> 16.5 us
  Pallas kernels: 21.8 us -> 18.8 us
    all_to_all x2 -> x1, blocking collectives: 68.8 us -> 19.9 us  [exchanged(): return lax.all_to_all(x, axis, 0, 0, tiled=True)]
    all_to_all x4 -> x2, waiting for transfers between devices: 54.3 us -> 10.4 us  [exchanged(): return lax.all_to_all(x, axis, 0, 0, tiled=True)]
    ppermute x4 -> x16, starting transfers between devices: 15.5 us -> 49.2 us  [permuted(): return lax.ppermute(x, axis, pairs)]
    ppermute x4 -> x16, waiting for transfers between devices: 4.75 us -> 28.2 us  [permuted(): return lax.ppermute(x, axis, pairs)]
    unnamed x12 -> x78, local copies, waits for them, and re-layouts: 3.06 us -> 16.4 us
    convert_element_type x2 -> x0, other arithmetic: 4.98 us -> none  [the longest x1 2.99 us: local(): parts = (mine.astype(F32) + other.astype(F32)).astype(BF16)]
    reshape x4 -> x0, local copies, waits for them, and re-layouts: 4.46 us -> none  [the longest x1 1.31 us: local(): attenuation_speed_exponent.reshape(-1, 1)]
    pallas_call x6 -> x13, Pallas kernels: 21.8 us -> 18.8 us  [call(): pl.pallas_call(body, out_shape=outs, in_specs=[SMEM] * smem + [VMEM] * (l...]
  transfers between devices with their start and end apart: 8 -> 18, of which waited for: 6 -> 5; matrix products, arithmetic and copies ran while one was open for 5% -> 0% of each run, Pallas kernels for 3% -> 7%
where the time goes in v2:
time: 166 us; the launch traced here: 163 us
  starting transfers between devices  68.2 us (41%)
  waiting for transfers between devices  38.6 us (23%)
  blocking collectives  19.9 us (12%)
  Pallas kernels  18.8 us (11%)
  local copies, waits for them, and re-layouts  16.5 us (10%)
    ppermute x16, starting transfers between devices, permuted(): return lax.ppermute(x, axis, pairs)  49.2 us
    ppermute x16, waiting for transfers between devices, permuted(): return lax.ppermute(x, axis, pairs)  28.2 us
    all_to_all x1, blocking collectives, exchanged(): return lax.all_to_all(x, axis, 0, 0, tiled=True)  19.9 us
    all_to_all x2, starting transfers between devices, exchanged(): return lax.all_to_all(x, axis, 0, 0, tiled=True)  19 us
    pallas_call x13, Pallas kernels, call(): pl.pallas_call(body, out_shape=outs, in_specs=[SMEM] * smem + [VMEM] * (l...  18.8 us
    unnamed x78, local copies, waits for them, and re-layouts  16.4 us
    all_to_all x2, waiting for transfers between devices, exchanged(): return lax.all_to_all(x, axis, 0, 0, tiled=True)  10.4 us
  transfers between devices with their start and end apart: 18, of which 5 were waited for; matrix products, arithmetic and copies ran while one was open for 0% of the time, Pallas kernels for 7%

profile of v2, /device:TPU:1, one launch (start us, length us, event | category | flops | bytes accessed | tf_op | source)
XLA Modules:
  0.0 163.1 jit_solution(12801850622448421276)
XLA Ops:
  3.3 3.9 %collective-permute-start = (bf16[8,512]{1,0:T(8,128)(2,1)S(1)}, bf16[8,512]{1,0:T(8,128)(2,1)S(1)}, u32[]{:S(2)}, u32[]{:S(2)}) collective-permute-start(bf16[8,512]{1,0:T(8,128)(2,1)S(1)} %shard_map.213), channel_id=1, source_target_pairs={{0,16},{16,32},{32,48},{48,64},{64,80},{80,96},{96,112},{112,128},... | collective-permute-start | bytes 24584 | tf_op jit(solution)/shard_map/ppermute | solution.py:422
  11.2 2.8 %shard_map.214 = (bf16[32,64,128]{2,1,0:T(8,128)(2,1)}, f32[256,256]{1,0:T(8,128)S(1)}, bf16[256,128]{1,0:T(8,128)(2,1)S(1)}, bf16[256,128]{1,0:T(8,128)(2,1)S(1...) custom-call(f32[4]{0:T(128)S(1)} %copy-done.19, f32[4]{0:T(128)S(1)} %copy-done.20, ...), custom_call_target="tpu_custom_call" | custom-call | flops 1073741824 | bytes 1048576 | tf_op jit(solution)/shard_map/pallas_call | solution.py:28
  17.3 12.7 %all-to-all-start = ((bf16[32,64,128]{2,1,0:T(8,128)(2,1)}), bf16[32,64,128]{2,1,0:T(8,128)(2,1)S(1)}, u32[]{:S(2)}, u32[]{:S(2)}) async-start(bf16[32,64,128]{2,1,0:T(8,128)(2,1)} %get-tuple-element.28), calls=%async_computation | async-start | bytes 1048576 | tf_op jit(solution)/shard_map/all_to_all | solution.py:438
  31.7 3.3 %collective-permute-start.9 = (bf16[256,1024]{1,0:T(8,128)(2,1)S(1)}, bf16[256,1024]{1,0:T(8,128)(2,1)S(1)}, u32[]{:S(2)}, u32[]{:S(2)}) collective-permute-start(bf16[256,1024]{1,0:T(8,128)(2,1)S(1)} %get-tuple-element.34), channel_id=1, source_target_pairs={{0,1},{1,0},{2,3},{3,2},{4,5},{5,4},{6,7},{7,6},{8,9},{9,8},{10,11... | collective-permute-start | bytes 1572872 | tf_op jit(solution)/shard_map/ppermute | solution.py:422
  35.0 10.4 %all-to-all-done.got = bf16[32,64,128]{2,1,0:T(8,128)(2,1)S(1)} async-done(((bf16[32,64,128]{2,1,0:T(8,128)(2,1)}), bf16[32,64,128]{2,1,0:T(8,128)(2,1)S(1)}, u32[]{:S(2)}, u32[]{:S(2)}) %all-to-all-start) | async-done | bytes 524320 | tf_op jit(solution)/shard_map/all_to_all | solution.py:438
  45.4 3.2 %collective-permute-start.1 = (bf16[32,48,128]{2,1,0:T(8,128)(2,1)S(1)}, bf16[32,48,128]{2,1,0:T(8,128)(2,1)}, u32[]{:S(2)}, u32[]{:S(2)}) collective-permute-start(bf16[32,48,128]{2,1,0:T(8,128)(2,1)S(1)} %slice.4.refs_0_), channel_id=1, source_target_pairs={{0,2},{2,4},{4,6},{6,8},{8,10},{10,12},{12,14},{14,0},{1,3},{3,5},... | collective-permute-start | bytes 1179656 | tf_op jit(solution)/shard_map/ppermute | solution.py:422
  48.6 3.8 %collective-permute-start.2 = (bf16[32,48,128]{2,1,0:T(8,128)(2,1)S(1)}, bf16[32,48,128]{2,1,0:T(8,128)(2,1)}, u32[]{:S(2)}, u32[]{:S(2)}) collective-permute-start(bf16[32,48,128]{2,1,0:T(8,128)(2,1)S(1)} %slice.4.refs_0_), channel_id=1, source_target_pairs={{0,14},{2,0},{4,2},{6,4},{8,6},{10,8},{12,10},{14,12},{1,15},{3,1}... | collective-permute-start | bytes 1179656 | tf_op jit(solution)/shard_map/ppermute | solution.py:422
  52.5 4.1 %collective-permute-start.3 = (bf16[32,48,128]{2,1,0:T(8,128)(2,1)S(1)}, bf16[32,48,128]{2,1,0:T(8,128)(2,1)S(1)}, u32[]{:S(2)}, u32[]{:S(2)}) collective-permute-start(bf16[32,48,128]{2,1,0:T(8,128)(2,1)S(1)} %slice.4.refs_0_), channel_id=1, source_target_pairs={{0,4},{1,13},{2,6},{3,15},{4,8},{5,1},{6,10},{7,3},{8,12},{9,5},{1... | collective-permute-start | bytes 1179656 | tf_op jit(solution)/shard_map/ppermute | solution.py:422
  56.6 1.3 shard_map.220
  58.0 6.3 %all-to-all-start.1 = ((bf16[32,8,128]{2,1,0:T(8,128)(2,1)}), bf16[32,8,128]{2,1,0:T(8,128)(2,1)S(1)}, u32[]{:S(2)}, u32[]{:S(2)}) async-start(bf16[32,8,128]{2,1,0:T(8,128)(2,1)} %shard_map.220), calls=%async_computation.1 | async-start | bytes 131072 | tf_op jit(solution)/shard_map/all_to_all | solution.py:438
  67.6 1.3 shard_map.219.y
  69.6 2.9 %collective-permute-start.4 = (bf16[32,48,128]{2,1,0:T(8,128)(2,1)S(1)}, bf16[32,48,128]{2,1,0:T(8,128)(2,1)S(1)}, u32[]{:S(2)}, u32[]{:S(2)}) collective-permute-start(bf16[32,48,128]{2,1,0:T(8,128)(2,1)S(1)} %slice.4.refs_0_), channel_id=1, source_target_pairs={{0,1},{1,0},{2,3},{3,2},{4,5},{5,4},{6,7},{7,6},{8,9},{9,8},{10,11... | collective-permute-start | bytes 1179656 | tf_op jit(solution)/shard_map/ppermute | solution.py:422
  72.5 1.9 %collective-permute-start.5 = (bf16[32,48,128]{2,1,0:T(8,128)(2,1)}, bf16[32,48,128]{2,1,0:T(8,128)(2,1)}, u32[]{:S(2)}, u32[]{:S(2)}) collective-permute-start(bf16[32,48,128]{2,1,0:T(8,128)(2,1)} %collective-permute-done.1.refs_1_), channel_id=1, source_target_pairs={{0,1},{1,0},{2,3},{3,2},{4,5},{5,4},{6,7},{7,6},{8,9},{9,8},{10,11... | collective-permute-start | bytes 1179656 | tf_op jit(solution)/shard_map/ppermute | solution.py:422
  74.4 2.4 %collective-permute-start.6 = (bf16[32,48,128]{2,1,0:T(8,128)(2,1)}, bf16[32,48,128]{2,1,0:T(8,128)(2,1)}, u32[]{:S(2)}, u32[]{:S(2)}) collective-permute-start(bf16[32,48,128]{2,1,0:T(8,128)(2,1)} %collective-permute-done.2.refs_2_), channel_id=1, source_target_pairs={{0,1},{1,0},{2,3},{3,2},{4,5},{5,4},{6,7},{7,6},{8,9},{9,8},{10,11... | collective-permute-start | bytes 1179656 | tf_op jit(solution)/shard_map/ppermute | solution.py:422
  78.7 1.3 shard_map.221
  80.1 1.9 %collective-permute-start.7 = (bf16[32,48,128]{2,1,0:T(8,128)(2,1)S(1)}, bf16[32,48,128]{2,1,0:T(8,128)(2,1)S(1)}, u32[]{:S(2)}, u32[]{:S(2)}) collective-permute-start(bf16[32,48,128]{2,1,0:T(8,128)(2,1)S(1)} %collective-permute-done.3.refs_2_), channel_id=1, source_target_pairs={{0,1},{1,0},{2,3},{3,2},{4,5},{5,4},{6,7},{7,6},{8,9},{9,8},{10,11... | collective-permute-start | bytes 1179656 | tf_op jit(solution)/shard_map/ppermute | solution.py:422
  82.0 2.5 %shard_map.215 = (f32[768,256]{1,0:T(8,128)S(1)}, f32[768,256]{1,0:T(8,128)S(1)}) custom-call(s32[2]{0:T(128)S(1)} %pad_add_fusion.place, bf16[32,48,128]{2,1,0:T(8,128)(2,1)S(1)} %slice.4.refs_0_, bf16[32,48,128]{2,1,0:T(8,128)(2,1)} %collective-permute-done.1.refs_1_, bf16[32,48,128]{2,1,0:T(8,128)(2,1)} %collective-permute-done.2.refs_2_, ...), custom_call_target="tpu_custom_call" | custom-call | flops 2147483648 | bytes 1048576 | tf_op jit(solution)/shard_map/pallas_call | solution.py:28
  84.5 2.4 %collective-permute-start.10 = (bf16[8,256,128]{2,1,0:T(8,128)(2,1)S(1)}, bf16[8,256,128]{2,1,0:T(8,128)(2,1)S(1)}, u32[]{:S(2)}, u32[]{:S(2)}) collective-permute-start(bf16[8,256,128]{2,1,0:T(8,128)(2,1)S(1)} %get-tuple-element.41), channel_id=1, source_target_pairs={{0,1},{1,0},{2,3},{3,2},{4,5},{5,4},{6,7},{7,6},{8,9},{9,8},{10,11... | collective-permute-start | bytes 1572872 | tf_op jit(solution)/shard_map/ppermute | solution.py:422
  86.9 2.7 %shard_map.216 = (f32[768,256]{1,0:T(8,128)S(1)}, f32[768,256]{1,0:T(8,128)S(1)}) custom-call(s32[2]{0:T(128)S(1)} %pad_add_fusion.place, f32[768,256]{1,0:T(8,128)S(1)} %get-tuple-element.29.refs_0_, f32[768,256]{1,0:T(8,128)S(1)} %get-tuple-element.30.refs_1_, bf16[32,48,128]{2,1,0:T(8,128)(2,1)S(1)} %collective-permute-done.3.refs_2_, ...), custom_call_target="tpu_custom_call" | custom-call | flops 2147483648 | bytes 1048576 | tf_op jit(solution)/shard_map/pallas_call | solution.py:28
  89.6 1.5 shard_map.217.hidden
  91.1 1.9 %collective-permute-start.8 = (bf16[768,256]{1,0:T(8,128)(2,1)S(1)}, bf16[768,256]{1,0:T(8,128)(2,1)S(1)}, u32[]{:S(2)}, u32[]{:S(2)}) collective-permute-start(bf16[768,256]{1,0:T(8,128)(2,1)S(1)} %shard_map.217.hidden), channel_id=1, source_target_pairs={{0,1},{1,0},{2,3},{3,2},{4,5},{5,4},{6,7},{7,6},{8,9},{9,8},{10,11... | collective-permute-start | bytes 1179656 | tf_op jit(solution)/shard_map/ppermute | solution.py:422
  93.0 1.7 %collective-permute-done.8.hidden_far = bf16[768,256]{1,0:T(8,128)(2,1)S(1)} collective-permute-done((bf16[768,256]{1,0:T(8,128)(2,1)S(1)}, bf16[768,256]{1,0:T(8,128)(2,1)S(1)}, u32[]{:S(2)}, u32[]{:S(2)}) %collective-permute-start.8) | collective-permute-done | bytes 393248 | tf_op jit(solution)/shard_map/ppermute | solution.py:422
  94.7 1.3 shard_map.222
  96.0 4.0 %collective-permute-start.11 = (bf16[2,1024,128]{2,1,0:T(8,128)(2,1)S(1)}, bf16[2,1024,128]{2,1,0:T(8,128)(2,1)S(1)}, u32[]{:S(2)}, u32[]{:S(2)}) collective-permute-start(bf16[2,1024,128]{2,1,0:T(8,128)(2,1)S(1)} %get-tuple-element.43), channel_id=1, source_target_pairs={{0,2},{2,4},{4,6},{6,8},{8,10},{10,12},{12,14},{14,0},{1,3},{3,5},... | collective-permute-start | bytes 1572872 | tf_op jit(solution)/shard_map/ppermute | solution.py:422
  100.0 2.5 %collective-permute-start.12 = (bf16[2,1024,128]{2,1,0:T(8,128)(2,1)S(1)}, bf16[2,1024,128]{2,1,0:T(8,128)(2,1)S(1)}, u32[]{:S(2)}, u32[]{:S(2)}) collective-permute-start(bf16[2,1024,128]{2,1,0:T(8,128)(2,1)S(1)} %get-tuple-element.44), channel_id=1, source_target_pairs={{0,14},{2,0},{4,2},{6,4},{8,6},{10,8},{12,10},{14,12},{1,15},{3,1}... | collective-permute-start | bytes 1572872 | tf_op jit(solution)/shard_map/ppermute | solution.py:422
  102.5 3.4 %collective-permute-start.13 = (bf16[1,1024,128]{2,1,0:T(8,128)(2,1)S(1)}, bf16[1,1024,128]{2,1,0:T(8,128)(2,1)S(1)}, u32[]{:S(2)}, u32[]{:S(2)}) collective-permute-start(bf16[1,1024,128]{2,1,0:T(8,128)(2,1)S(1)} %get-tuple-element.45), channel_id=1, source_target_pairs={{0,4},{1,13},{2,6},{3,15},{4,8},{5,1},{6,10},{7,3},{8,12},{9,5},{1... | collective-permute-start | bytes 786440 | tf_op jit(solution)/shard_map/ppermute | solution.py:422
  105.9 17.9 %collective-permute-done.13.from_across = bf16[1,1024,128]{2,1,0:T(8,128)(2,1)S(1)} collective-permute-done((bf16[1,1024,128]{2,1,0:T(8,128)(2,1)S(1)}, bf16[1,1024,128]{2,1,0:T(8,128)(2,1)S(1)}, u32[]{:S(2)}, u32[]{:S(2)}) %collective-permute-start.13) | collective-permute-done | bytes 262176 | tf_op jit(solution)/shard_map/ppermute | solution.py:422
  124.7 2.9 %collective-permute-start.14 = (bf16[1024,128]{1,0:T(8,128)(2,1)S(1)}, bf16[1024,128]{1,0:T(8,128)(2,1)S(1)}, u32[]{:S(2)}, u32[]{:S(2)}) collective-permute-start(bf16[1024,128]{1,0:T(8,128)(2,1)S(1)} %get-tuple-element.47), channel_id=1, source_target_pairs={{0,4},{2,6},{4,8},{6,10},{8,12},{10,14},{12,0},{14,2},{1,5},{3,7},... | collective-permute-start | bytes 786440 | tf_op jit(solution)/shard_map/ppermute | solution.py:422
  127.5 4.5 %collective-permute-start.15 = (bf16[1024,128]{1,0:T(8,128)(2,1)S(1)}, bf16[1024,128]{1,0:T(8,128)(2,1)S(1)}, u32[]{:S(2)}, u32[]{:S(2)}) collective-permute-start(bf16[1024,128]{1,0:T(8,128)(2,1)S(1)} %get-tuple-element.48), channel_id=1, source_target_pairs={{0,12},{2,14},{4,0},{6,2},{8,4},{10,6},{12,8},{14,10},{1,13},{3,15... | collective-permute-start | bytes 786440 | tf_op jit(solution)/shard_map/ppermute | solution.py:422
  132.1 5.6 %collective-permute-done.14.from_up = bf16[1024,128]{1,0:T(8,128)(2,1)S(1)} collective-permute-done((bf16[1024,128]{1,0:T(8,128)(2,1)S(1)}, bf16[1024,128]{1,0:T(8,128)(2,1)S(1)}, u32[]{:S(2)}, u32[]{:S(2)}) %collective-permute-start.14) | collective-permute-done | bytes 262176 | tf_op jit(solution)/shard_map/ppermute | solution.py:422
  137.7 3.0 %collective-permute-done.15.from_down = bf16[1024,128]{1,0:T(8,128)(2,1)S(1)} collective-permute-done((bf16[1024,128]{1,0:T(8,128)(2,1)S(1)}, bf16[1024,128]{1,0:T(8,128)(2,1)S(1)}, u32[]{:S(2)}, u32[]{:S(2)}) %collective-permute-start.15) | collective-permute-done | bytes 262176 | tf_op jit(solution)/shard_map/ppermute | solution.py:422
  141.4 19.9 %all_to_all.15.got = bf16[32,24,128]{2,1,0:T(8,128)(2,1)S(1)} all-to-all(bf16[32,24,128]{2,1,0:T(8,128)(2,1)S(1)} %bitcast.18), channel_id=1, replica_groups=mesh['ep_0'=8,'ep_1'=4,'tp_0'=8,'tp_1'=2] {'ep_0','ep_1'}, dimensions={0} | all-to-all | bytes 393216 | tf_op jit(solution)/shard_map/all_to_all | solution.py:438
  (101 shorter events, 20.7 us)
Async XLA Ops:
  3.3 7.2 %collective-permute-start = (bf16[8,512]{1,0:T(8,128)(2,1)S(1)}, bf16[8,512]{1,0:T(8,128)(2,1)S(1)}, u32[]{:S(2)}, u32[]{:S(2)}) collective-permute-start(bf16[8,512]{1,0:T(8,128)(2,1)S(1)} %shard_map.213), channel_id=1, source_target_pairs={{0,16},{16,32},{32,48},{48,64},{64,80},{80,96},{96,112},{112,128},... | collective-permute-start | bytes 24584 | tf_op jit(solution)/shard_map/ppermute | solution.py:422
  8.6 1.2 copy-start.6
  9.8 0.9 copy-start.5
  9.8 0.9 copy-start.13
  9.8 0.9 copy-start.15
  17.3 12.8 %copy-start.7 = (bf16[1,256,2048]{2,1,0:T(8,128)(2,1)S(1)}, bf16[1,256,2048]{2,1,0:T(8,128)(2,1)}, u32[]{:S(2)}) copy-start(bf16[1,256,2048]{2,1,0:T(8,128)(2,1)} %param.39) | copy-start | bytes 3145732
  17.3 28.1 %all-to-all-start = ((bf16[32,64,128]{2,1,0:T(8,128)(2,1)}), bf16[32,64,128]{2,1,0:T(8,128)(2,1)S(1)}, u32[]{:S(2)}, u32[]{:S(2)}) async-start(bf16[32,64,128]{2,1,0:T(8,128)(2,1)} %get-tuple-element.28), calls=%async_computation | async-start | bytes 1048576 | tf_op jit(solution)/shard_map/all_to_all | solution.py:438
  31.7 20.7 %copy-start.38 = (bf16[256]{0:T(256)(128)(2,1)S(1)}, bf16[256]{0:T(256)(128)(2,1)}, u32[]{:S(2)}) copy-start(bf16[256]{0:T(256)(128)(2,1)} %param.33) | copy-start | bytes 1540
  31.7 61.3 %collective-permute-start.9 = (bf16[256,1024]{1,0:T(8,128)(2,1)S(1)}, bf16[256,1024]{1,0:T(8,128)(2,1)S(1)}, u32[]{:S(2)}, u32[]{:S(2)}) collective-permute-start(bf16[256,1024]{1,0:T(8,128)(2,1)S(1)} %get-tuple-element.34), channel_id=1, source_target_pairs={{0,1},{1,0},{2,3},{3,2},{4,5},{5,4},{6,7},{7,6},{8,9},{9,8},{10,11... | collective-permute-start | bytes 1572872 | tf_op jit(solution)/shard_map/ppermute | solution.py:422
  45.4 27.1 %collective-permute-start.1 = (bf16[32,48,128]{2,1,0:T(8,128)(2,1)S(1)}, bf16[32,48,128]{2,1,0:T(8,128)(2,1)}, u32[]{:S(2)}, u32[]{:S(2)}) collective-permute-start(bf16[32,48,128]{2,1,0:T(8,128)(2,1)S(1)} %slice.4.refs_0_), channel_id=1, source_target_pairs={{0,2},{2,4},{4,6},{6,8},{8,10},{10,12},{12,14},{14,0},{1,3},{3,5},... | collective-permute-start | bytes 1179656 | tf_op jit(solution)/shard_map/ppermute | solution.py:422
  48.6 25.8 %collective-permute-start.2 = (bf16[32,48,128]{2,1,0:T(8,128)(2,1)S(1)}, bf16[32,48,128]{2,1,0:T(8,128)(2,1)}, u32[]{:S(2)}, u32[]{:S(2)}) collective-permute-start(bf16[32,48,128]{2,1,0:T(8,128)(2,1)S(1)} %slice.4.refs_0_), channel_id=1, source_target_pairs={{0,14},{2,0},{4,2},{6,4},{8,6},{10,8},{12,10},{14,12},{1,15},{3,1}... | collective-permute-start | bytes 1179656 | tf_op jit(solution)/shard_map/ppermute | solution.py:422
  52.5 27.6 %collective-permute-start.3 = (bf16[32,48,128]{2,1,0:T(8,128)(2,1)S(1)}, bf16[32,48,128]{2,1,0:T(8,128)(2,1)S(1)}, u32[]{:S(2)}, u32[]{:S(2)}) collective-permute-start(bf16[32,48,128]{2,1,0:T(8,128)(2,1)S(1)} %slice.4.refs_0_), channel_id=1, source_target_pairs={{0,4},{1,13},{2,6},{3,15},{4,8},{5,1},{6,10},{7,3},{8,12},{9,5},{1... | collective-permute-start | bytes 1179656 | tf_op jit(solution)/shard_map/ppermute | solution.py:422
  58.0 6.3 %copy-start.27 = (f32[256,8]{1,0:T(8,128)S(1)}, f32[256,8]{1,0:T(8,128)}, u32[]{:S(2)}) copy-start(f32[256,8]{1,0:T(8,128)} %copy-done.26) | copy-start | bytes 24580
  58.0 18.9 %all-to-all-start.1 = ((bf16[32,8,128]{2,1,0:T(8,128)(2,1)}), bf16[32,8,128]{2,1,0:T(8,128)(2,1)S(1)}, u32[]{:S(2)}, u32[]{:S(2)}) async-start(bf16[32,8,128]{2,1,0:T(8,128)(2,1)} %shard_map.220), calls=%async_computation.1 | async-start | bytes 131072 | tf_op jit(solution)/shard_map/all_to_all | solution.py:438
  64.9 1.0 copy-start.25
  67.6 9.3 %copy-start.8 = (bf16[256,2048]{1,0:T(8,128)(2,1)S(1)}, bf16[256,2048]{1,0:T(8,128)(2,1)}, u32[]{:S(2)}) copy-start(bf16[256,2048]{1,0:T(8,128)(2,1)} %result.1) | copy-start | bytes 3145732
  67.6 9.3 %copy-start.11 = (bf16[256,256]{1,0:T(8,128)(2,1)S(1)}, bf16[256,256]{1,0:T(8,128)(2,1)}, u32[]{:S(2)}) copy-start(bf16[256,256]{1,0:T(8,128)(2,1)} %valve.1) | copy-start | bytes 393220
  69.6 14.9 %collective-permute-start.4 = (bf16[32,48,128]{2,1,0:T(8,128)(2,1)S(1)}, bf16[32,48,128]{2,1,0:T(8,128)(2,1)S(1)}, u32[]{:S(2)}, u32[]{:S(2)}) collective-permute-start(bf16[32,48,128]{2,1,0:T(8,128)(2,1)S(1)} %slice.4.refs_0_), channel_id=1, source_target_pairs={{0,1},{1,0},{2,3},{3,2},{4,5},{5,4},{6,7},{7,6},{8,9},{9,8},{10,11... | collective-permute-start | bytes 1179656 | tf_op jit(solution)/shard_map/ppermute | solution.py:422
  72.5 14.4 %collective-permute-start.5 = (bf16[32,48,128]{2,1,0:T(8,128)(2,1)}, bf16[32,48,128]{2,1,0:T(8,128)(2,1)}, u32[]{:S(2)}, u32[]{:S(2)}) collective-permute-start(bf16[32,48,128]{2,1,0:T(8,128)(2,1)} %collective-permute-done.1.refs_1_), channel_id=1, source_target_pairs={{0,1},{1,0},{2,3},{3,2},{4,5},{5,4},{6,7},{7,6},{8,9},{9,8},{10,11... | collective-permute-start | bytes 1179656 | tf_op jit(solution)/shard_map/ppermute | solution.py:422
  74.4 12.5 %collective-permute-start.6 = (bf16[32,48,128]{2,1,0:T(8,128)(2,1)}, bf16[32,48,128]{2,1,0:T(8,128)(2,1)}, u32[]{:S(2)}, u32[]{:S(2)}) collective-permute-start(bf16[32,48,128]{2,1,0:T(8,128)(2,1)} %collective-permute-done.2.refs_2_), channel_id=1, source_target_pairs={{0,1},{1,0},{2,3},{3,2},{4,5},{5,4},{6,7},{7,6},{8,9},{9,8},{10,11... | collective-permute-start | bytes 1179656 | tf_op jit(solution)/shard_map/ppermute | solution.py:422
  77.8 0.9 copy-start.30
  78.7 3.3 %copy-start.9 = (bf16[1,2048,256]{2,1,0:T(8,128)(2,1)S(1)}, bf16[1,2048,256]{2,1,0:T(8,128)(2,1)}, u32[]{:S(2)}) copy-start(bf16[1,2048,256]{2,1,0:T(8,128)(2,1)} %param.37) | copy-start | bytes 3145732
  78.7 3.3 %copy-start.10 = (bf16[1,2048,256]{2,1,0:T(8,128)(2,1)S(1)}, bf16[1,2048,256]{2,1,0:T(8,128)(2,1)}, u32[]{:S(2)}) copy-start(bf16[1,2048,256]{2,1,0:T(8,128)(2,1)} %param.38) | copy-start | bytes 3145732
  80.1 9.5 %collective-permute-start.7 = (bf16[32,48,128]{2,1,0:T(8,128)(2,1)S(1)}, bf16[32,48,128]{2,1,0:T(8,128)(2,1)S(1)}, u32[]{:S(2)}, u32[]{:S(2)}) collective-permute-start(bf16[32,48,128]{2,1,0:T(8,128)(2,1)S(1)} %collective-permute-done.3.refs_2_), channel_id=1, source_target_pairs={{0,1},{1,0},{2,3},{3,2},{4,5},{5,4},{6,7},{7,6},{8,9},{9,8},{10,11... | collective-permute-start | bytes 1179656 | tf_op jit(solution)/shard_map/ppermute | solution.py:422
  84.5 8.5 %collective-permute-start.10 = (bf16[8,256,128]{2,1,0:T(8,128)(2,1)S(1)}, bf16[8,256,128]{2,1,0:T(8,128)(2,1)S(1)}, u32[]{:S(2)}, u32[]{:S(2)}) collective-permute-start(bf16[8,256,128]{2,1,0:T(8,128)(2,1)S(1)} %get-tuple-element.41), channel_id=1, source_target_pairs={{0,1},{1,0},{2,3},{3,2},{4,5},{5,4},{6,7},{7,6},{8,9},{9,8},{10,11... | collective-permute-start | bytes 1572872 | tf_op jit(solution)/shard_map/ppermute | solution.py:422
  89.6 5.1 %copy-start.23 = (bf16[256,1024]{1,0:T(8,128)(2,1)S(1)}, bf16[256,1024]{1,0:T(8,128)(2,1)}, u32[]{:S(2)}) copy-start(bf16[256,1024]{1,0:T(8,128)(2,1)} %copy-done.22) | copy-start | bytes 1572868
  91.1 3.6 %collective-permute-start.8 = (bf16[768,256]{1,0:T(8,128)(2,1)S(1)}, bf16[768,256]{1,0:T(8,128)(2,1)S(1)}, u32[]{:S(2)}, u32[]{:S(2)}) collective-permute-start(bf16[768,256]{1,0:T(8,128)(2,1)S(1)} %shard_map.217.hidden), channel_id=1, source_target_pairs={{0,1},{1,0},{2,3},{3,2},{4,5},{5,4},{6,7},{7,6},{8,9},{9,8},{10,11... | collective-permute-start | bytes 1179656 | tf_op jit(solution)/shard_map/ppermute | solution.py:422
  96.0 27.8 %collective-permute-start.11 = (bf16[2,1024,128]{2,1,0:T(8,128)(2,1)S(1)}, bf16[2,1024,128]{2,1,0:T(8,128)(2,1)S(1)}, u32[]{:S(2)}, u32[]{:S(2)}) collective-permute-start(bf16[2,1024,128]{2,1,0:T(8,128)(2,1)S(1)} %get-tuple-element.43), channel_id=1, source_target_pairs={{0,2},{2,4},{4,6},{6,8},{8,10},{10,12},{12,14},{14,0},{1,3},{3,5},... | collective-permute-start | bytes 1572872 | tf_op jit(solution)/shard_map/ppermute | solution.py:422
  100.0 23.8 %collective-permute-start.12 = (bf16[2,1024,128]{2,1,0:T(8,128)(2,1)S(1)}, bf16[2,1024,128]{2,1,0:T(8,128)(2,1)S(1)}, u32[]{:S(2)}, u32[]{:S(2)}) collective-permute-start(bf16[2,1024,128]{2,1,0:T(8,128)(2,1)S(1)} %get-tuple-element.44), channel_id=1, source_target_pairs={{0,14},{2,0},{4,2},{6,4},{8,6},{10,8},{12,10},{14,12},{1,15},{3,1}... | collective-permute-start | bytes 1572872 | tf_op jit(solution)/shard_map/ppermute | solution.py:422
  102.5 21.3 %collective-permute-start.13 = (bf16[1,1024,128]{2,1,0:T(8,128)(2,1)S(1)}, bf16[1,1024,128]{2,1,0:T(8,128)(2,1)S(1)}, u32[]{:S(2)}, u32[]{:S(2)}) collective-permute-start(bf16[1,1024,128]{2,1,0:T(8,128)(2,1)S(1)} %get-tuple-element.45), channel_id=1, source_target_pairs={{0,4},{1,13},{2,6},{3,15},{4,8},{5,1},{6,10},{7,3},{8,12},{9,5},{1... | collective-permute-start | bytes 786440 | tf_op jit(solution)/shard_map/ppermute | solution.py:422
  124.7 13.0 %collective-permute-start.14 = (bf16[1024,128]{1,0:T(8,128)(2,1)S(1)}, bf16[1024,128]{1,0:T(8,128)(2,1)S(1)}, u32[]{:S(2)}, u32[]{:S(2)}) collective-permute-start(bf16[1024,128]{1,0:T(8,128)(2,1)S(1)} %get-tuple-element.47), channel_id=1, source_target_pairs={{0,4},{2,6},{4,8},{6,10},{8,12},{10,14},{12,0},{14,2},{1,5},{3,7},... | collective-permute-start | bytes 786440 | tf_op jit(solution)/shard_map/ppermute | solution.py:422
  127.5 13.2 %collective-permute-start.15 = (bf16[1024,128]{1,0:T(8,128)(2,1)S(1)}, bf16[1024,128]{1,0:T(8,128)(2,1)S(1)}, u32[]{:S(2)}, u32[]{:S(2)}) collective-permute-start(bf16[1024,128]{1,0:T(8,128)(2,1)S(1)} %get-tuple-element.48), channel_id=1, source_target_pairs={{0,12},{2,14},{4,0},{6,2},{8,4},{10,6},{12,8},{14,10},{1,13},{3,15... | collective-permute-start | bytes 786440 | tf_op jit(solution)/shard_map/ppermute | solution.py:422
  (25 other events, 19.1 us)

commit v3 on v2

--- a/solution.py
+++ b/solution.py
@@ -32,7 +32,7 @@
         out_specs=jax.tree.map(lambda _: VMEM, outs),
         scratch_shapes=scratch,
         cost_estimate=pl.CostEstimate(flops=flops, bytes_accessed=1 << 20, transcendentals=0),
-        compiler_params=pltpu.CompilerParams(vmem_limit_bytes=room << 20),
+        compiler_params=pltpu.CompilerParams(vmem_limit_bytes=room << 20 if room else None),
     )(*ins)
 
 
@@ -216,30 +216,20 @@
         out[:, part] = inside + bypass[head] * x
 
 
-def finish_body(place, y, c, columns, enter, valve, gain, result, mine, other, normed):
+def finish_body(place, y, c, columns, enter, valve, gain, mine, other, normed):
     carried = dot(c[...], enter[...], (1, 1))
     carried = carried * spread(jnp.exp(columns[:, 0:4]), HEAD_DIM)
     gated = (y[...] + carried) * silu(valve[...].astype(F32))
     scale = lax.rsqrt(jnp.mean(gated * gated, axis=1, keepdims=True) + NORM_EPS)
     normed[...] = gated * scale * jnp.concatenate([gain[0:1, :], gain[1:2, :]], axis=1)
-    chips, size, lanes = mine.shape
-    width = result.shape[1]
-    rows = size * lanes // width
+    chips = 8
+    rows = mine.shape[0] // chips
     for target, core in ((mine, place[0]), (other, 1 - place[0])):
         parts = []
         for k in range(chips):
             at = (2 * ((place[1] + k) % chips) + core) * rows
             parts.append(normed[pl.ds(pl.multiple_of(at, rows), rows), :])
-        left = jnp.concatenate(parts, axis=0).astype(BF16)
-        block = 512
-        for first in range(0, width, block):
-            product = dot(left, result[:, first : first + block]).astype(BF16)
-            for k in range(chips):
-                for j in range(block // lanes):
-                    at = (first // lanes + j) * rows
-                    target[k, at : at + rows, :] = product[
-                        k * rows : (k + 1) * rows, j * lanes : (j + 1) * lanes
-                    ]
+        target[...] = jnp.concatenate(parts, axis=0).astype(BF16)
 
 
 def joined_rows(piece, at, capacity):
@@ -252,47 +242,83 @@
 SOURCE_BLOCK = 8
 
 
-def sums_body(which, first, final, place, *refs):
-    refs = list(refs)
-    before = [] if first else [refs.pop(0), refs.pop(0)]
-    pieces = [refs.pop(0) for _ in which]
-    valve, expand, *outs = refs
-    sources = pieces[0].shape[0]
-    capacity, size = pieces[0].shape[1] // 2, 2 * pieces[0].shape[2]
+def feature_sums(pieces, at, capacity, rows_of, gates, ups):
+    gate = up = None
+    for shift, piece in zip((0, 3, 1, 2), pieces):
+        x = joined_rows(piece, at, capacity)
+        rows = rows_of(shift)
+        more = dot(x, gates[rows[0], :]), dot(x, ups[rows[1], :])
+        gate, up = more if gate is None else (gate + more[0], up + more[1])
+    return gate, up
+
+
+def theirs_body(place, own, left, right, across, weights, out):
+    sources, capacity = own.shape[0], own.shape[1] // 2
+    size = 2 * own.shape[2]
     count = SOURCE_BLOCK * capacity
+
+    def rows_of(shift):
+        first = (place[1] + shift) % 4 * size
+        return [pl.ds(pl.multiple_of(first + 4 * size * k, size), size) for k in range(2)]
 
     def step(i, _):
         at = pl.ds(i * SOURCE_BLOCK, SOURCE_BLOCK)
-        out = pl.ds(pl.multiple_of(i * count, count), count)
-        total = [ref[out, :] for ref in before]
-        for (other, shift), piece in zip(which, pieces):
-            core = 1 - place[0] if other else place[0]
-            row = core * (4 * size) + (place[1] + shift) % 4 * size
-            rows = pl.ds(pl.multiple_of(row, size), size)
-            x = joined_rows(piece, at, capacity)
-            more = [dot(x, matrix[rows, :]) for matrix in (valve, expand)]
-            total = [t + m for t, m in zip(total, more)] if total else more
-        if final:
-            outs[0][out, :] = (silu(total[0]) * total[1]).astype(BF16)
-        else:
-            outs[0][out, :], outs[1][out, :] = total
+        to = pl.ds(pl.multiple_of(i * count, count), count)
+        gate, up = feature_sums(
+            (own, left, right, across), at, capacity, rows_of, weights, weights
+        )
+        width = gate.shape[1]
+        out[to, 0:width] = gate.astype(BF16)
+        out[to, width:] = up.astype(BF16)
         return 0
 
     lax.fori_loop(0, sources // SOURCE_BLOCK, step, 0)
 
 
-def split_body(place, contract, keep, give):
-    chips = keep.shape[1] // 128
+def ours_body(place, own, left, right, across, valve, expand, other, rows, out):
+    sources, capacity = own.shape[0], own.shape[1] // 2
+    size = 2 * own.shape[2]
+    count = SOURCE_BLOCK * capacity
+
+    def rows_of(shift):
+        first = place[0] * (4 * size) + (place[1] + shift) % 4 * size
+        return [pl.ds(pl.multiple_of(first, size), size)] * 2
+
+    def step(i, _):
+        at = pl.ds(i * SOURCE_BLOCK, SOURCE_BLOCK)
+        to = pl.ds(pl.multiple_of(i * count, count), count)
+        gate, up = feature_sums((own, left, right, across), at, capacity, rows_of, valve, expand)
+        width = gate.shape[1]
+        gate = gate + other[to, 0:width].astype(F32)
+        up = up + other[to, width:].astype(F32)
+        out[to, :] = (silu(gate) * up).astype(BF16)
+        return 0
+
+    lax.fori_loop(0, sources // SOURCE_BLOCK, step, 0)
+    out[sources * capacity :, :] = rows[...]
+
+
+def split_body(place, valve, expand, contract, keep, give):
+    half = valve.shape[0] // 2
+    theirs = pl.ds(pl.multiple_of((1 - place[0]) * half, half), half)
+    give[0:half, :] = valve[theirs, :]
+    give[half : 2 * half, :] = expand[theirs, :]
+    depth = contract.shape[0]
+    chips = 8
     for k in range(chips):
-        at = slice(k * 128, (k + 1) * 128)
         base = 2 * ((place[1] + k) % chips)
-        for target, core in ((keep, place[0]), (give, 1 - place[0])):
-            target[:, at] = contract[:, pl.ds(pl.multiple_of((base + core) * 128, 128), 128)]
-
-
-def down_body(hidden, hidden_far, keep, keep_far, mine, other, right, left, across, stay):
-    chips = keep.shape[1] // 128
-    total = hidden.shape[0]
+        row, lane = k // 2 * depth, k % 2 * 128
+        for target, core, first in ((keep, place[0], 0), (give, 1 - place[0], 2 * half)):
+            target[first + row : first + row + depth, lane : lane + 128] = contract[
+                :, pl.ds(pl.multiple_of((base + core) * 128, 128), 128)
+            ]
+
+
+def down_body(own, far, rows, keep, weights, result, result_far, right, left, across, stay):
+    chips, depth = 8, own.shape[1]
+    count = rows.shape[0]
+    total = own.shape[0] - count
+    far_first = weights.shape[0] - keep.shape[0]
     block = total // 2
     homes = {
         0: (stay, 0), 1: (right, 0), 2: (stay, 1), 3: (right, 1),
@@ -301,19 +327,31 @@
 
     def step(i, _):
         at = pl.ds(pl.multiple_of(i * block, block), block)
-        near, far = hidden[at, :], hidden_far[at, :]
+        near, beyond = own[at, :], far[at, :]
         for k in range(0, chips, 2):
-            columns = slice(k * 128, (k + 2) * 128)
-            product = dot(near, keep[:, columns]) + dot(far, keep_far[:, columns])
+            row = k // 2 * depth
+            product = dot(near, keep[row : row + depth, :]) + dot(
+                beyond, weights[far_first + row : far_first + row + depth, :]
+            )
             for j in range(2):
                 home, slot = homes[k + j]
                 home[slot, at, :] = product[:, j * 128 : (j + 1) * 128].astype(BF16)
         return 0
 
-    for k in range(chips):
-        home, slot = homes[k]
-        home[slot, total:, :] = (mine[k].astype(F32) + other[k].astype(F32)).astype(BF16)
     lax.fori_loop(0, total // block, step, 0)
+    near, beyond = rows[...], far[total:, :]
+    each, wide = count // chips, 512
+    for first in range(0, result.shape[1], wide):
+        columns = slice(first, first + wide)
+        product = dot(near, result[:, columns]) + dot(beyond, result_far[:, columns])
+        product = product.astype(BF16)
+        for k in range(chips):
+            home, slot = homes[k]
+            for j in range(wide // 128):
+                to = total + (first // 128 + j) * each
+                home[slot, to : to + each, :] = product[
+                    k * each : (k + 1) * each, j * 128 : (j + 1) * 128
+                ]
 
 
 def rim_body(x, b, c, out, done):
@@ -340,7 +378,6 @@
         in_specs=[pl.BlockSpec(memory_space=pltpu.HBM)] * len(parts),
         out_specs=VMEM,
         scratch_shapes=[pltpu.SemaphoreType.DMA((len(parts),))],
-        compiler_params=pltpu.CompilerParams(vmem_limit_bytes=1 << 20),
     )(*parts)
 
 
@@ -418,36 +455,24 @@
     contract = specialist_contract_matrix.reshape(-1, model_width)
     hidden_width = valve.shape[1]
 
-    def permuted(x, axis, pairs):
-        return lax.ppermute(x, axis, pairs)
-
     def around(x, distance):
-        return permuted(x, "tp_0", [(i, (i + distance) % chips) for i in range(chips)])
+        return lax.ppermute(x, "tp_0", [(i, (i + distance) % chips) for i in range(chips)])
 
     def across(x):
         pairs = []
         for i in range(chips):
             pairs.append((2 * i, 2 * ((i + 2) % chips)))
             pairs.append((2 * i + 1, 2 * ((i - 2) % chips) + 1))
-        return permuted(x, TP, pairs)
+        return lax.ppermute(x, TP, pairs)
 
     def partner(x):
-        return permuted(x, "tp_1", [(0, 1), (1, 0)])
+        return lax.ppermute(x, "tp_1", [(0, 1), (1, 0)])
 
     def exchanged(x, axis):
         return lax.all_to_all(x, axis, 0, 0, tiled=True)
 
     rim = last_rows(blender_incoming_features, entry_latent_matrix, exit_latent_matrix)
-    rim = permuted(rim, EP, [(i, i + 1) for i in range(ep_count - 1)])
-    keep, give = call(
-        split_body,
-        (shaped(hidden_width, model_width // 2),) * 2,
-        (place, contract),
-        1 << 30,
-        8,
-        smem=1,
-    )
-    keep_far = partner(give)
+    rim = lax.ppermute(rim, EP, [(i, i + 1) for i in range(ep_count - 1)])
     routed, slots = call(
         functools.partial(route_body, ep_count),
         (shaped(total_rows, 2 * lanes), shaped(TOPK, token_count, dtype=jnp.int32)),
@@ -458,7 +483,7 @@
             specialist_picks.T,
         ),
         1 << 30,
-        16,
+        None,
         smem=1,
     )
     send, x, b, c, columns, rows = call(
@@ -486,43 +511,45 @@
             extra_attenuation.T,
         ),
         1 << 30,
-        10,
+        None,
         scratch=(pltpu.VMEM((RIM + count, width + 2 * state), F32),),
         smem=2,
     )
     got = exchanged(send, EP)
     y = inside(bypass_coef_vector, x, b, c, columns, rows)
 
+    half = model_width // 2
+    keep, give = call(
+        split_body,
+        (shaped(half, hidden_width), shaped(3 * half, hidden_width)),
+        (place, valve, expand, contract),
+        1 << 30,
+        None,
+        smem=1,
+    )
+    weights_far = partner(give)
+    result_far = partner(blender_result_matrix)
+
     own = got[:, 0 : 2 * capacity, :]
+    beyond = across(own)
     left, right = around(own, 1), around(own, -1)
-    beyond = across(own)
-    far_own, far_left = partner(own), partner(left)
-    far_right, far_beyond = partner(right), partner(beyond)
-
-    def sums(which, before, pieces, final=False):
-        first = before is None
-        return call(
-            functools.partial(sums_body, which, first, final),
-            shaped(total_rows, hidden_width)
-            if final
-            else (shaped(total_rows, hidden_width, dtype=F32),) * 2,
-            (place, *(() if first else before), *pieces, valve, expand),
-            1 << 31,
-            12,
-            smem=1,
-        )
-
-    partial = sums(((0, 0), (0, 3), (0, 1)), None, (own, left, right))
-    partial = sums(
-        ((0, 2), (1, 0), (1, 3), (1, 1)), partial, (beyond, far_own, far_left, far_right)
-    )
-    hidden = sums(((1, 2),), partial, (far_beyond,), True)
+    pieces = (own, left, right, beyond)
+    theirs = call(
+        theirs_body,
+        shaped(total_rows, 2 * hidden_width),
+        (place, *pieces, weights_far),
+        1 << 31,
+        10,
+        smem=1,
+    )
+    theirs = partner(theirs)
+
     enter = call(enter_body, shaped(ep_count, PIECE, lanes), (got,), 1 << 30, 8)
     enter = exchanged(enter, EP).reshape(width, state)
-    row_block = count * model_width // (2 * chips * lanes)
-    mine_a, other_a = call(
+    row_count = count // 2
+    mine_rows, other_rows = call(
         finish_body,
-        (shaped(chips, row_block, lanes),) * 2,
+        (shaped(row_count, width),) * 2,
         (
             place,
             y,
@@ -531,20 +558,27 @@
             enter,
             unactivated_valve,
             cluster_rescale_coefs.astype(F32).reshape(-1, 128),
-            blender_result_matrix,
         ),
         1 << 31,
-        10,
+        8,
         scratch=(pltpu.VMEM((count, width), F32),),
         smem=1,
     )
-    other_a = partner(other_a)
-    hidden_far = partner(hidden)
+    ours = call(
+        ours_body,
+        shaped(total_rows + row_count, hidden_width),
+        (place, *pieces, valve, expand, theirs, other_rows),
+        1 << 31,
+        10,
+        smem=1,
+    )
+    ours_far = partner(ours)
+    row_block = count * model_width // (2 * chips * lanes)
     all_rows = total_rows + row_block
     to_right, to_left, to_across, stay = call(
         down_body,
         tuple(shaped(k, all_rows, lanes) for k in (2, 2, 1, 3)),
-        (hidden, hidden_far, keep, keep_far, mine_a, other_a),
+        (ours, ours_far, mine_rows, keep, weights_far, blender_result_matrix, result_far),
         1 << 31,
         14,
     )

time: 166 us -> 177 us (1.066)
  blocking collectives: 19.9 us -> 41.4 us
  starting transfers between devices: 68.2 us -> 51.5 us
  local copies, waits for them, and re-layouts: 16.5 us -> 8.33 us
  waiting for transfers between devices: 38.6 us -> 45.7 us
  Pallas kernels: 18.8 us -> 25.7 us
    all_to_all x1 -> x2, blocking collectives: 19.9 us -> 41.4 us  [exchanged(): return lax.all_to_all(x, axis, 0, 0, tiled=True)]
    all_to_all x2 -> x1, starting transfers between devices: 19 us -> 5.04 us  [exchanged(): return lax.all_to_all(x, axis, 0, 0, tiled=True)]
    ppermute x16 -> x13, waiting for transfers between devices: 28.2 us -> 42.1 us  [the longest x2 29.1 us: across(): return lax.ppermute(x, TP, pairs)]
    unnamed x78 -> x48, local copies, waits for them, and re-layouts: 16.4 us -> 8.3 us
    all_to_all x2 -> x1, waiting for transfers between devices: 10.4 us -> 3.53 us  [exchanged(): return lax.all_to_all(x, axis, 0, 0, tiled=True)]
    pallas_call x13 -> x12, Pallas kernels: 18.8 us -> 24.3 us  [call(): pl.pallas_call(body, out_shape=outs, in_specs=[SMEM] * smem + [VMEM] * (l...]
    ppermute x16 -> x13, starting transfers between devices: 49.2 us -> 46.4 us  [the longest x6 21 us: around(): lax.ppermute(x, 'tp_0', [(i, (i + distance) % chips) for i in range(chips)])]
  transfers between devices with their start and end apart: 18 -> 14, of which waited for: 5 -> 8; matrix products, arithmetic and copies ran while one was open for 0% -> 1% of each run, Pallas kernels for 7% -> 9%
where the time goes in v3:
time: 177 us; the launch traced here: 175 us
  starting transfers between devices  51.5 us (29%)
  waiting for transfers between devices  45.7 us (26%)
  blocking collectives  41.4 us (23%)
  Pallas kernels  25.7 us (15%)
  local copies, waits for them, and re-layouts  8.33 us (5%)
    all_to_all x2, blocking collectives, exchanged(): return lax.all_to_all(x, axis, 0, 0, tiled=True)  41.4 us
    ppermute x2, waiting for transfers between devices, across(): return lax.ppermute(x, TP, pairs)  29.1 us
    pallas_call x12, Pallas kernels, call(): pl.pallas_call(body, out_shape=outs, in_specs=[SMEM] * smem + [VMEM] * (l...  24.3 us
    ppermute x6, starting transfers between devices, around(): lax.ppermute(x, 'tp_0', [(i, (i + distance) % chips) for i in range(chips)])  21 us
    ppermute x4, starting transfers between devices, partner(): return lax.ppermute(x, 'tp_1', [(0, 1), (1, 0)])  13.6 us
    ppermute x6, waiting for transfers between devices, around(): lax.ppermute(x, 'tp_0', [(i, (i + distance) % chips) for i in range(chips)])  11.6 us
    unnamed x48, local copies, waits for them, and re-layouts  8.3 us
    ppermute x2, starting transfers between devices, across(): return lax.ppermute(x, TP, pairs)  7.84 us
  transfers between devices with their start and end apart: 14, of which 8 were waited for; matrix products, arithmetic and copies ran while one was open for 1% of the time, Pallas kernels for 9%

profile of v3, /device:TPU:1, one launch (start us, length us, event | category | flops | bytes accessed | tf_op | source)
XLA Modules:
  0.0 174.7 jit_solution(10409010147051935069)
XLA Ops:
  0.6 1.3 shard_map.213
  2.0 3.9 %collective-permute-start = (bf16[8,512]{1,0:T(8,128)(2,1)}, bf16[8,512]{1,0:T(8,128)(2,1)S(1)}, u32[]{:S(2)}, u32[]{:S(2)}) collective-permute-start(bf16[8,512]{1,0:T(8,128)(2,1)} %shard_map.213), channel_id=1, source_target_pairs={{0,16},{16,32},{32,48},{48,64},{64,80},{80,96},{96,112},{112,128},... | collective-permute-start | bytes 24584 | tf_op jit(solution)/shard_map/ppermute | solution.py:475
  6.5 3.5 %shard_map.215 = (bf16[1024,256]{1,0:T(8,128)(2,1)}, bf16[3072,256]{1,0:T(8,128)(2,1)}) custom-call(s32[2]{0:T(128)} %pad_add_fusion.place, bf16[2048,256]{1,0:T(8,128)(2,1)} %bitcast.20, bf16[2048,256]{1,0:T(8,128)(2,1)} %bitcast.22, bf16[256,2048]{1,0:T(8,128)(2,1)} %bitcast.25), custom_call_target="tpu_custom_call" | custom-call | flops 1073741824 | bytes 1048576 | tf_op jit(solution)/shard_map/pallas_call | solution.py:28
  10.1 6.1 %collective-permute-start.4 = (bf16[3072,256]{1,0:T(8,128)(2,1)}, bf16[3072,256]{1,0:T(8,128)(2,1)S(1)}, u32[]{:S(2)}, u32[]{:S(2)}) collective-permute-start(bf16[3072,256]{1,0:T(8,128)(2,1)} %get-tuple-element.25), channel_id=1, source_target_pairs={{0,1},{1,0},{2,3},{3,2},{4,5},{5,4},{6,7},{7,6},{8,9},{9,8},{10,11... | collective-permute-start | bytes 4718600 | tf_op jit(solution)/shard_map/ppermute | solution.py:469
  16.8 2.6 %shard_map.212 = (bf16[768,256]{1,0:T(8,128)(2,1)}, s32[2,256]{1,0:T(2,128)}) custom-call(s32[1]{0:T(128)} %bitcast.2.place, bf16[256,2048]{1,0:T(8,128)(2,1)} %tokens.1, f32[16,128]{1,0:T(8,128)} %bitcast_convert_fusion.token_gain, s32[2,256]{1,0:T(2,128)} %bitcast.28), custom_call_target="tpu_custom_call" | custom-call | flops 1073741824 | bytes 1048576 | tf_op jit(solution)/shard_map/pallas_call | solution.py:28
  20.0 3.4 %shard_map.214 = (bf16[32,64,128]{2,1,0:T(8,128)(2,1)}, f32[256,256]{1,0:T(8,128)}, bf16[256,128]{1,0:T(8,128)(2,1)}, bf16[256,128]{1,0:T(8,128)(2,1)}, f32[256,8]{1,0:T(8,128)}, /*index=5*/f32[8,256]{1,0:T(8,128)}) custom-call(f32[4]{0:T(128)} %offset.1, f32[4]{0:T(128)} %speed.1, bf16[768,256]{1,0:T(8,128)(2,1)} %get-tuple-element.23.routed, ...), custom_call_target="tpu_custom_call" | custom-call | flops 1073741824 | bytes 1048576 | tf_op jit(solution)/shard_map/pallas_call | solution.py:28
  23.5 26.1 %all_to_all.15.got = bf16[32,64,128]{2,1,0:T(8,128)(2,1)S(1)} all-to-all(bf16[32,64,128]{2,1,0:T(8,128)(2,1)} %get-tuple-element.24), channel_id=1, replica_groups=mesh['ep_0'=8,'ep_1'=4,'tp_0'=8,'tp_1'=2] {'ep_0','ep_1'}, dimensions={0} | all-to-all | bytes 1048576 | tf_op jit(solution)/shard_map/all_to_all | solution.py:472
  49.6 3.3 %collective-permute-start.1 = (bf16[32,48,128]{2,1,0:T(8,128)(2,1)S(1)}, bf16[32,48,128]{2,1,0:T(8,128)(2,1)S(1)}, u32[]{:S(2)}, u32[]{:S(2)}) collective-permute-start(bf16[32,48,128]{2,1,0:T(8,128)(2,1)S(1)} %slice.4.own), channel_id=1, source_target_pairs={{0,2},{2,4},{4,6},{6,8},{8,10},{10,12},{12,14},{14,0},{1,3},{3,5},... | collective-permute-start | bytes 1179656 | tf_op jit(solution)/shard_map/ppermute | solution.py:459
  53.0 3.8 %collective-permute-start.2 = (bf16[32,48,128]{2,1,0:T(8,128)(2,1)S(1)}, bf16[32,48,128]{2,1,0:T(8,128)(2,1)S(1)}, u32[]{:S(2)}, u32[]{:S(2)}) collective-permute-start(bf16[32,48,128]{2,1,0:T(8,128)(2,1)S(1)} %slice.4.own), channel_id=1, source_target_pairs={{0,14},{2,0},{4,2},{6,4},{8,6},{10,8},{12,10},{14,12},{1,15},{3,1}... | collective-permute-start | bytes 1179656 | tf_op jit(solution)/shard_map/ppermute | solution.py:459
  56.8 4.1 %collective-permute-start.3 = (bf16[32,48,128]{2,1,0:T(8,128)(2,1)S(1)}, bf16[32,48,128]{2,1,0:T(8,128)(2,1)S(1)}, u32[]{:S(2)}, u32[]{:S(2)}) collective-permute-start(bf16[32,48,128]{2,1,0:T(8,128)(2,1)S(1)} %slice.4.own), channel_id=1, source_target_pairs={{0,4},{1,13},{2,6},{3,15},{4,8},{5,1},{6,10},{7,3},{8,12},{9,5},{1... | collective-permute-start | bytes 1179656 | tf_op jit(solution)/shard_map/ppermute | solution.py:466
  60.9 1.4 collective-permute-done.1.left
  62.3 1.3 collective-permute-done.2.right
  63.6 11.5 %collective-permute-done.3.across = bf16[32,48,128]{2,1,0:T(8,128)(2,1)S(1)} collective-permute-done((bf16[32,48,128]{2,1,0:T(8,128)(2,1)S(1)}, bf16[32,48,128]{2,1,0:T(8,128)(2,1)S(1)}, u32[]{:S(2)}, u32[]{:S(2)}) %collective-permute-start.3) | collective-permute-done | bytes 393248 | tf_op jit(solution)/shard_map/ppermute | solution.py:466
  75.1 3.0 %shard_map.216 = bf16[768,512]{1,0:T(8,128)(2,1)} custom-call(s32[2]{0:T(128)S(1)} %copy-done, bf16[32,48,128]{2,1,0:T(8,128)(2,1)S(1)} %slice.4.own, bf16[32,48,128]{2,1,0:T(8,128)(2,1)S(1)} %collective-permute-done.1.left, bf16[32,48,128]{2,1,0:T(8,128)(2,1)S(1)} %collective-permute-done.2.right, bf16[32,48,128]{2,1,0:T(8,128)(2,1)S(1)} %collective-permute-done.3.across, ...), custom_call_target="tpu_custom_call" | custom-call | flops 2147483648 | bytes 1048576 | tf_op jit(solution)/shard_map/pallas_call | solution.py:28
  78.1 1.9 %collective-permute-start.5 = (bf16[768,512]{1,0:T(8,128)(2,1)}, bf16[768,512]{1,0:T(8,128)(2,1)}, u32[]{:S(2)}, u32[]{:S(2)}) collective-permute-start(bf16[768,512]{1,0:T(8,128)(2,1)} %shard_map.216), channel_id=1, source_target_pairs={{0,1},{1,0},{2,3},{3,2},{4,5},{5,4},{6,7},{7,6},{8,9},{9,8},{10,11... | collective-permute-start | bytes 2359304 | tf_op jit(solution)/shard_map/ppermute | solution.py:469
  80.0 2.4 %collective-permute-start.7 = (bf16[256,2048]{1,0:T(8,128)(2,1)S(1)}, bf16[256,2048]{1,0:T(8,128)(2,1)}, u32[]{:S(2)}, u32[]{:S(2)}) collective-permute-start(bf16[256,2048]{1,0:T(8,128)(2,1)S(1)} %copy-done.3), channel_id=1, source_target_pairs={{0,1},{1,0},{2,3},{3,2},{4,5},{5,4},{6,7},{7,6},{8,9},{9,8},{10,11... | collective-permute-start | bytes 3145736 | tf_op jit(solution)/shard_map/ppermute | solution.py:469
  82.5 1.3 shard_map.218
  83.8 5.0 %all-to-all-start.1 = ((bf16[32,8,128]{2,1,0:T(8,128)(2,1)}), bf16[32,8,128]{2,1,0:T(8,128)(2,1)S(1)}, u32[]{:S(2)}, u32[]{:S(2)}) async-start(bf16[32,8,128]{2,1,0:T(8,128)(2,1)} %shard_map.218), calls=%async_computation.1 | async-start | bytes 131072 | tf_op jit(solution)/shard_map/all_to_all | solution.py:472
  94.3 3.5 %all-to-all-done.1 = bf16[32,8,128]{2,1,0:T(8,128)(2,1)S(1)} async-done(((bf16[32,8,128]{2,1,0:T(8,128)(2,1)}), bf16[32,8,128]{2,1,0:T(8,128)(2,1)S(1)}, u32[]{:S(2)}, u32[]{:S(2)}) %all-to-all-start.1) | async-done | bytes 65568 | tf_op jit(solution)/shard_map/all_to_all | solution.py:472
  102.3 2.8 %shard_map.220.own = bf16[896,256]{1,0:T(8,128)(2,1)S(1)} custom-call(s32[2]{0:T(128)S(1)} %copy-done, bf16[32,48,128]{2,1,0:T(8,128)(2,1)S(1)} %slice.4.own, bf16[32,48,128]{2,1,0:T(8,128)(2,1)S(1)} %collective-permute-done.1.left, bf16[32,48,128]{2,1,0:T(8,128)(2,1)S(1)} %copy-done.5, bf16[32,48,128]{2,1,0:T(8,128)(2,1)S(1)} %copy-done.7, ...), custom_call_target="tpu_custom_call" | custom-call | flops 2147483648 | bytes 1048576 | tf_op jit(solution)/shard_map/pallas_call | solution.py:28
  105.1 3.2 %collective-permute-start.6 = (bf16[896,256]{1,0:T(8,128)(2,1)S(1)}, bf16[896,256]{1,0:T(8,128)(2,1)S(1)}, u32[]{:S(2)}, u32[]{:S(2)}) collective-permute-start(bf16[896,256]{1,0:T(8,128)(2,1)S(1)} %shard_map.220.own), channel_id=1, source_target_pairs={{0,1},{1,0},{2,3},{3,2},{4,5},{5,4},{6,7},{7,6},{8,9},{9,8},{10,11... | collective-permute-start | bytes 1376264 | tf_op jit(solution)/shard_map/ppermute | solution.py:469
  108.4 1.4 collective-permute-done.6.far
  109.8 2.8 %shard_map.221 = (bf16[2,1024,128]{2,1,0:T(8,128)(2,1)S(1)}, bf16[2,1024,128]{2,1,0:T(8,128)(2,1)S(1)}, bf16[1,1024,128]{2,1,0:T(8,128)(2,1)S(1)}, bf16[3,1024,128]{2,1,0:T(8,128)(2,1)S(1)}) custom-call(bf16[896,256]{1,0:T(8,128)(2,1)S(1)} %shard_map.220.own, bf16[896,256]{1,0:T(8,128)(2,1)S(1)} %collective-permute-done.6.far, ...), custom_call_target="tpu_custom_call" | custom-call | flops 2147483648 | bytes 1048576 | tf_op jit(solution)/shard_map/pallas_call | solution.py:28
  112.6 1.9 %collective-permute-start.8 = (bf16[2,1024,128]{2,1,0:T(8,128)(2,1)S(1)}, bf16[2,1024,128]{2,1,0:T(8,128)(2,1)S(1)}, u32[]{:S(2)}, u32[]{:S(2)}) collective-permute-start(bf16[2,1024,128]{2,1,0:T(8,128)(2,1)S(1)} %get-tuple-element.35), channel_id=1, source_target_pairs={{0,2},{2,4},{4,6},{6,8},{8,10},{10,12},{12,14},{14,0},{1,3},{3,5},... | collective-permute-start | bytes 1572872 | tf_op jit(solution)/shard_map/ppermute | solution.py:459
  114.5 4.6 %collective-permute-start.9 = (bf16[2,1024,128]{2,1,0:T(8,128)(2,1)S(1)}, bf16[2,1024,128]{2,1,0:T(8,128)(2,1)S(1)}, u32[]{:S(2)}, u32[]{:S(2)}) collective-permute-start(bf16[2,1024,128]{2,1,0:T(8,128)(2,1)S(1)} %get-tuple-element.36), channel_id=1, source_target_pairs={{0,14},{2,0},{4,2},{6,4},{8,6},{10,8},{12,10},{14,12},{1,15},{3,1}... | collective-permute-start | bytes 1572872 | tf_op jit(solution)/shard_map/ppermute | solution.py:459
  119.1 3.7 %collective-permute-start.10 = (bf16[1,1024,128]{2,1,0:T(8,128)(2,1)S(1)}, bf16[1,1024,128]{2,1,0:T(8,128)(2,1)S(1)}, u32[]{:S(2)}, u32[]{:S(2)}) collective-permute-start(bf16[1,1024,128]{2,1,0:T(8,128)(2,1)S(1)} %get-tuple-element.37), channel_id=1, source_target_pairs={{0,4},{1,13},{2,6},{3,15},{4,8},{5,1},{6,10},{7,3},{8,12},{9,5},{1... | collective-permute-start | bytes 786440 | tf_op jit(solution)/shard_map/ppermute | solution.py:466
  122.8 17.6 %collective-permute-done.10.from_across = bf16[1,1024,128]{2,1,0:T(8,128)(2,1)S(1)} collective-permute-done((bf16[1,1024,128]{2,1,0:T(8,128)(2,1)S(1)}, bf16[1,1024,128]{2,1,0:T(8,128)(2,1)S(1)}, u32[]{:S(2)}, u32[]{:S(2)}) %collective-permute-start.10) | collective-permute-done | bytes 262176 | tf_op jit(solution)/shard_map/ppermute | solution.py:466
  141.3 2.7 %collective-permute-start.11 = (bf16[1024,128]{1,0:T(8,128)(2,1)S(1)}, bf16[1024,128]{1,0:T(8,128)(2,1)S(1)}, u32[]{:S(2)}, u32[]{:S(2)}) collective-permute-start(bf16[1024,128]{1,0:T(8,128)(2,1)S(1)} %get-tuple-element.39), channel_id=1, source_target_pairs={{0,4},{2,6},{4,8},{6,10},{8,12},{10,14},{12,0},{14,2},{1,5},{3,7},... | collective-permute-start | bytes 786440 | tf_op jit(solution)/shard_map/ppermute | solution.py:459
  143.9 4.7 %collective-permute-start.12 = (bf16[1024,128]{1,0:T(8,128)(2,1)S(1)}, bf16[1024,128]{1,0:T(8,128)(2,1)S(1)}, u32[]{:S(2)}, u32[]{:S(2)}) collective-permute-start(bf16[1024,128]{1,0:T(8,128)(2,1)S(1)} %get-tuple-element.40), channel_id=1, source_target_pairs={{0,12},{2,14},{4,0},{6,2},{8,4},{10,6},{12,8},{14,10},{1,13},{3,15... | collective-permute-start | bytes 786440 | tf_op jit(solution)/shard_map/ppermute | solution.py:459
  148.7 2.4 %collective-permute-done.11.from_up = bf16[1024,128]{1,0:T(8,128)(2,1)S(1)} collective-permute-done((bf16[1024,128]{1,0:T(8,128)(2,1)S(1)}, bf16[1024,128]{1,0:T(8,128)(2,1)S(1)}, u32[]{:S(2)}, u32[]{:S(2)}) %collective-permute-start.11) | collective-permute-done | bytes 262176 | tf_op jit(solution)/shard_map/ppermute | solution.py:459
  151.0 6.6 %collective-permute-done.12.from_down = bf16[1024,128]{1,0:T(8,128)(2,1)S(1)} collective-permute-done((bf16[1024,128]{1,0:T(8,128)(2,1)S(1)}, bf16[1024,128]{1,0:T(8,128)(2,1)S(1)}, u32[]{:S(2)}, u32[]{:S(2)}) %collective-permute-start.12) | collective-permute-done | bytes 262176 | tf_op jit(solution)/shard_map/ppermute | solution.py:459
  158.3 15.3 %all_to_all.16.got = bf16[32,24,128]{2,1,0:T(8,128)(2,1)S(1)} all-to-all(bf16[32,24,128]{2,1,0:T(8,128)(2,1)S(1)} %bitcast.18), channel_id=1, replica_groups=mesh['ep_0'=8,'ep_1'=4,'tp_0'=8,'tp_1'=2] {'ep_0','ep_1'}, dimensions={0} | all-to-all | bytes 393216 | tf_op jit(solution)/shard_map/all_to_all | solution.py:472
  (63 shorter events, 14.4 us)
Async XLA Ops:
  2.0 17.5 %collective-permute-start = (bf16[8,512]{1,0:T(8,128)(2,1)}, bf16[8,512]{1,0:T(8,128)(2,1)S(1)}, u32[]{:S(2)}, u32[]{:S(2)}) collective-permute-start(bf16[8,512]{1,0:T(8,128)(2,1)} %shard_map.213), channel_id=1, source_target_pairs={{0,16},{16,32},{32,48},{48,64},{64,80},{80,96},{96,112},{112,128},... | collective-permute-start | bytes 24584 | tf_op jit(solution)/shard_map/ppermute | solution.py:475
  6.5 9.7 %copy-start.21 = (bf16[2048]{0:T(1024)(128)(2,1)S(1)}, bf16[2048]{0:T(1024)(128)(2,1)}, u32[]{:S(2)}) copy-start(bf16[2048]{0:T(1024)(128)(2,1)} %param.36) | copy-start | bytes 12292
  10.1 65.1 %collective-permute-start.4 = (bf16[3072,256]{1,0:T(8,128)(2,1)}, bf16[3072,256]{1,0:T(8,128)(2,1)S(1)}, u32[]{:S(2)}, u32[]{:S(2)}) collective-permute-start(bf16[3072,256]{1,0:T(8,128)(2,1)} %get-tuple-element.25), channel_id=1, source_target_pairs={{0,1},{1,0},{2,3},{3,2},{4,5},{5,4},{6,7},{7,6},{8,9},{9,8},{10,11... | collective-permute-start | bytes 4718600 | tf_op jit(solution)/shard_map/ppermute | solution.py:469
  23.4 51.7 %copy-start = (s32[2]{0:T(128)S(1)}, s32[2]{0:T(128)}, u32[]{:S(2)}) copy-start(s32[2]{0:T(128)} %pad_add_fusion.place) | copy-start | bytes 28
  49.6 30.4 %copy-start.3 = (bf16[256,2048]{1,0:T(8,128)(2,1)S(1)}, bf16[256,2048]{1,0:T(8,128)(2,1)}, u32[]{:S(2)}) copy-start(bf16[256,2048]{1,0:T(8,128)(2,1)} %result.1) | copy-start | bytes 3145732
  49.6 32.9 %copy-start.23 = (bf16[256]{0:T(256)(128)(2,1)S(1)}, bf16[256]{0:T(256)(128)(2,1)}, u32[]{:S(2)}) copy-start(bf16[256]{0:T(256)(128)(2,1)} %param.33) | copy-start | bytes 1540
  49.6 12.7 %collective-permute-start.1 = (bf16[32,48,128]{2,1,0:T(8,128)(2,1)S(1)}, bf16[32,48,128]{2,1,0:T(8,128)(2,1)S(1)}, u32[]{:S(2)}, u32[]{:S(2)}) collective-permute-start(bf16[32,48,128]{2,1,0:T(8,128)(2,1)S(1)} %slice.4.own), channel_id=1, source_target_pairs={{0,2},{2,4},{4,6},{6,8},{8,10},{10,12},{12,14},{14,0},{1,3},{3,5},... | collective-permute-start | bytes 1179656 | tf_op jit(solution)/shard_map/ppermute | solution.py:459
  53.0 10.6 %collective-permute-start.2 = (bf16[32,48,128]{2,1,0:T(8,128)(2,1)S(1)}, bf16[32,48,128]{2,1,0:T(8,128)(2,1)S(1)}, u32[]{:S(2)}, u32[]{:S(2)}) collective-permute-start(bf16[32,48,128]{2,1,0:T(8,128)(2,1)S(1)} %slice.4.own), channel_id=1, source_target_pairs={{0,14},{2,0},{4,2},{6,4},{8,6},{10,8},{12,10},{14,12},{1,15},{3,1}... | collective-permute-start | bytes 1179656 | tf_op jit(solution)/shard_map/ppermute | solution.py:459
  56.8 18.4 %collective-permute-start.3 = (bf16[32,48,128]{2,1,0:T(8,128)(2,1)S(1)}, bf16[32,48,128]{2,1,0:T(8,128)(2,1)S(1)}, u32[]{:S(2)}, u32[]{:S(2)}) collective-permute-start(bf16[32,48,128]{2,1,0:T(8,128)(2,1)S(1)} %slice.4.own), channel_id=1, source_target_pairs={{0,4},{1,13},{2,6},{3,15},{4,8},{5,1},{6,10},{7,3},{8,12},{9,5},{1... | collective-permute-start | bytes 1179656 | tf_op jit(solution)/shard_map/ppermute | solution.py:466
  63.6 14.5 %copy-start.4 = (bf16[32,48,128]{2,1,0:T(8,128)(2,1)}, bf16[32,48,128]{2,1,0:T(8,128)(2,1)S(1)}, u32[]{:S(2)}) copy-start(bf16[32,48,128]{2,1,0:T(8,128)(2,1)S(1)} %collective-permute-done.2.right) | copy-start | bytes 1179652
  75.1 3.0 %copy-start.6 = (bf16[32,48,128]{2,1,0:T(8,128)(2,1)}, bf16[32,48,128]{2,1,0:T(8,128)(2,1)S(1)}, u32[]{:S(2)}) copy-start(bf16[32,48,128]{2,1,0:T(8,128)(2,1)S(1)} %collective-permute-done.3.across) | copy-start | bytes 1179652
  78.1 23.4 %collective-permute-start.5 = (bf16[768,512]{1,0:T(8,128)(2,1)}, bf16[768,512]{1,0:T(8,128)(2,1)}, u32[]{:S(2)}, u32[]{:S(2)}) collective-permute-start(bf16[768,512]{1,0:T(8,128)(2,1)} %shard_map.216), channel_id=1, source_target_pairs={{0,1},{1,0},{2,3},{3,2},{4,5},{5,4},{6,7},{7,6},{8,9},{9,8},{10,11... | collective-permute-start | bytes 2359304 | tf_op jit(solution)/shard_map/ppermute | solution.py:469
  80.0 28.3 %collective-permute-start.7 = (bf16[256,2048]{1,0:T(8,128)(2,1)S(1)}, bf16[256,2048]{1,0:T(8,128)(2,1)}, u32[]{:S(2)}, u32[]{:S(2)}) collective-permute-start(bf16[256,2048]{1,0:T(8,128)(2,1)S(1)} %copy-done.3), channel_id=1, source_target_pairs={{0,1},{1,0},{2,3},{3,2},{4,5},{5,4},{6,7},{7,6},{8,9},{9,8},{10,11... | collective-permute-start | bytes 3145736 | tf_op jit(solution)/shard_map/ppermute | solution.py:469
  82.5 6.4 %copy-start.10 = (f32[4]{0:T(128)S(1)}, f32[4]{0:T(128)}, u32[]{:S(2)}) copy-start(f32[4]{0:T(128)} %bypass.1) | copy-start | bytes 52
  82.5 6.4 %copy-start.15 = (bf16[256,128]{1,0:T(8,128)(2,1)S(1)}, bf16[256,128]{1,0:T(8,128)(2,1)}, u32[]{:S(2)}) copy-start(bf16[256,128]{1,0:T(8,128)(2,1)} %get-tuple-element.28.c) | copy-start | bytes 196612
  83.8 14.0 %all-to-all-start.1 = ((bf16[32,8,128]{2,1,0:T(8,128)(2,1)}), bf16[32,8,128]{2,1,0:T(8,128)(2,1)S(1)}, u32[]{:S(2)}, u32[]{:S(2)}) async-start(bf16[32,8,128]{2,1,0:T(8,128)(2,1)} %shard_map.218), calls=%async_computation.1 | async-start | bytes 131072 | tf_op jit(solution)/shard_map/all_to_all | solution.py:472
  88.9 1.0 copy-start.12
  97.8 0.9 copy-start.8
  99.6 0.9 copy-start.18
  100.6 1.2 copy-start.1
  100.6 1.5 copy-start.2
  100.6 1.6 copy-start.5
  100.6 1.7 copy-start.7
  102.3 7.4 %copy-start.11 = (bf16[1024,256]{1,0:T(8,128)(2,1)S(1)}, bf16[1024,256]{1,0:T(8,128)(2,1)}, u32[]{:S(2)}) copy-start(bf16[1024,256]{1,0:T(8,128)(2,1)} %get-tuple-element.33.keep) | copy-start | bytes 1572868
  105.1 4.7 %collective-permute-start.6 = (bf16[896,256]{1,0:T(8,128)(2,1)S(1)}, bf16[896,256]{1,0:T(8,128)(2,1)S(1)}, u32[]{:S(2)}, u32[]{:S(2)}) collective-permute-start(bf16[896,256]{1,0:T(8,128)(2,1)S(1)} %shard_map.220.own), channel_id=1, source_target_pairs={{0,1},{1,0},{2,3},{3,2},{4,5},{5,4},{6,7},{7,6},{8,9},{9,8},{10,11... | collective-permute-start | bytes 1376264 | tf_op jit(solution)/shard_map/ppermute | solution.py:469
  112.6 27.8 %collective-permute-start.8 = (bf16[2,1024,128]{2,1,0:T(8,128)(2,1)S(1)}, bf16[2,1024,128]{2,1,0:T(8,128)(2,1)S(1)}, u32[]{:S(2)}, u32[]{:S(2)}) collective-permute-start(bf16[2,1024,128]{2,1,0:T(8,128)(2,1)S(1)} %get-tuple-element.35), channel_id=1, source_target_pairs={{0,2},{2,4},{4,6},{6,8},{8,10},{10,12},{12,14},{14,0},{1,3},{3,5},... | collective-permute-start | bytes 1572872 | tf_op jit(solution)/shard_map/ppermute | solution.py:459
  114.5 25.9 %collective-permute-start.9 = (bf16[2,1024,128]{2,1,0:T(8,128)(2,1)S(1)}, bf16[2,1024,128]{2,1,0:T(8,128)(2,1)S(1)}, u32[]{:S(2)}, u32[]{:S(2)}) collective-permute-start(bf16[2,1024,128]{2,1,0:T(8,128)(2,1)S(1)} %get-tuple-element.36), channel_id=1, source_target_pairs={{0,14},{2,0},{4,2},{6,4},{8,6},{10,8},{12,10},{14,12},{1,15},{3,1}... | collective-permute-start | bytes 1572872 | tf_op jit(solution)/shard_map/ppermute | solution.py:459
  119.1 21.3 %collective-permute-start.10 = (bf16[1,1024,128]{2,1,0:T(8,128)(2,1)S(1)}, bf16[1,1024,128]{2,1,0:T(8,128)(2,1)S(1)}, u32[]{:S(2)}, u32[]{:S(2)}) collective-permute-start(bf16[1,1024,128]{2,1,0:T(8,128)(2,1)S(1)} %get-tuple-element.37), channel_id=1, source_target_pairs={{0,4},{1,13},{2,6},{3,15},{4,8},{5,1},{6,10},{7,3},{8,12},{9,5},{1... | collective-permute-start | bytes 786440 | tf_op jit(solution)/shard_map/ppermute | solution.py:466
  141.2 32.3 %copy-start.9 = (f32[256,2]{0,1:T(2,128)S(1)}, f32[256,2]{0,1:T(2,128)}, u32[]{:S(2)}) copy-start(f32[256,2]{0,1:T(2,128)} %param.41) | copy-start | bytes 6148
  141.3 32.3 %copy-start.19 = (s32[2,256]{1,0:T(2,128)S(1)}, s32[2,256]{1,0:T(2,128)}, u32[]{:S(2)}) copy-start(s32[2,256]{1,0:T(2,128)} %get-tuple-element.43.slots) | copy-start | bytes 6148
  141.3 9.8 %collective-permute-start.11 = (bf16[1024,128]{1,0:T(8,128)(2,1)S(1)}, bf16[1024,128]{1,0:T(8,128)(2,1)S(1)}, u32[]{:S(2)}, u32[]{:S(2)}) collective-permute-start(bf16[1024,128]{1,0:T(8,128)(2,1)S(1)} %get-tuple-element.39), channel_id=1, source_target_pairs={{0,4},{2,6},{4,8},{6,10},{8,12},{10,14},{12,0},{14,2},{1,5},{3,7},... | collective-permute-start | bytes 786440 | tf_op jit(solution)/shard_map/ppermute | solution.py:459
  143.9 13.7 %collective-permute-start.12 = (bf16[1024,128]{1,0:T(8,128)(2,1)S(1)}, bf16[1024,128]{1,0:T(8,128)(2,1)S(1)}, u32[]{:S(2)}, u32[]{:S(2)}) collective-permute-start(bf16[1024,128]{1,0:T(8,128)(2,1)S(1)} %get-tuple-element.40), channel_id=1, source_target_pairs={{0,12},{2,14},{4,0},{6,2},{8,4},{10,6},{12,8},{14,10},{1,13},{3,15... | collective-permute-start | bytes 786440 | tf_op jit(solution)/shard_map/ppermute | solution.py:459
  (6 other events, 4.6 us)

commit v4 on v3

--- a/solution.py
+++ b/solution.py
@@ -16,6 +16,7 @@
 EP_TP = ("ep_0", "ep_1", "tp_0", "tp_1")
 RIM = 8
 PIECE = 8
+HOMES = (3, 5, 4, 6, 1, 7, 0, 2)
 
 NORM_EPS = 1e-06
 F32 = jnp.float32
@@ -36,6 +37,13 @@
     )(*ins)
 
 
+def placed(body):
+    def run(core, chip, *refs):
+        body((core[0], chip[0]), *refs)
+
+    return run
+
+
 def shaped(*shape, dtype=BF16):
     return jax.ShapeDtypeStruct(shape, dtype)
 
@@ -63,14 +71,14 @@
 
 
 def route_body(experts, place, tokens, token_gain, picks, routed, slots_out):
-    lanes = token_gain.shape[1]
+    lanes = 128
     total_rows, token_count = routed.shape[0], tokens.shape[0]
     capacity = total_rows // experts
     data = tokens[...].astype(F32)
     scale = lax.rsqrt(jnp.mean(data * data, axis=1, keepdims=True) + NORM_EPS)
-    first = pl.multiple_of(place[0] * lanes, lanes)
+    first = pl.multiple_of(place[0] * (2 * lanes), 2 * lanes)
     chosen = tokens[:, pl.ds(first, 2 * lanes)].astype(F32)
-    gain = jnp.concatenate([token_gain[pl.ds(place[0] + k, 1), :] for k in range(2)], axis=1)
+    gain = token_gain[pl.ds(first, 2 * lanes)].astype(F32).reshape(1, 2 * lanes)
     chosen = (chosen * scale * gain).astype(BF16)
     expert = iota((experts, token_count), 0)
     earlier = (
@@ -222,11 +230,11 @@
     gated = (y[...] + carried) * silu(valve[...].astype(F32))
     scale = lax.rsqrt(jnp.mean(gated * gated, axis=1, keepdims=True) + NORM_EPS)
     normed[...] = gated * scale * jnp.concatenate([gain[0:1, :], gain[1:2, :]], axis=1)
-    chips = 8
+    chips = len(HOMES)
     rows = mine.shape[0] // chips
     for target, core in ((mine, place[0]), (other, 1 - place[0])):
         parts = []
-        for k in range(chips):
+        for k in HOMES:
             at = (2 * ((place[1] + k) % chips) + core) * rows
             parts.append(normed[pl.ds(pl.multiple_of(at, rows), rows), :])
         target[...] = jnp.concatenate(parts, axis=0).astype(BF16)
@@ -304,9 +312,8 @@
     give[0:half, :] = valve[theirs, :]
     give[half : 2 * half, :] = expand[theirs, :]
     depth = contract.shape[0]
-    chips = 8
-    for k in range(chips):
-        base = 2 * ((place[1] + k) % chips)
+    for k, home in enumerate(HOMES):
+        base = 2 * ((place[1] + home) % len(HOMES))
         row, lane = k // 2 * depth, k % 2 * 128
         for target, core, first in ((keep, place[0], 0), (give, 1 - place[0], 2 * half)):
             target[first + row : first + row + depth, lane : lane + 128] = contract[
@@ -314,42 +321,37 @@
             ]
 
 
-def down_body(own, far, rows, keep, weights, result, result_far, right, left, across, stay):
-    chips, depth = 8, own.shape[1]
-    count = rows.shape[0]
-    total = own.shape[0] - count
+def down_body(start, own, far, rows, keep, weights, result, result_far, *outs):
+    depth = own.shape[1]
+    each = rows.shape[0] // len(HOMES)
+    total = own.shape[0] - rows.shape[0]
     far_first = weights.shape[0] - keep.shape[0]
     block = total // 2
-    homes = {
-        0: (stay, 0), 1: (right, 0), 2: (stay, 1), 3: (right, 1),
-        4: (across, 0), 5: (left, 1), 6: (stay, 2), 7: (left, 0),
-    }
 
     def step(i, _):
         at = pl.ds(pl.multiple_of(i * block, block), block)
         near, beyond = own[at, :], far[at, :]
-        for k in range(0, chips, 2):
-            row = k // 2 * depth
+        for k in range(0, len(outs), 2):
+            row = (start + k) // 2 * depth
             product = dot(near, keep[row : row + depth, :]) + dot(
                 beyond, weights[far_first + row : far_first + row + depth, :]
             )
             for j in range(2):
-                home, slot = homes[k + j]
-                home[slot, at, :] = product[:, j * 128 : (j + 1) * 128].astype(BF16)
+                outs[k + j][at, :] = product[:, j * 128 : (j + 1) * 128].astype(BF16)
         return 0
 
     lax.fori_loop(0, total // block, step, 0)
-    near, beyond = rows[...], far[total:, :]
-    each, wide = count // chips, 512
-    for first in range(0, result.shape[1], wide):
-        columns = slice(first, first + wide)
+    first, last = start * each, (start + len(outs)) * each
+    near, beyond = rows[first:last, :], far[total + first : total + last, :]
+    wide = 512
+    for column in range(0, result.shape[1], wide):
+        columns = slice(column, column + wide)
         product = dot(near, result[:, columns]) + dot(beyond, result_far[:, columns])
         product = product.astype(BF16)
-        for k in range(chips):
-            home, slot = homes[k]
+        for k, out in enumerate(outs):
             for j in range(wide // 128):
-                to = total + (first // 128 + j) * each
-                home[slot, to : to + each, :] = product[
+                to = total + (column // 128 + j) * each
+                out[to : to + each, :] = product[
                     k * each : (k + 1) * each, j * 128 : (j + 1) * 128
                 ]
 
@@ -381,21 +383,18 @@
     )(*parts)
 
 
-def merge_body(place, stay, from_left, from_right, from_across, so_far, up_two, down_two):
-    far = from_across[0].astype(F32)
+def merge_body(place, stay_up, stay_down, from_left, from_right, from_across, up, down):
+    far = from_across[...].astype(F32)
     core = jnp.full((1, 1), place[0])
-    so_far[...] = (
-        stay[0].astype(F32) + from_left[0].astype(F32) + from_right[0].astype(F32)
-    )
-    up = stay[1].astype(F32) + from_left[1].astype(F32) + jnp.where(core == 0, far, 0.0)
-    down = stay[2].astype(F32) + from_right[1].astype(F32) + jnp.where(core == 1, far, 0.0)
-    up_two[...] = up.astype(BF16)
-    down_two[...] = down.astype(BF16)
-
-
-def total_body(so_far, from_up, from_down, out, rows_out):
-    total = so_far[...] + from_up[...].astype(F32) + from_down[...].astype(F32)
-    total = total.astype(BF16)
+    total = stay_up[...].astype(F32) + from_left[...].astype(F32)
+    up[...] = (total + jnp.where(core == 0, far, 0.0)).astype(BF16)
+    total = stay_down[...].astype(F32) + from_right[...].astype(F32)
+    down[...] = (total + jnp.where(core == 1, far, 0.0)).astype(BF16)
+
+
+def total_body(stay, left, right, up, down, out, rows_out):
+    total = stay[...].astype(F32) + left[...].astype(F32) + right[...].astype(F32)
+    total = (total + up[...].astype(F32) + down[...].astype(F32)).astype(BF16)
     count, lanes = out.shape
     rows, width = rows_out.shape
     out[...] = total[0:count]
@@ -449,37 +448,40 @@
     capacity = 3 * token_count * TOPK // (2 * ep_count)
     lanes = model_width // lax.axis_size(TP)
     total_rows = ep_count * capacity
-    place = jnp.stack([core, chip])
+    place = (core.reshape(1), chip.reshape(1))
     valve = specialist_valve_matrix.reshape(model_width, -1)
     expand = specialist_expand_matrix.reshape(model_width, -1)
     contract = specialist_contract_matrix.reshape(-1, model_width)
     hidden_width = valve.shape[1]
 
+    def permuted(x, axis, pairs):
+        return lax.ppermute(x, axis, pairs)
+
     def around(x, distance):
-        return lax.ppermute(x, "tp_0", [(i, (i + distance) % chips) for i in range(chips)])
+        return permuted(x, "tp_0", [(i, (i + distance) % chips) for i in range(chips)])
 
     def across(x):
         pairs = []
         for i in range(chips):
             pairs.append((2 * i, 2 * ((i + 2) % chips)))
             pairs.append((2 * i + 1, 2 * ((i - 2) % chips) + 1))
-        return lax.ppermute(x, TP, pairs)
+        return permuted(x, TP, pairs)
 
     def partner(x):
-        return lax.ppermute(x, "tp_1", [(0, 1), (1, 0)])
+        return permuted(x, "tp_1", [(0, 1), (1, 0)])
 
     def exchanged(x, axis):
         return lax.all_to_all(x, axis, 0, 0, tiled=True)
 
     rim = last_rows(blender_incoming_features, entry_latent_matrix, exit_latent_matrix)
-    rim = lax.ppermute(rim, EP, [(i, i + 1) for i in range(ep_count - 1)])
+    rim = permuted(rim, EP, [(i, i + 1) for i in range(ep_count - 1)])
     routed, slots = call(
         functools.partial(route_body, ep_count),
         (shaped(total_rows, 2 * lanes), shaped(TOPK, token_count, dtype=jnp.int32)),
         (
-            (core * chips + chip % 4 * 2).reshape(1),
+            (core * (chips // 2) + chip % (chips // 2)).reshape(1),
             latter_microbatch_activations,
-            specialist_rescale_coefs.astype(F32).reshape(-1, lanes),
+            specialist_rescale_coefs,
             specialist_picks.T,
         ),
         1 << 30,
@@ -520,12 +522,12 @@
 
     half = model_width // 2
     keep, give = call(
-        split_body,
+        placed(split_body),
         (shaped(half, hidden_width), shaped(3 * half, hidden_width)),
-        (place, valve, expand, contract),
+        (*place, valve, expand, contract),
         1 << 30,
         None,
-        smem=1,
+        smem=2,
     )
     weights_far = partner(give)
     result_far = partner(blender_result_matrix)
@@ -535,12 +537,12 @@
     left, right = around(own, 1), around(own, -1)
     pieces = (own, left, right, beyond)
     theirs = call(
-        theirs_body,
+        placed(theirs_body),
         shaped(total_rows, 2 * hidden_width),
-        (place, *pieces, weights_far),
+        (*place, *pieces, weights_far),
         1 << 31,
         10,
-        smem=1,
+        smem=2,
     )
     theirs = partner(theirs)
 
@@ -548,10 +550,10 @@
     enter = exchanged(enter, EP).reshape(width, state)
     row_count = count // 2
     mine_rows, other_rows = call(
-        finish_body,
+        placed(finish_body),
         (shaped(row_count, width),) * 2,
         (
-            place,
+            *place,
             y,
             c,
             columns,
@@ -562,45 +564,48 @@
         1 << 31,
         8,
         scratch=(pltpu.VMEM((count, width), F32),),
-        smem=1,
+        smem=2,
     )
     ours = call(
-        ours_body,
+        placed(ours_body),
         shaped(total_rows + row_count, hidden_width),
-        (place, *pieces, valve, expand, theirs, other_rows),
+        (*place, *pieces, valve, expand, theirs, other_rows),
         1 << 31,
         10,
-        smem=1,
+        smem=2,
     )
     ours_far = partner(ours)
     row_block = count * model_width // (2 * chips * lanes)
     all_rows = total_rows + row_block
-    to_right, to_left, to_across, stay = call(
-        down_body,
-        tuple(shaped(k, all_rows, lanes) for k in (2, 2, 1, 3)),
-        (ours, ours_far, mine_rows, keep, weights_far, blender_result_matrix, result_far),
-        1 << 31,
-        14,
-    )
-    from_left, from_right = around(to_right, 1), around(to_left, -1)
-    from_across = across(to_across)
-    so_far, up_two, down_two = call(
-        merge_body,
-        (
-            shaped(all_rows, lanes, dtype=F32),
-            shaped(all_rows, lanes),
-            shaped(all_rows, lanes),
-        ),
-        (place, stay, from_left, from_right, from_across),
+
+    def partials(start):
+        return call(
+            functools.partial(down_body, start),
+            (shaped(all_rows, lanes),) * 4,
+            (ours, ours_far, mine_rows, keep, weights_far, blender_result_matrix, result_far),
+            1 << 31,
+            12,
+        )
+
+    for_three, for_five, for_four, for_six = partials(0)
+    from_across = across(for_four)
+    from_left = around(for_three, 1)
+    from_right = around(for_five, -1)
+    for_one, for_seven, stay, for_two = partials(4)
+    left_of_me, right_of_me = around(for_one, 1), around(for_seven, -1)
+    up_two, down_two = call(
+        placed(merge_body),
+        (shaped(all_rows, lanes),) * 2,
+        (*place, for_two, for_six, from_left, from_right, from_across),
         1 << 29,
         6,
-        smem=1,
+        smem=2,
     )
     from_up, from_down = around(up_two, 2), around(down_two, -2)
     summed, mixed_a = call(
         total_body,
         (shaped(total_rows, lanes), shaped(count // (2 * chips), model_width)),
-        (so_far, from_up, from_down),
+        (stay, left_of_me, right_of_me, from_up, from_down),
         1 << 29,
         4,
     )
@@ -620,7 +625,12 @@
         inside_body(x, b, c, columns, rows, bypass, out)
 
     return call(
-        body, shaped(*x.shape, dtype=F32), (bypass, x, b, c, columns, rows), 1 << 31, 8, smem=1
+        body,
+        shaped(*x.shape, dtype=F32),
+        (bypass, x, b, c, columns, rows),
+        1 << 31,
+        None,
+        smem=1,
     )
 
 

time: 177 us -> 168 us (0.949)
  waiting for transfers between devices: 45.7 us -> 35.8 us
  starting transfers between devices: 51.5 us -> 58 us
  local copies, waits for them, and re-layouts: 8.33 us -> 4.77 us
  blocking collectives: 41.4 us -> 39.5 us
    ppermute x13 -> x15, waiting for transfers between devices: 42.1 us -> 29.5 us  [permuted(): return lax.ppermute(x, axis, pairs)]
    ppermute x13 -> x15, starting transfers between devices: 46.4 us -> 52.9 us  [permuted(): return lax.ppermute(x, axis, pairs)]
    unnamed x48 -> x32, local copies, waits for them, and re-layouts: 8.3 us -> 4.74 us
    all_to_all x1, waiting for transfers between devices: 3.53 us -> 6.37 us  [exchanged(): return lax.all_to_all(x, axis, 0, 0, tiled=True)]
    all_to_all x2, blocking collectives: 41.4 us -> 39.5 us  [exchanged(): return lax.all_to_all(x, axis, 0, 0, tiled=True)]
    pallas_call x12 -> x13, Pallas kernels: 24.3 us -> 25.9 us  [call(): pl.pallas_call(body, out_shape=outs, in_specs=[SMEM] * smem + [VMEM] * (l...]
  transfers between devices with their start and end apart: 14 -> 16, of which waited for: 8 -> 8; matrix products, arithmetic and copies ran while one was open for 1% -> 0% of each run, Pallas kernels for 9% -> 12%
where the time goes in v4:
time: 168 us; the launch traced here: 166 us
  starting transfers between devices  58 us (35%)
  blocking collectives  39.5 us (24%)
  waiting for transfers between devices  35.8 us (21%)
  Pallas kernels  27.3 us (16%)
  local copies, waits for them, and re-layouts  4.77 us (3%)
    ppermute x15, starting transfers between devices, permuted(): return lax.ppermute(x, axis, pairs)  52.9 us
    all_to_all x2, blocking collectives, exchanged(): return lax.all_to_all(x, axis, 0, 0, tiled=True)  39.5 us
    ppermute x15, waiting for transfers between devices, permuted(): return lax.ppermute(x, axis, pairs)  29.5 us
    pallas_call x13, Pallas kernels, call(): pl.pallas_call(body, out_shape=outs, in_specs=[SMEM] * smem + [VMEM] * (l...  25.9 us
    all_to_all x1, waiting for transfers between devices, exchanged(): return lax.all_to_all(x, axis, 0, 0, tiled=True)  6.37 us
    all_to_all x1, starting transfers between devices, exchanged(): return lax.all_to_all(x, axis, 0, 0, tiled=True)  5.04 us
    unnamed x32, local copies, waits for them, and re-layouts  4.74 us
  transfers between devices with their start and end apart: 16, of which 8 were waited for; matrix products, arithmetic and copies ran while one was open for 0% of the time, Pallas kernels for 12%

profile of v4, /device:TPU:1, one launch (start us, length us, event | category | flops | bytes accessed | tf_op | source)
XLA Modules:
  0.0 166.4 jit_solution(17854862005579634934)
XLA Ops:
  2.0 3.9 %collective-permute-start = (bf16[8,512]{1,0:T(8,128)(2,1)}, bf16[8,512]{1,0:T(8,128)(2,1)S(1)}, u32[]{:S(2)}, u32[]{:S(2)}) collective-permute-start(bf16[8,512]{1,0:T(8,128)(2,1)} %shard_map.213), channel_id=1, source_target_pairs={{0,16},{16,32},{32,48},{48,64},{64,80},{80,96},{96,112},{112,128},... | collective-permute-start | bytes 24584 | tf_op jit(solution)/shard_map/ppermute | solution.py:458
  5.9 3.5 %shard_map.215 = (bf16[1024,256]{1,0:T(8,128)(2,1)}, bf16[3072,256]{1,0:T(8,128)(2,1)}) custom-call(s32[1]{0:T(128)} %bitcast.core, s32[1]{0:T(128)} %bitcast.1.chip, bf16[2048,256]{1,0:T(8,128)(2,1)} %bitcast.17, bf16[2048,256]{1,0:T(8,128)(2,1)} %bitcast.19, bf16[256,2048]{1,0:T(8,128)(2,1)} %bitcast.22), custom_call_target="tpu_custom_call" | custom-call | flops 1073741824 | bytes 1048576 | tf_op jit(solution)/shard_map/pallas_call | solution.py:29
  9.5 6.1 %collective-permute-start.4 = (bf16[3072,256]{1,0:T(8,128)(2,1)}, bf16[3072,256]{1,0:T(8,128)(2,1)S(1)}, u32[]{:S(2)}, u32[]{:S(2)}) collective-permute-start(bf16[3072,256]{1,0:T(8,128)(2,1)} %get-tuple-element.28), channel_id=1, source_target_pairs={{0,1},{1,0},{2,3},{3,2},{4,5},{5,4},{6,7},{7,6},{8,9},{9,8},{10,11... | collective-permute-start | bytes 4718600 | tf_op jit(solution)/shard_map/ppermute | solution.py:458
  15.6 2.6 %shard_map.212 = (bf16[768,256]{1,0:T(8,128)(2,1)}, s32[2,256]{1,0:T(2,128)}) custom-call(s32[1]{0:T(128)} %bitcast.2.place, bf16[256,2048]{1,0:T(8,128)(2,1)} %tokens.1, bf16[2048]{0:T(1024)(128)(2,1)} %token_gain.1, s32[2,256]{1,0:T(2,128)} %bitcast.25), custom_call_target="tpu_custom_call" | custom-call | flops 1073741824 | bytes 1048576 | tf_op jit(solution)/shard_map/pallas_call | solution.py:29
  18.8 3.4 %shard_map.214 = (bf16[32,64,128]{2,1,0:T(8,128)(2,1)}, f32[256,256]{1,0:T(8,128)}, bf16[256,128]{1,0:T(8,128)(2,1)}, bf16[256,128]{1,0:T(8,128)(2,1)}, f32[256,8]{1,0:T(8,128)}, /*index=5*/f32[8,256]{1,0:T(8,128)}) custom-call(f32[4]{0:T(128)} %offset.1, f32[4]{0:T(128)} %speed.1, bf16[768,256]{1,0:T(8,128)(2,1)} %get-tuple-element.26.routed, ...), custom_call_target="tpu_custom_call" | custom-call | flops 1073741824 | bytes 1048576 | tf_op jit(solution)/shard_map/pallas_call | solution.py:29
  22.3 26.1 %all_to_all.15.got = bf16[32,64,128]{2,1,0:T(8,128)(2,1)S(1)} all-to-all(bf16[32,64,128]{2,1,0:T(8,128)(2,1)} %get-tuple-element.27), channel_id=1, replica_groups=mesh['ep_0'=8,'ep_1'=4,'tp_0'=8,'tp_1'=2] {'ep_0','ep_1'}, dimensions={0} | all-to-all | bytes 1048576 | tf_op jit(solution)/shard_map/all_to_all | solution.py:474
  48.4 3.3 %collective-permute-start.1 = (bf16[32,48,128]{2,1,0:T(8,128)(2,1)S(1)}, bf16[32,48,128]{2,1,0:T(8,128)(2,1)S(1)}, u32[]{:S(2)}, u32[]{:S(2)}) collective-permute-start(bf16[32,48,128]{2,1,0:T(8,128)(2,1)S(1)} %slice.4.refs_0_), channel_id=1, source_target_pairs={{0,2},{2,4},{4,6},{6,8},{8,10},{10,12},{12,14},{14,0},{1,3},{3,5},... | collective-permute-start | bytes 1179656 | tf_op jit(solution)/shard_map/ppermute | solution.py:458
  51.7 3.8 %collective-permute-start.2 = (bf16[32,48,128]{2,1,0:T(8,128)(2,1)S(1)}, bf16[32,48,128]{2,1,0:T(8,128)(2,1)S(1)}, u32[]{:S(2)}, u32[]{:S(2)}) collective-permute-start(bf16[32,48,128]{2,1,0:T(8,128)(2,1)S(1)} %slice.4.refs_0_), channel_id=1, source_target_pairs={{0,14},{2,0},{4,2},{6,4},{8,6},{10,8},{12,10},{14,12},{1,15},{3,1}... | collective-permute-start | bytes 1179656 | tf_op jit(solution)/shard_map/ppermute | solution.py:458
  55.6 4.1 %collective-permute-start.3 = (bf16[32,48,128]{2,1,0:T(8,128)(2,1)S(1)}, bf16[32,48,128]{2,1,0:T(8,128)(2,1)S(1)}, u32[]{:S(2)}, u32[]{:S(2)}) collective-permute-start(bf16[32,48,128]{2,1,0:T(8,128)(2,1)S(1)} %slice.4.refs_0_), channel_id=1, source_target_pairs={{0,4},{1,13},{2,6},{3,15},{4,8},{5,1},{6,10},{7,3},{8,12},{9,5},{1... | collective-permute-start | bytes 1179656 | tf_op jit(solution)/shard_map/ppermute | solution.py:458
  62.4 11.5 %collective-permute-done.3.refs_3_ = bf16[32,48,128]{2,1,0:T(8,128)(2,1)S(1)} collective-permute-done((bf16[32,48,128]{2,1,0:T(8,128)(2,1)S(1)}, bf16[32,48,128]{2,1,0:T(8,128)(2,1)S(1)}, u32[]{:S(2)}, u32[]{:S(2)}) %collective-permute-start.3) | collective-permute-done | bytes 393248 | tf_op jit(solution)/shard_map/ppermute | solution.py:458
  73.9 2.4 %shard_map.216 = bf16[768,512]{1,0:T(8,128)(2,1)} custom-call(s32[1]{0:T(128)} %bitcast.core, s32[1]{0:T(128)} %bitcast.1.chip, bf16[32,48,128]{2,1,0:T(8,128)(2,1)S(1)} %slice.4.refs_0_, bf16[32,48,128]{2,1,0:T(8,128)(2,1)S(1)} %collective-permute-done.1.refs_1_, bf16[32,48,128]{2,1,0:T(8,128)(2,1)S(1)} %collective-permute-done.2.refs_2_, ...), custom_call_target="tpu_custom_call" | custom-call | flops 2147483648 | bytes 1048576 | tf_op jit(solution)/shard_map/pallas_call | solution.py:29
  76.3 1.9 %collective-permute-start.5 = (bf16[768,512]{1,0:T(8,128)(2,1)}, bf16[768,512]{1,0:T(8,128)(2,1)}, u32[]{:S(2)}, u32[]{:S(2)}) collective-permute-start(bf16[768,512]{1,0:T(8,128)(2,1)} %shard_map.216), channel_id=1, source_target_pairs={{0,1},{1,0},{2,3},{3,2},{4,5},{5,4},{6,7},{7,6},{8,9},{9,8},{10,11... | collective-permute-start | bytes 2359304 | tf_op jit(solution)/shard_map/ppermute | solution.py:458
  78.2 2.4 %collective-permute-start.7 = (bf16[256,2048]{1,0:T(8,128)(2,1)S(1)}, bf16[256,2048]{1,0:T(8,128)(2,1)}, u32[]{:S(2)}, u32[]{:S(2)}) collective-permute-start(bf16[256,2048]{1,0:T(8,128)(2,1)S(1)} %copy-done.2), channel_id=1, source_target_pairs={{0,1},{1,0},{2,3},{3,2},{4,5},{5,4},{6,7},{7,6},{8,9},{9,8},{10,11... | collective-permute-start | bytes 3145736 | tf_op jit(solution)/shard_map/ppermute | solution.py:458
  82.0 5.0 %all-to-all-start.1 = ((bf16[32,8,128]{2,1,0:T(8,128)(2,1)}), bf16[32,8,128]{2,1,0:T(8,128)(2,1)S(1)}, u32[]{:S(2)}, u32[]{:S(2)}) async-start(bf16[32,8,128]{2,1,0:T(8,128)(2,1)} %shard_map.218), calls=%async_computation.1 | async-start | bytes 131072 | tf_op jit(solution)/shard_map/all_to_all | solution.py:474
  87.0 2.6 %shard_map.217.refs_0_ = f32[256,256]{1,0:T(8,128)} custom-call(f32[4]{0:T(128)} %bypass.1, f32[256,256]{1,0:T(8,128)} %get-tuple-element.29.x, bf16[256,128]{1,0:T(8,128)(2,1)} %get-tuple-element.30.b, bf16[256,128]{1,0:T(8,128)(2,1)} %get-tuple-element.31.c.refs_1_, f32[256,8]{1,0:T(8,128)} %get-tuple-element.32.columns.refs_2_, ...), custom_call_target="tpu_custom_call" | custom-call | flops 2147483648 | bytes 1048576 | tf_op jit(solution)/shard_map/pallas_call | solution.py:29
  89.6 6.4 %all-to-all-done.1 = bf16[32,8,128]{2,1,0:T(8,128)(2,1)S(1)} async-done(((bf16[32,8,128]{2,1,0:T(8,128)(2,1)}), bf16[32,8,128]{2,1,0:T(8,128)(2,1)S(1)}, u32[]{:S(2)}, u32[]{:S(2)}) %all-to-all-start.1) | async-done | bytes 65568 | tf_op jit(solution)/shard_map/all_to_all | solution.py:474
  100.5 2.8 %shard_map.220.own = bf16[896,256]{1,0:T(8,128)(2,1)S(1)} custom-call(s32[1]{0:T(128)} %bitcast.core, s32[1]{0:T(128)} %bitcast.1.chip, bf16[32,48,128]{2,1,0:T(8,128)(2,1)S(1)} %slice.4.refs_0_, bf16[32,48,128]{2,1,0:T(8,128)(2,1)S(1)} %collective-permute-done.1.refs_1_, bf16[32,48,128]{2,1,0:T(8,128)(2,1)S(1)} %copy-done.4, ...), custom_call_target="tpu_custom_call" | custom-call | flops 2147483648 | bytes 1048576 | tf_op jit(solution)/shard_map/pallas_call | solution.py:29
  103.3 3.2 %collective-permute-start.6 = (bf16[896,256]{1,0:T(8,128)(2,1)S(1)}, bf16[896,256]{1,0:T(8,128)(2,1)S(1)}, u32[]{:S(2)}, u32[]{:S(2)}) collective-permute-start(bf16[896,256]{1,0:T(8,128)(2,1)S(1)} %shard_map.220.own), channel_id=1, source_target_pairs={{0,1},{1,0},{2,3},{3,2},{4,5},{5,4},{6,7},{7,6},{8,9},{9,8},{10,11... | collective-permute-start | bytes 1376264 | tf_op jit(solution)/shard_map/ppermute | solution.py:458
  106.5 1.4 collective-permute-done.6.far
  107.9 2.4 %shard_map.222 = (bf16[1024,128]{1,0:T(8,128)(2,1)S(1)}, bf16[1024,128]{1,0:T(8,128)(2,1)S(1)}, bf16[1024,128]{1,0:T(8,128)(2,1)S(1)}, bf16[1024,128]{1,0:T(8,128)(2,1)S(1)}) custom-call(bf16[896,256]{1,0:T(8,128)(2,1)S(1)} %shard_map.220.own, bf16[896,256]{1,0:T(8,128)(2,1)S(1)} %collective-permute-done.6.far, bf16[128,256]{1,0:T(8,128)(2,1)S(1)} %get-tuple-element.35.rows, ...), custom_call_target="tpu_custom_call" | custom-call | flops 2147483648 | bytes 1048576 | tf_op jit(solution)/shard_map/pallas_call | solution.py:29
  110.4 1.9 %collective-permute-start.10 = (bf16[1024,128]{1,0:T(8,128)(2,1)S(1)}, bf16[1024,128]{1,0:T(8,128)(2,1)S(1)}, u32[]{:S(2)}, u32[]{:S(2)}) collective-permute-start(bf16[1024,128]{1,0:T(8,128)(2,1)S(1)} %get-tuple-element.42), channel_id=1, source_target_pairs={{0,2},{2,4},{4,6},{6,8},{8,10},{10,12},{12,14},{14,0},{1,3},{3,5},... | collective-permute-start | bytes 786440 | tf_op jit(solution)/shard_map/ppermute | solution.py:458
  112.3 4.6 %collective-permute-start.11 = (bf16[1024,128]{1,0:T(8,128)(2,1)S(1)}, bf16[1024,128]{1,0:T(8,128)(2,1)S(1)}, u32[]{:S(2)}, u32[]{:S(2)}) collective-permute-start(bf16[1024,128]{1,0:T(8,128)(2,1)S(1)} %get-tuple-element.43), channel_id=1, source_target_pairs={{0,14},{2,0},{4,2},{6,4},{8,6},{10,8},{12,10},{14,12},{1,15},{3,1}... | collective-permute-start | bytes 786440 | tf_op jit(solution)/shard_map/ppermute | solution.py:458
  116.9 3.7 %collective-permute-start.12 = (bf16[1024,128]{1,0:T(8,128)(2,1)S(1)}, bf16[1024,128]{1,0:T(8,128)(2,1)S(1)}, u32[]{:S(2)}, u32[]{:S(2)}) collective-permute-start(bf16[1024,128]{1,0:T(8,128)(2,1)S(1)} %get-tuple-element.44), channel_id=1, source_target_pairs={{0,4},{1,13},{2,6},{3,15},{4,8},{5,1},{6,10},{7,3},{8,12},{9,5},{1... | collective-permute-start | bytes 786440 | tf_op jit(solution)/shard_map/ppermute | solution.py:458
  120.6 2.4 %shard_map.221 = (bf16[1024,128]{1,0:T(8,128)(2,1)S(1)}, bf16[1024,128]{1,0:T(8,128)(2,1)S(1)}, bf16[1024,128]{1,0:T(8,128)(2,1)S(1)}, bf16[1024,128]{1,0:T(8,128)(2,1)S(1)}) custom-call(bf16[896,256]{1,0:T(8,128)(2,1)S(1)} %shard_map.220.own, bf16[896,256]{1,0:T(8,128)(2,1)S(1)} %collective-permute-done.6.far, bf16[128,256]{1,0:T(8,128)(2,1)S(1)} %get-tuple-element.35.rows, ...), custom_call_target="tpu_custom_call" | custom-call | flops 2147483648 | bytes 1048576 | tf_op jit(solution)/shard_map/pallas_call | solution.py:29
  123.0 2.5 %collective-permute-start.8 = (bf16[1024,128]{1,0:T(8,128)(2,1)S(1)}, bf16[1024,128]{1,0:T(8,128)(2,1)S(1)}, u32[]{:S(2)}, u32[]{:S(2)}) collective-permute-start(bf16[1024,128]{1,0:T(8,128)(2,1)S(1)} %get-tuple-element.38), channel_id=1, source_target_pairs={{0,2},{2,4},{4,6},{6,8},{8,10},{10,12},{12,14},{14,0},{1,3},{3,5},... | collective-permute-start | bytes 786440 | tf_op jit(solution)/shard_map/ppermute | solution.py:458
  125.5 4.0 %collective-permute-start.9 = (bf16[1024,128]{1,0:T(8,128)(2,1)S(1)}, bf16[1024,128]{1,0:T(8,128)(2,1)S(1)}, u32[]{:S(2)}, u32[]{:S(2)}) collective-permute-start(bf16[1024,128]{1,0:T(8,128)(2,1)S(1)} %get-tuple-element.39), channel_id=1, source_target_pairs={{0,14},{2,0},{4,2},{6,4},{8,6},{10,8},{12,10},{14,12},{1,15},{3,1}... | collective-permute-start | bytes 786440 | tf_op jit(solution)/shard_map/ppermute | solution.py:458
  129.5 3.3 %collective-permute-done.12.refs_4_ = bf16[1024,128]{1,0:T(8,128)(2,1)S(1)} collective-permute-done((bf16[1024,128]{1,0:T(8,128)(2,1)S(1)}, bf16[1024,128]{1,0:T(8,128)(2,1)S(1)}, u32[]{:S(2)}, u32[]{:S(2)}) %collective-permute-start.12) | collective-permute-done | bytes 262176 | tf_op jit(solution)/shard_map/ppermute | solution.py:458
  133.1 2.3 %collective-permute-start.13 = (bf16[1024,128]{1,0:T(8,128)(2,1)S(1)}, bf16[1024,128]{1,0:T(8,128)(2,1)S(1)}, u32[]{:S(2)}, u32[]{:S(2)}) collective-permute-start(bf16[1024,128]{1,0:T(8,128)(2,1)S(1)} %get-tuple-element.45), channel_id=1, source_target_pairs={{0,4},{2,6},{4,8},{6,10},{8,12},{10,14},{12,0},{14,2},{1,5},{3,7},... | collective-permute-start | bytes 786440 | tf_op jit(solution)/shard_map/ppermute | solution.py:458
  135.5 5.1 %collective-permute-start.14 = (bf16[1024,128]{1,0:T(8,128)(2,1)S(1)}, bf16[1024,128]{1,0:T(8,128)(2,1)S(1)}, u32[]{:S(2)}, u32[]{:S(2)}) collective-permute-start(bf16[1024,128]{1,0:T(8,128)(2,1)S(1)} %get-tuple-element.46), channel_id=1, source_target_pairs={{0,12},{2,14},{4,0},{6,2},{8,4},{10,6},{12,8},{14,10},{1,13},{3,15... | collective-permute-start | bytes 786440 | tf_op jit(solution)/shard_map/ppermute | solution.py:458
  140.6 8.4 %collective-permute-done.13.up = bf16[1024,128]{1,0:T(8,128)(2,1)S(1)} collective-permute-done((bf16[1024,128]{1,0:T(8,128)(2,1)S(1)}, bf16[1024,128]{1,0:T(8,128)(2,1)S(1)}, u32[]{:S(2)}, u32[]{:S(2)}) %collective-permute-start.13) | collective-permute-done | bytes 262176 | tf_op jit(solution)/shard_map/ppermute | solution.py:458
  149.0 2.1 %collective-permute-done.14.down = bf16[1024,128]{1,0:T(8,128)(2,1)S(1)} collective-permute-done((bf16[1024,128]{1,0:T(8,128)(2,1)S(1)}, bf16[1024,128]{1,0:T(8,128)(2,1)S(1)}, u32[]{:S(2)}, u32[]{:S(2)}) %collective-permute-start.14) | collective-permute-done | bytes 262176 | tf_op jit(solution)/shard_map/ppermute | solution.py:458
  151.8 13.5 %all_to_all.16.got = bf16[32,24,128]{2,1,0:T(8,128)(2,1)S(1)} all-to-all(bf16[32,24,128]{2,1,0:T(8,128)(2,1)S(1)} %bitcast.15), channel_id=1, replica_groups=mesh['ep_0'=8,'ep_1'=4,'tp_0'=8,'tp_1'=2] {'ep_0','ep_1'}, dimensions={0} | all-to-all | bytes 393216 | tf_op jit(solution)/shard_map/all_to_all | solution.py:474
  (50 shorter events, 12.6 us)
Async XLA Ops:
  2.0 16.2 %collective-permute-start = (bf16[8,512]{1,0:T(8,128)(2,1)}, bf16[8,512]{1,0:T(8,128)(2,1)S(1)}, u32[]{:S(2)}, u32[]{:S(2)}) collective-permute-start(bf16[8,512]{1,0:T(8,128)(2,1)} %shard_map.213), channel_id=1, source_target_pairs={{0,16},{16,32},{32,48},{48,64},{64,80},{80,96},{96,112},{112,128},... | collective-permute-start | bytes 24584 | tf_op jit(solution)/shard_map/ppermute | solution.py:458
  9.5 64.5 %collective-permute-start.4 = (bf16[3072,256]{1,0:T(8,128)(2,1)}, bf16[3072,256]{1,0:T(8,128)(2,1)S(1)}, u32[]{:S(2)}, u32[]{:S(2)}) collective-permute-start(bf16[3072,256]{1,0:T(8,128)(2,1)} %get-tuple-element.28), channel_id=1, source_target_pairs={{0,1},{1,0},{2,3},{3,2},{4,5},{5,4},{6,7},{7,6},{8,9},{9,8},{10,11... | collective-permute-start | bytes 4718600 | tf_op jit(solution)/shard_map/ppermute | solution.py:458
  18.2 0.6 copy-start.14
  48.4 29.8 %copy-start.2 = (bf16[256,2048]{1,0:T(8,128)(2,1)S(1)}, bf16[256,2048]{1,0:T(8,128)(2,1)}, u32[]{:S(2)}) copy-start(bf16[256,2048]{1,0:T(8,128)(2,1)} %result.3) | copy-start | bytes 3145732
  48.4 32.3 %copy-start.15 = (bf16[256]{0:T(256)(128)(2,1)S(1)}, bf16[256]{0:T(256)(128)(2,1)}, u32[]{:S(2)}) copy-start(bf16[256]{0:T(256)(128)(2,1)} %param.33) | copy-start | bytes 1540
  48.4 12.7 %collective-permute-start.1 = (bf16[32,48,128]{2,1,0:T(8,128)(2,1)S(1)}, bf16[32,48,128]{2,1,0:T(8,128)(2,1)S(1)}, u32[]{:S(2)}, u32[]{:S(2)}) collective-permute-start(bf16[32,48,128]{2,1,0:T(8,128)(2,1)S(1)} %slice.4.refs_0_), channel_id=1, source_target_pairs={{0,2},{2,4},{4,6},{6,8},{8,10},{10,12},{12,14},{14,0},{1,3},{3,5},... | collective-permute-start | bytes 1179656 | tf_op jit(solution)/shard_map/ppermute | solution.py:458
  51.7 10.6 %collective-permute-start.2 = (bf16[32,48,128]{2,1,0:T(8,128)(2,1)S(1)}, bf16[32,48,128]{2,1,0:T(8,128)(2,1)S(1)}, u32[]{:S(2)}, u32[]{:S(2)}) collective-permute-start(bf16[32,48,128]{2,1,0:T(8,128)(2,1)S(1)} %slice.4.refs_0_), channel_id=1, source_target_pairs={{0,14},{2,0},{4,2},{6,4},{8,6},{10,8},{12,10},{14,12},{1,15},{3,1}... | collective-permute-start | bytes 1179656 | tf_op jit(solution)/shard_map/ppermute | solution.py:458
  55.6 18.4 %collective-permute-start.3 = (bf16[32,48,128]{2,1,0:T(8,128)(2,1)S(1)}, bf16[32,48,128]{2,1,0:T(8,128)(2,1)S(1)}, u32[]{:S(2)}, u32[]{:S(2)}) collective-permute-start(bf16[32,48,128]{2,1,0:T(8,128)(2,1)S(1)} %slice.4.refs_0_), channel_id=1, source_target_pairs={{0,4},{1,13},{2,6},{3,15},{4,8},{5,1},{6,10},{7,3},{8,12},{9,5},{1... | collective-permute-start | bytes 1179656 | tf_op jit(solution)/shard_map/ppermute | solution.py:458
  62.4 13.9 %copy-start.3 = (bf16[32,48,128]{2,1,0:T(8,128)(2,1)}, bf16[32,48,128]{2,1,0:T(8,128)(2,1)S(1)}, u32[]{:S(2)}) copy-start(bf16[32,48,128]{2,1,0:T(8,128)(2,1)S(1)} %collective-permute-done.2.refs_2_) | copy-start | bytes 1179652
  73.9 2.4 %copy-start.5 = (bf16[32,48,128]{2,1,0:T(8,128)(2,1)}, bf16[32,48,128]{2,1,0:T(8,128)(2,1)S(1)}, u32[]{:S(2)}) copy-start(bf16[32,48,128]{2,1,0:T(8,128)(2,1)S(1)} %collective-permute-done.3.refs_3_) | copy-start | bytes 1179652
  76.3 22.9 %collective-permute-start.5 = (bf16[768,512]{1,0:T(8,128)(2,1)}, bf16[768,512]{1,0:T(8,128)(2,1)}, u32[]{:S(2)}, u32[]{:S(2)}) collective-permute-start(bf16[768,512]{1,0:T(8,128)(2,1)} %shard_map.216), channel_id=1, source_target_pairs={{0,1},{1,0},{2,3},{3,2},{4,5},{5,4},{6,7},{7,6},{8,9},{9,8},{10,11... | collective-permute-start | bytes 2359304 | tf_op jit(solution)/shard_map/ppermute | solution.py:458
  78.2 28.3 %collective-permute-start.7 = (bf16[256,2048]{1,0:T(8,128)(2,1)S(1)}, bf16[256,2048]{1,0:T(8,128)(2,1)}, u32[]{:S(2)}, u32[]{:S(2)}) collective-permute-start(bf16[256,2048]{1,0:T(8,128)(2,1)S(1)} %copy-done.2), channel_id=1, source_target_pairs={{0,1},{1,0},{2,3},{3,2},{4,5},{5,4},{6,7},{7,6},{8,9},{9,8},{10,11... | collective-permute-start | bytes 3145736 | tf_op jit(solution)/shard_map/ppermute | solution.py:458
  82.0 14.0 %all-to-all-start.1 = ((bf16[32,8,128]{2,1,0:T(8,128)(2,1)}), bf16[32,8,128]{2,1,0:T(8,128)(2,1)S(1)}, u32[]{:S(2)}, u32[]{:S(2)}) async-start(bf16[32,8,128]{2,1,0:T(8,128)(2,1)} %shard_map.218), calls=%async_computation.1 | async-start | bytes 131072 | tf_op jit(solution)/shard_map/all_to_all | solution.py:474
  87.0 9.0 %copy-start.11 = (bf16[256,128]{1,0:T(8,128)(2,1)S(1)}, bf16[256,128]{1,0:T(8,128)(2,1)}, u32[]{:S(2)}) copy-start(bf16[256,128]{1,0:T(8,128)(2,1)} %get-tuple-element.31.c.refs_1_) | copy-start | bytes 196612
  96.0 0.9 copy-start.7
  96.9 0.9 copy-start.10
  97.8 0.9 copy-start.12
  98.8 1.2 copy-start
  98.8 1.5 copy-start.1
  98.8 1.6 copy-start.4
  98.8 1.7 %copy-start.6 = (bf16[32,48,128]{2,1,0:T(8,128)(2,1)S(1)}, bf16[32,48,128]{2,1,0:T(8,128)(2,1)}, u32[]{:S(2)}) copy-start(bf16[32,48,128]{2,1,0:T(8,128)(2,1)} %copy-done.5) | copy-start | bytes 1179652
  100.5 7.4 %copy-start.9 = (bf16[1024,256]{1,0:T(8,128)(2,1)S(1)}, bf16[1024,256]{1,0:T(8,128)(2,1)}, u32[]{:S(2)}) copy-start(bf16[1024,256]{1,0:T(8,128)(2,1)} %get-tuple-element.36.keep) | copy-start | bytes 1572868
  103.3 4.6 %collective-permute-start.6 = (bf16[896,256]{1,0:T(8,128)(2,1)S(1)}, bf16[896,256]{1,0:T(8,128)(2,1)S(1)}, u32[]{:S(2)}, u32[]{:S(2)}) collective-permute-start(bf16[896,256]{1,0:T(8,128)(2,1)S(1)} %shard_map.220.own), channel_id=1, source_target_pairs={{0,1},{1,0},{2,3},{3,2},{4,5},{5,4},{6,7},{7,6},{8,9},{9,8},{10,11... | collective-permute-start | bytes 1376264 | tf_op jit(solution)/shard_map/ppermute | solution.py:458
  110.4 19.2 %collective-permute-start.10 = (bf16[1024,128]{1,0:T(8,128)(2,1)S(1)}, bf16[1024,128]{1,0:T(8,128)(2,1)S(1)}, u32[]{:S(2)}, u32[]{:S(2)}) collective-permute-start(bf16[1024,128]{1,0:T(8,128)(2,1)S(1)} %get-tuple-element.42), channel_id=1, source_target_pairs={{0,2},{2,4},{4,6},{6,8},{8,10},{10,12},{12,14},{14,0},{1,3},{3,5},... | collective-permute-start | bytes 786440 | tf_op jit(solution)/shard_map/ppermute | solution.py:458
  112.3 17.3 %collective-permute-start.11 = (bf16[1024,128]{1,0:T(8,128)(2,1)S(1)}, bf16[1024,128]{1,0:T(8,128)(2,1)S(1)}, u32[]{:S(2)}, u32[]{:S(2)}) collective-permute-start(bf16[1024,128]{1,0:T(8,128)(2,1)S(1)} %get-tuple-element.43), channel_id=1, source_target_pairs={{0,14},{2,0},{4,2},{6,4},{8,6},{10,8},{12,10},{14,12},{1,15},{3,1}... | collective-permute-start | bytes 786440 | tf_op jit(solution)/shard_map/ppermute | solution.py:458
  116.9 16.0 %collective-permute-start.12 = (bf16[1024,128]{1,0:T(8,128)(2,1)S(1)}, bf16[1024,128]{1,0:T(8,128)(2,1)S(1)}, u32[]{:S(2)}, u32[]{:S(2)}) collective-permute-start(bf16[1024,128]{1,0:T(8,128)(2,1)S(1)} %get-tuple-element.44), channel_id=1, source_target_pairs={{0,4},{1,13},{2,6},{3,15},{4,8},{5,1},{6,10},{7,3},{8,12},{9,5},{1... | collective-permute-start | bytes 786440 | tf_op jit(solution)/shard_map/ppermute | solution.py:458
  123.0 17.5 %collective-permute-start.8 = (bf16[1024,128]{1,0:T(8,128)(2,1)S(1)}, bf16[1024,128]{1,0:T(8,128)(2,1)S(1)}, u32[]{:S(2)}, u32[]{:S(2)}) collective-permute-start(bf16[1024,128]{1,0:T(8,128)(2,1)S(1)} %get-tuple-element.38), channel_id=1, source_target_pairs={{0,2},{2,4},{4,6},{6,8},{8,10},{10,12},{12,14},{14,0},{1,3},{3,5},... | collective-permute-start | bytes 786440 | tf_op jit(solution)/shard_map/ppermute | solution.py:458
  125.5 15.1 %collective-permute-start.9 = (bf16[1024,128]{1,0:T(8,128)(2,1)S(1)}, bf16[1024,128]{1,0:T(8,128)(2,1)S(1)}, u32[]{:S(2)}, u32[]{:S(2)}) collective-permute-start(bf16[1024,128]{1,0:T(8,128)(2,1)S(1)} %get-tuple-element.39), channel_id=1, source_target_pairs={{0,14},{2,0},{4,2},{6,4},{8,6},{10,8},{12,10},{14,12},{1,15},{3,1}... | collective-permute-start | bytes 786440 | tf_op jit(solution)/shard_map/ppermute | solution.py:458
  133.1 32.1 %copy-start.8 = (f32[256,2]{0,1:T(2,128)S(1)}, f32[256,2]{0,1:T(2,128)}, u32[]{:S(2)}) copy-start(f32[256,2]{0,1:T(2,128)} %param.41) | copy-start | bytes 6148
  133.1 32.1 %copy-start.13 = (s32[2,256]{1,0:T(2,128)S(1)}, s32[2,256]{1,0:T(2,128)}, u32[]{:S(2)}) copy-start(s32[2,256]{1,0:T(2,128)} %get-tuple-element.49.slots) | copy-start | bytes 6148
  133.1 15.9 %collective-permute-start.13 = (bf16[1024,128]{1,0:T(8,128)(2,1)S(1)}, bf16[1024,128]{1,0:T(8,128)(2,1)S(1)}, u32[]{:S(2)}, u32[]{:S(2)}) collective-permute-start(bf16[1024,128]{1,0:T(8,128)(2,1)S(1)} %get-tuple-element.45), channel_id=1, source_target_pairs={{0,4},{2,6},{4,8},{6,10},{8,12},{10,14},{12,0},{14,2},{1,5},{3,7},... | collective-permute-start | bytes 786440 | tf_op jit(solution)/shard_map/ppermute | solution.py:458
  135.5 15.6 %collective-permute-start.14 = (bf16[1024,128]{1,0:T(8,128)(2,1)S(1)}, bf16[1024,128]{1,0:T(8,128)(2,1)S(1)}, u32[]{:S(2)}, u32[]{:S(2)}) collective-permute-start(bf16[1024,128]{1,0:T(8,128)(2,1)S(1)} %get-tuple-element.46), channel_id=1, source_target_pairs={{0,12},{2,14},{4,0},{6,2},{8,4},{10,6},{12,8},{14,10},{1,13},{3,15... | collective-permute-start | bytes 786440 | tf_op jit(solution)/shard_map/ppermute | solution.py:458

commit v5 on v4

--- a/solution.py
+++ b/solution.py
@@ -25,11 +25,13 @@
 SMEM = pl.BlockSpec(memory_space=pltpu.SMEM)
 
 
-def call(body, outs, ins, flops, room, scratch=(), smem=0):
+def call(body, outs, ins, flops, room, scratch=(), smem=0, still=0):
     return pl.pallas_call(
         body,
         out_shape=outs,
-        in_specs=[SMEM] * smem + [VMEM] * (len(ins) - smem),
+        in_specs=[SMEM] * smem
+        + [pl.BlockSpec(memory_space=pl.ANY)] * still
+        + [VMEM] * (len(ins) - smem - still),
         out_specs=jax.tree.map(lambda _: VMEM, outs),
         scratch_shapes=scratch,
         cost_estimate=pl.CostEstimate(flops=flops, bytes_accessed=1 << 20, transcendentals=0),
@@ -70,7 +72,32 @@
     return wide
 
 
-def route_body(experts, place, tokens, token_gain, picks, routed, slots_out):
+def route_body(
+    experts,
+    place,
+    offset,
+    speed,
+    tokens,
+    token_gain,
+    picks,
+    x_in,
+    b_in,
+    c_in,
+    x_taps,
+    b_taps,
+    c_taps,
+    strides,
+    extra,
+    routed,
+    slots_out,
+    x_out,
+    b_out,
+    c_out,
+    heads_out,
+    columns_out,
+    rows_out,
+    joined,
+):
     lanes = 128
     total_rows, token_count = routed.shape[0], tokens.shape[0]
     capacity = total_rows // experts
@@ -99,53 +126,16 @@
         placing = hit if placing is None else placing | hit
     routed[...] = dot(placing.astype(F32).astype(BF16), chosen).astype(BF16)
 
-
-def filter_body(
-    offset,
-    speed,
-    routed,
-    x_in,
-    b_in,
-    c_in,
-    rim,
-    x_taps,
-    b_taps,
-    c_taps,
-    strides,
-    extra,
-    send,
-    x_out,
-    b_out,
-    c_out,
-    columns_out,
-    rows_out,
-    joined,
-):
     count, width = x_in.shape
     state = b_in.shape[1]
-    experts, rows, lanes = send.shape
-    capacity = (rows - 2 * PIECE) // 2
-
-    joined[0:RIM, :] = rim[...].astype(F32)
+    joined[0:RIM, :] = jnp.zeros((RIM, width + 2 * state), F32)
     joined[RIM:, 0:width] = x_in[...].astype(F32)
     joined[RIM:, width : width + state] = b_in[...].astype(F32)
     joined[RIM:, width + state :] = c_in[...].astype(F32)
-
-    def filtered(first, size, taps_ref):
-        taps = taps_ref[...].astype(F32)
-        total = None
-        for j in range(taps.shape[0]):
-            start = RIM - taps.shape[0] + 1 + j
-            term = taps[j : j + 1] * joined[start : start + count, first : first + size]
-            total = term if total is None else total + term
-        return silu(total)
-
-    x = filtered(0, width, x_taps)
-    b = filtered(width, state, b_taps).astype(BF16)
-    c = filtered(width + state, state, c_taps).astype(BF16)
-    x_out[...] = x
-    b_out[...] = b
-    c_out[...] = c
+    heads_out[...] = joined[RIM : 2 * RIM, :]
+    x_out[...] = filtered(joined, count, 0, width, x_taps)
+    b_out[...] = filtered(joined, count, width, state, b_taps).astype(BF16)
+    c_out[...] = filtered(joined, count, width + state, state, c_taps).astype(BF16)
 
     def per_head(values):
         head = iota(strides.shape, 0)
@@ -164,14 +154,56 @@
         moved = jnp.where((lane >= shift), pltpu.roll(both, shift, axis=1), 0.0)
         both = jnp.where(iota(both.shape, 0) < 4, both + moved, both)
         shift *= 2
-    columns = both.T
+    columns_out[...] = both.T
     rows_out[...] = both
-    columns_out[...] = columns
+
+
+def filtered(joined, count, first, size, taps_ref):
+    taps = taps_ref[...].astype(F32)
+    total = None
+    for j in range(taps.shape[0]):
+        start = RIM - taps.shape[0] + 1 + j
+        term = taps[j : j + 1] * joined[start : start + count, first : first + size]
+        total = term if total is None else total + term
+    return silu(total)
+
+
+def filter_body(
+    routed,
+    x_in,
+    b_in,
+    c_in,
+    heads,
+    rim,
+    x_taps,
+    b_taps,
+    c_taps,
+    columns_in,
+    send,
+    x_out,
+    b_out,
+    c_out,
+    joined,
+):
+    count, width = x_in.shape
+    state = b_in.shape[1]
+    experts, rows, lanes = send.shape
+    capacity = (rows - 2 * PIECE) // 2
+    joined[0:RIM, :] = rim[...].astype(F32)
+    joined[RIM:, :] = heads[...]
+    for source, target, first, size, taps in (
+        (x_in, x_out, 0, width, x_taps),
+        (b_in, b_out, width, state, b_taps),
+        (c_in, c_out, width + state, state, c_taps),
+    ):
+        target[RIM:, :] = source[RIM:, :]
+        target[0:RIM, :] = filtered(joined, RIM, first, size, taps).astype(target.dtype)
+    columns = columns_in[...]
     running, step_column = columns[:, 0:4], columns[:, 4:8]
     last = columns[count - 1 : count, 0:4]
     weight = step_column * jnp.exp(last - running)
-    weighted = (x * spread(weight, HEAD_DIM)).astype(BF16)
-    end_state = dot(weighted, b, (0, 0)).astype(BF16)
+    weighted = (x_out[...] * spread(weight, HEAD_DIM)).astype(BF16)
+    end_state = dot(weighted, b_out[...], (0, 0)).astype(BF16)
     high = last.astype(BF16).astype(F32)
     low = last - high
     half = iota((PIECE, lanes), 1) < lanes // 2
@@ -321,7 +353,14 @@
             ]
 
 
-def down_body(start, own, far, rows, keep, weights, result, result_far, *outs):
+def project_body(rows, result, out):
+    wide = 512
+    for column in range(0, result.shape[1], wide):
+        columns = slice(column, column + wide)
+        out[:, columns] = dot(rows[...], result[:, columns])
+
+
+def down_body(start, own, far, rows, keep, weights, result_far, *outs):
     depth = own.shape[1]
     each = rows.shape[0] // len(HOMES)
     total = own.shape[0] - rows.shape[0]
@@ -342,11 +381,11 @@
 
     lax.fori_loop(0, total // block, step, 0)
     first, last = start * each, (start + len(outs)) * each
-    near, beyond = rows[first:last, :], far[total + first : total + last, :]
+    beyond = far[total + first : total + last, :]
     wide = 512
-    for column in range(0, result.shape[1], wide):
+    for column in range(0, rows.shape[1], wide):
         columns = slice(column, column + wide)
-        product = dot(near, result[:, columns]) + dot(beyond, result_far[:, columns])
+        product = rows[first:last, columns] + dot(beyond, result_far[:, columns])
         product = product.astype(BF16)
         for k, out in enumerate(outs):
             for j in range(wide // 128):
@@ -475,47 +514,48 @@
 
     rim = last_rows(blender_incoming_features, entry_latent_matrix, exit_latent_matrix)
     rim = permuted(rim, EP, [(i, i + 1) for i in range(ep_count - 1)])
-    routed, slots = call(
+    taps = (incoming_feature_kernel, entry_latent_kernel, exit_latent_kernel)
+    filtered_shapes = (
+        shaped(count, width, dtype=F32),
+        shaped(count, state),
+        shaped(count, state),
+    )
+    routed, slots, x, b, c, heads, columns, rows = call(
         functools.partial(route_body, ep_count),
-        (shaped(total_rows, 2 * lanes), shaped(TOPK, token_count, dtype=jnp.int32)),
         (
-            (core * (chips // 2) + chip % (chips // 2)).reshape(1),
-            latter_microbatch_activations,
-            specialist_rescale_coefs,
-            specialist_picks.T,
-        ),
-        1 << 30,
-        None,
-        smem=1,
-    )
-    send, x, b, c, columns, rows = call(
-        filter_body,
-        (
-            shaped(ep_count, 2 * capacity + 2 * PIECE, lanes),
-            shaped(count, width, dtype=F32),
-            shaped(count, state),
-            shaped(count, state),
+            shaped(total_rows, 2 * lanes),
+            shaped(TOPK, token_count, dtype=jnp.int32),
+            *filtered_shapes,
+            shaped(RIM, width + 2 * state, dtype=F32),
             shaped(count, 8, dtype=F32),
             shaped(8, count, dtype=F32),
         ),
         (
+            (core * (chips // 2) + chip % (chips // 2)).reshape(1),
             stride_offset_vector,
             attenuation_speed_exponent,
-            routed,
+            latter_microbatch_activations,
+            specialist_rescale_coefs,
+            specialist_picks.T,
             blender_incoming_features,
             entry_latent_matrix,
             exit_latent_matrix,
-            rim,
-            incoming_feature_kernel,
-            entry_latent_kernel,
-            exit_latent_kernel,
+            *taps,
             presoftplus_strides.T,
             extra_attenuation.T,
         ),
         1 << 30,
         None,
         scratch=(pltpu.VMEM((RIM + count, width + 2 * state), F32),),
-        smem=2,
+        smem=3,
+    )
+    send, x, b, c = call(
+        filter_body,
+        (shaped(ep_count, 2 * capacity + 2 * PIECE, lanes), *filtered_shapes),
+        (routed, x, b, c, heads, rim, *taps, columns),
+        1 << 30,
+        None,
+        scratch=(pltpu.VMEM((2 * RIM, width + 2 * state), F32),),
     )
     got = exchanged(send, EP)
     y = inside(bypass_coef_vector, x, b, c, columns, rows)
@@ -577,12 +617,19 @@
     ours_far = partner(ours)
     row_block = count * model_width // (2 * chips * lanes)
     all_rows = total_rows + row_block
+    projected = call(
+        project_body,
+        shaped(row_count, model_width, dtype=F32),
+        (mine_rows, blender_result_matrix),
+        1 << 29,
+        6,
+    )
 
     def partials(start):
         return call(
             functools.partial(down_body, start),
             (shaped(all_rows, lanes),) * 4,
-            (ours, ours_far, mine_rows, keep, weights_far, blender_result_matrix, result_far),
+            (ours, ours_far, projected, keep, weights_far, result_far),
             1 << 31,
             12,
         )

time: 168 us -> 168 us (level)
    pallas_call x13 -> x14, Pallas kernels: 25.9 us -> 25.7 us  [call(): pl.pallas_call(body, out_shape=outs, in_specs=[SMEM] * smem + [pl.BlockSp...]
where the time goes in v5:
time: 168 us; the launch traced here: 166 us
  starting transfers between devices  58.1 us (35%)
  blocking collectives  39.5 us (24%)
  waiting for transfers between devices  35.5 us (21%)
  Pallas kernels  27.1 us (16%)
  local copies, waits for them, and re-layouts  4.77 us (3%)
    ppermute x15, starting transfers between devices, permuted(): return lax.ppermute(x, axis, pairs)  53.1 us
    all_to_all x2, blocking collectives, exchanged(): return lax.all_to_all(x, axis, 0, 0, tiled=True)  39.5 us
    ppermute x15, waiting for transfers between devices, permuted(): return lax.ppermute(x, axis, pairs)  29.1 us
    pallas_call x14, Pallas kernels, call(): pl.pallas_call(body, out_shape=outs, in_specs=[SMEM] * smem + [pl.BlockSp...  25.7 us
    all_to_all x1, waiting for transfers between devices, exchanged(): return lax.all_to_all(x, axis, 0, 0, tiled=True)  6.37 us
    all_to_all x1, starting transfers between devices, exchanged(): return lax.all_to_all(x, axis, 0, 0, tiled=True)  5.04 us
    unnamed x32, local copies, waits for them, and re-layouts  4.73 us
  transfers between devices with their start and end apart: 16, of which 8 were waited for; matrix products, arithmetic and copies ran while one was open for 0% of the time, Pallas kernels for 12%

profile of v5, /device:TPU:1, one launch (start us, length us, event | category | flops | bytes accessed | tf_op | source)
XLA Modules:
  0.0 166.0 jit_solution(15435800366996614347)
XLA Ops:
  2.0 3.9 %collective-permute-start = (bf16[8,512]{1,0:T(8,128)(2,1)}, bf16[8,512]{1,0:T(8,128)(2,1)S(1)}, u32[]{:S(2)}, u32[]{:S(2)}) collective-permute-start(bf16[8,512]{1,0:T(8,128)(2,1)} %shard_map.213), channel_id=1, source_target_pairs={{0,16},{16,32},{32,48},{48,64},{64,80},{80,96},{96,112},{112,128},... | collective-permute-start | bytes 24584 | tf_op jit(solution)/shard_map/ppermute | solution.py:497
  5.9 3.5 %shard_map.215 = (bf16[1024,256]{1,0:T(8,128)(2,1)}, bf16[3072,256]{1,0:T(8,128)(2,1)}) custom-call(s32[1]{0:T(128)} %bitcast.core, s32[1]{0:T(128)} %bitcast.1.chip, bf16[2048,256]{1,0:T(8,128)(2,1)} %bitcast.17, bf16[2048,256]{1,0:T(8,128)(2,1)} %bitcast.19, bf16[256,2048]{1,0:T(8,128)(2,1)} %bitcast.22), custom_call_target="tpu_custom_call" | custom-call | flops 1073741824 | bytes 1048576 | tf_op jit(solution)/shard_map/pallas_call | solution.py:29
  9.5 6.1 %collective-permute-start.4 = (bf16[3072,256]{1,0:T(8,128)(2,1)}, bf16[3072,256]{1,0:T(8,128)(2,1)S(1)}, u32[]{:S(2)}, u32[]{:S(2)}) collective-permute-start(bf16[3072,256]{1,0:T(8,128)(2,1)} %get-tuple-element.37), channel_id=1, source_target_pairs={{0,1},{1,0},{2,3},{3,2},{4,5},{5,4},{6,7},{7,6},{8,9},{9,8},{10,11... | collective-permute-start | bytes 4718600 | tf_op jit(solution)/shard_map/ppermute | solution.py:497
  15.6 3.4 %shard_map.212 = (bf16[768,256]{1,0:T(8,128)(2,1)}, s32[2,256]{1,0:T(2,128)}, f32[256,256]{1,0:T(8,128)}, bf16[256,128]{1,0:T(8,128)(2,1)}, bf16[256,128]{1,0:T(...) custom-call(s32[1]{0:T(128)} %bitcast.2.place, f32[4]{0:T(128)} %offset.1, f32[4]{0:T(128)} %speed.1, ...), custom_call_target="tpu_custom_call" | custom-call | flops 1073741824 | bytes 1048576 | tf_op jit(solution)/shard_map/pallas_call | solution.py:29
  19.6 2.6 %shard_map.214 = (bf16[32,64,128]{2,1,0:T(8,128)(2,1)}, f32[256,256]{1,0:T(8,128)}, bf16[256,128]{1,0:T(8,128)(2,1)}, bf16[256,128]{1,0:T(8,128)(2,1)}) custom-call(bf16[768,256]{1,0:T(8,128)(2,1)} %get-tuple-element.30.routed, f32[256,256]{1,0:T(8,128)} %get-tuple-element.31.x_in, bf16[256,128]{1,0:T(8,128)(2,1)} %get-tuple-element.32.b_in, ...), custom_call_target="tpu_custom_call" | custom-call | flops 1073741824 | bytes 1048576 | tf_op jit(solution)/shard_map/pallas_call | solution.py:29
  22.2 26.1 %all_to_all.15.got = bf16[32,64,128]{2,1,0:T(8,128)(2,1)S(1)} all-to-all(bf16[32,64,128]{2,1,0:T(8,128)(2,1)} %get-tuple-element.36), channel_id=1, replica_groups=mesh['ep_0'=8,'ep_1'=4,'tp_0'=8,'tp_1'=2] {'ep_0','ep_1'}, dimensions={0} | all-to-all | bytes 1048576 | tf_op jit(solution)/shard_map/all_to_all | solution.py:513
  48.3 3.3 %collective-permute-start.1 = (bf16[32,48,128]{2,1,0:T(8,128)(2,1)S(1)}, bf16[32,48,128]{2,1,0:T(8,128)(2,1)S(1)}, u32[]{:S(2)}, u32[]{:S(2)}) collective-permute-start(bf16[32,48,128]{2,1,0:T(8,128)(2,1)S(1)} %slice.4.refs_0_), channel_id=1, source_target_pairs={{0,2},{2,4},{4,6},{6,8},{8,10},{10,12},{12,14},{14,0},{1,3},{3,5},... | collective-permute-start | bytes 1179656 | tf_op jit(solution)/shard_map/ppermute | solution.py:497
  51.6 3.8 %collective-permute-start.2 = (bf16[32,48,128]{2,1,0:T(8,128)(2,1)S(1)}, bf16[32,48,128]{2,1,0:T(8,128)(2,1)S(1)}, u32[]{:S(2)}, u32[]{:S(2)}) collective-permute-start(bf16[32,48,128]{2,1,0:T(8,128)(2,1)S(1)} %slice.4.refs_0_), channel_id=1, source_target_pairs={{0,14},{2,0},{4,2},{6,4},{8,6},{10,8},{12,10},{14,12},{1,15},{3,1}... | collective-permute-start | bytes 1179656 | tf_op jit(solution)/shard_map/ppermute | solution.py:497
  55.5 4.1 %collective-permute-start.3 = (bf16[32,48,128]{2,1,0:T(8,128)(2,1)S(1)}, bf16[32,48,128]{2,1,0:T(8,128)(2,1)S(1)}, u32[]{:S(2)}, u32[]{:S(2)}) collective-permute-start(bf16[32,48,128]{2,1,0:T(8,128)(2,1)S(1)} %slice.4.refs_0_), channel_id=1, source_target_pairs={{0,4},{1,13},{2,6},{3,15},{4,8},{5,1},{6,10},{7,3},{8,12},{9,5},{1... | collective-permute-start | bytes 1179656 | tf_op jit(solution)/shard_map/ppermute | solution.py:497
  59.6 1.4 collective-permute-done.1.refs_1_
  62.3 11.5 %collective-permute-done.3.refs_3_ = bf16[32,48,128]{2,1,0:T(8,128)(2,1)S(1)} collective-permute-done((bf16[32,48,128]{2,1,0:T(8,128)(2,1)S(1)}, bf16[32,48,128]{2,1,0:T(8,128)(2,1)S(1)}, u32[]{:S(2)}, u32[]{:S(2)}) %collective-permute-start.3) | collective-permute-done | bytes 393248 | tf_op jit(solution)/shard_map/ppermute | solution.py:497
  73.8 2.4 %shard_map.216 = bf16[768,512]{1,0:T(8,128)(2,1)} custom-call(s32[1]{0:T(128)} %bitcast.core, s32[1]{0:T(128)} %bitcast.1.chip, bf16[32,48,128]{2,1,0:T(8,128)(2,1)S(1)} %slice.4.refs_0_, bf16[32,48,128]{2,1,0:T(8,128)(2,1)S(1)} %collective-permute-done.1.refs_1_, bf16[32,48,128]{2,1,0:T(8,128)(2,1)S(1)} %collective-permute-done.2.refs_2_, ...), custom_call_target="tpu_custom_call" | custom-call | flops 2147483648 | bytes 1048576 | tf_op jit(solution)/shard_map/pallas_call | solution.py:29
  76.2 1.9 %collective-permute-start.5 = (bf16[768,512]{1,0:T(8,128)(2,1)}, bf16[768,512]{1,0:T(8,128)(2,1)}, u32[]{:S(2)}, u32[]{:S(2)}) collective-permute-start(bf16[768,512]{1,0:T(8,128)(2,1)} %shard_map.216), channel_id=1, source_target_pairs={{0,1},{1,0},{2,3},{3,2},{4,5},{5,4},{6,7},{7,6},{8,9},{9,8},{10,11... | collective-permute-start | bytes 2359304 | tf_op jit(solution)/shard_map/ppermute | solution.py:497
  78.1 2.4 %collective-permute-start.7 = (bf16[256,2048]{1,0:T(8,128)(2,1)S(1)}, bf16[256,2048]{1,0:T(8,128)(2,1)}, u32[]{:S(2)}, u32[]{:S(2)}) collective-permute-start(bf16[256,2048]{1,0:T(8,128)(2,1)S(1)} %copy-done), channel_id=1, source_target_pairs={{0,1},{1,0},{2,3},{3,2},{4,5},{5,4},{6,7},{7,6},{8,9},{9,8},{10,11... | collective-permute-start | bytes 3145736 | tf_op jit(solution)/shard_map/ppermute | solution.py:497
  81.9 5.0 %all-to-all-start.1 = ((bf16[32,8,128]{2,1,0:T(8,128)(2,1)}), bf16[32,8,128]{2,1,0:T(8,128)(2,1)S(1)}, u32[]{:S(2)}, u32[]{:S(2)}) async-start(bf16[32,8,128]{2,1,0:T(8,128)(2,1)} %shard_map.218), calls=%async_computation.1 | async-start | bytes 131072 | tf_op jit(solution)/shard_map/all_to_all | solution.py:513
  86.9 2.6 %shard_map.217.refs_0_ = f32[256,256]{1,0:T(8,128)} custom-call(f32[4]{0:T(128)} %bypass.1, f32[256,256]{1,0:T(8,128)} %get-tuple-element.38.x, bf16[256,128]{1,0:T(8,128)(2,1)} %get-tuple-element.39.b, bf16[256,128]{1,0:T(8,128)(2,1)} %get-tuple-element.40.c.refs_1_, f32[256,8]{1,0:T(8,128)} %get-tuple-element.35.columns_in.columns.refs_2_, ...), custom_call_target="tpu_custom_call" | custom-call | flops 2147483648 | bytes 1048576 | tf_op jit(solution)/shard_map/pallas_call | solution.py:29
  89.5 6.4 %all-to-all-done.1 = bf16[32,8,128]{2,1,0:T(8,128)(2,1)S(1)} async-done(((bf16[32,8,128]{2,1,0:T(8,128)(2,1)}), bf16[32,8,128]{2,1,0:T(8,128)(2,1)S(1)}, u32[]{:S(2)}, u32[]{:S(2)}) %all-to-all-start.1) | async-done | bytes 65568 | tf_op jit(solution)/shard_map/all_to_all | solution.py:513
  100.4 2.7 %shard_map.220.own = bf16[896,256]{1,0:T(8,128)(2,1)S(1)} custom-call(s32[1]{0:T(128)} %bitcast.core, s32[1]{0:T(128)} %bitcast.1.chip, bf16[32,48,128]{2,1,0:T(8,128)(2,1)S(1)} %slice.4.refs_0_, bf16[32,48,128]{2,1,0:T(8,128)(2,1)S(1)} %collective-permute-done.1.refs_1_, bf16[32,48,128]{2,1,0:T(8,128)(2,1)S(1)} %copy-done.4, ...), custom_call_target="tpu_custom_call" | custom-call | flops 2147483648 | bytes 1048576 | tf_op jit(solution)/shard_map/pallas_call | solution.py:29
  103.1 3.4 %collective-permute-start.6 = (bf16[896,256]{1,0:T(8,128)(2,1)S(1)}, bf16[896,256]{1,0:T(8,128)(2,1)S(1)}, u32[]{:S(2)}, u32[]{:S(2)}) collective-permute-start(bf16[896,256]{1,0:T(8,128)(2,1)S(1)} %shard_map.220.own), channel_id=1, source_target_pairs={{0,1},{1,0},{2,3},{3,2},{4,5},{5,4},{6,7},{7,6},{8,9},{9,8},{10,11... | collective-permute-start | bytes 1376264 | tf_op jit(solution)/shard_map/ppermute | solution.py:497
  107.9 2.2 %shard_map.223 = (bf16[1024,128]{1,0:T(8,128)(2,1)S(1)}, bf16[1024,128]{1,0:T(8,128)(2,1)S(1)}, bf16[1024,128]{1,0:T(8,128)(2,1)S(1)}, bf16[1024,128]{1,0:T(8,128)(2,1)S(1)}) custom-call(bf16[896,256]{1,0:T(8,128)(2,1)S(1)} %shard_map.220.own, bf16[896,256]{1,0:T(8,128)(2,1)S(1)} %collective-permute-done.6.far, f32[128,2048]{1,0:T(8,128)S(1)} %shard_map.221.rows, ...), custom_call_target="tpu_custom_call" | custom-call | flops 2147483648 | bytes 1048576 | tf_op jit(solution)/shard_map/pallas_call | solution.py:29
  110.1 1.9 %collective-permute-start.10 = (bf16[1024,128]{1,0:T(8,128)(2,1)S(1)}, bf16[1024,128]{1,0:T(8,128)(2,1)S(1)}, u32[]{:S(2)}, u32[]{:S(2)}) collective-permute-start(bf16[1024,128]{1,0:T(8,128)(2,1)S(1)} %get-tuple-element.50), channel_id=1, source_target_pairs={{0,2},{2,4},{4,6},{6,8},{8,10},{10,12},{12,14},{14,0},{1,3},{3,5},... | collective-permute-start | bytes 786440 | tf_op jit(solution)/shard_map/ppermute | solution.py:497
  112.1 4.6 %collective-permute-start.11 = (bf16[1024,128]{1,0:T(8,128)(2,1)S(1)}, bf16[1024,128]{1,0:T(8,128)(2,1)S(1)}, u32[]{:S(2)}, u32[]{:S(2)}) collective-permute-start(bf16[1024,128]{1,0:T(8,128)(2,1)S(1)} %get-tuple-element.51), channel_id=1, source_target_pairs={{0,14},{2,0},{4,2},{6,4},{8,6},{10,8},{12,10},{14,12},{1,15},{3,1}... | collective-permute-start | bytes 786440 | tf_op jit(solution)/shard_map/ppermute | solution.py:497
  116.7 3.7 %collective-permute-start.12 = (bf16[1024,128]{1,0:T(8,128)(2,1)S(1)}, bf16[1024,128]{1,0:T(8,128)(2,1)S(1)}, u32[]{:S(2)}, u32[]{:S(2)}) collective-permute-start(bf16[1024,128]{1,0:T(8,128)(2,1)S(1)} %get-tuple-element.52), channel_id=1, source_target_pairs={{0,4},{1,13},{2,6},{3,15},{4,8},{5,1},{6,10},{7,3},{8,12},{9,5},{1... | collective-permute-start | bytes 786440 | tf_op jit(solution)/shard_map/ppermute | solution.py:497
  120.4 2.3 %shard_map.222 = (bf16[1024,128]{1,0:T(8,128)(2,1)S(1)}, bf16[1024,128]{1,0:T(8,128)(2,1)S(1)}, bf16[1024,128]{1,0:T(8,128)(2,1)S(1)}, bf16[1024,128]{1,0:T(8,128)(2,1)S(1)}) custom-call(bf16[896,256]{1,0:T(8,128)(2,1)S(1)} %shard_map.220.own, bf16[896,256]{1,0:T(8,128)(2,1)S(1)} %collective-permute-done.6.far, f32[128,2048]{1,0:T(8,128)S(1)} %shard_map.221.rows, ...), custom_call_target="tpu_custom_call" | custom-call | flops 2147483648 | bytes 1048576 | tf_op jit(solution)/shard_map/pallas_call | solution.py:29
  122.6 2.5 %collective-permute-start.8 = (bf16[1024,128]{1,0:T(8,128)(2,1)S(1)}, bf16[1024,128]{1,0:T(8,128)(2,1)S(1)}, u32[]{:S(2)}, u32[]{:S(2)}) collective-permute-start(bf16[1024,128]{1,0:T(8,128)(2,1)S(1)} %get-tuple-element.46), channel_id=1, source_target_pairs={{0,2},{2,4},{4,6},{6,8},{8,10},{10,12},{12,14},{14,0},{1,3},{3,5},... | collective-permute-start | bytes 786440 | tf_op jit(solution)/shard_map/ppermute | solution.py:497
  125.1 4.0 %collective-permute-start.9 = (bf16[1024,128]{1,0:T(8,128)(2,1)S(1)}, bf16[1024,128]{1,0:T(8,128)(2,1)S(1)}, u32[]{:S(2)}, u32[]{:S(2)}) collective-permute-start(bf16[1024,128]{1,0:T(8,128)(2,1)S(1)} %get-tuple-element.47), channel_id=1, source_target_pairs={{0,14},{2,0},{4,2},{6,4},{8,6},{10,8},{12,10},{14,12},{1,15},{3,1}... | collective-permute-start | bytes 786440 | tf_op jit(solution)/shard_map/ppermute | solution.py:497
  129.2 3.5 %collective-permute-done.12.refs_4_ = bf16[1024,128]{1,0:T(8,128)(2,1)S(1)} collective-permute-done((bf16[1024,128]{1,0:T(8,128)(2,1)S(1)}, bf16[1024,128]{1,0:T(8,128)(2,1)S(1)}, u32[]{:S(2)}, u32[]{:S(2)}) %collective-permute-start.12) | collective-permute-done | bytes 262176 | tf_op jit(solution)/shard_map/ppermute | solution.py:497
  132.9 2.4 %collective-permute-start.13 = (bf16[1024,128]{1,0:T(8,128)(2,1)S(1)}, bf16[1024,128]{1,0:T(8,128)(2,1)S(1)}, u32[]{:S(2)}, u32[]{:S(2)}) collective-permute-start(bf16[1024,128]{1,0:T(8,128)(2,1)S(1)} %get-tuple-element.53), channel_id=1, source_target_pairs={{0,4},{2,6},{4,8},{6,10},{8,12},{10,14},{12,0},{14,2},{1,5},{3,7},... | collective-permute-start | bytes 786440 | tf_op jit(solution)/shard_map/ppermute | solution.py:497
  135.3 5.0 %collective-permute-start.14 = (bf16[1024,128]{1,0:T(8,128)(2,1)S(1)}, bf16[1024,128]{1,0:T(8,128)(2,1)S(1)}, u32[]{:S(2)}, u32[]{:S(2)}) collective-permute-start(bf16[1024,128]{1,0:T(8,128)(2,1)S(1)} %get-tuple-element.54), channel_id=1, source_target_pairs={{0,12},{2,14},{4,0},{6,2},{8,4},{10,6},{12,8},{14,10},{1,13},{3,15... | collective-permute-start | bytes 786440 | tf_op jit(solution)/shard_map/ppermute | solution.py:497
  140.4 8.4 %collective-permute-done.13.up = bf16[1024,128]{1,0:T(8,128)(2,1)S(1)} collective-permute-done((bf16[1024,128]{1,0:T(8,128)(2,1)S(1)}, bf16[1024,128]{1,0:T(8,128)(2,1)S(1)}, u32[]{:S(2)}, u32[]{:S(2)}) %collective-permute-start.13) | collective-permute-done | bytes 262176 | tf_op jit(solution)/shard_map/ppermute | solution.py:497
  148.8 1.9 %collective-permute-done.14.down = bf16[1024,128]{1,0:T(8,128)(2,1)S(1)} collective-permute-done((bf16[1024,128]{1,0:T(8,128)(2,1)S(1)}, bf16[1024,128]{1,0:T(8,128)(2,1)S(1)}, u32[]{:S(2)}, u32[]{:S(2)}) %collective-permute-start.14) | collective-permute-done | bytes 262176 | tf_op jit(solution)/shard_map/ppermute | solution.py:497
  151.4 13.5 %all_to_all.16.got = bf16[32,24,128]{2,1,0:T(8,128)(2,1)S(1)} all-to-all(bf16[32,24,128]{2,1,0:T(8,128)(2,1)S(1)} %bitcast.15), channel_id=1, replica_groups=mesh['ep_0'=8,'ep_1'=4,'tp_0'=8,'tp_1'=2] {'ep_0','ep_1'}, dimensions={0} | all-to-all | bytes 393216 | tf_op jit(solution)/shard_map/all_to_all | solution.py:513
  (51 shorter events, 12.6 us)
Async XLA Ops:
  2.0 17.0 %collective-permute-start = (bf16[8,512]{1,0:T(8,128)(2,1)}, bf16[8,512]{1,0:T(8,128)(2,1)S(1)}, u32[]{:S(2)}, u32[]{:S(2)}) collective-permute-start(bf16[8,512]{1,0:T(8,128)(2,1)} %shard_map.213), channel_id=1, source_target_pairs={{0,16},{16,32},{32,48},{48,64},{64,80},{80,96},{96,112},{112,128},... | collective-permute-start | bytes 24584 | tf_op jit(solution)/shard_map/ppermute | solution.py:497
  9.5 64.3 %collective-permute-start.4 = (bf16[3072,256]{1,0:T(8,128)(2,1)}, bf16[3072,256]{1,0:T(8,128)(2,1)S(1)}, u32[]{:S(2)}, u32[]{:S(2)}) collective-permute-start(bf16[3072,256]{1,0:T(8,128)(2,1)} %get-tuple-element.37), channel_id=1, source_target_pairs={{0,1},{1,0},{2,3},{3,2},{4,5},{5,4},{6,7},{7,6},{8,9},{9,8},{10,11... | collective-permute-start | bytes 4718600 | tf_op jit(solution)/shard_map/ppermute | solution.py:497
  19.0 0.6 copy-start.14
  48.3 29.8 %copy-start = (bf16[256,2048]{1,0:T(8,128)(2,1)S(1)}, bf16[256,2048]{1,0:T(8,128)(2,1)}, u32[]{:S(2)}) copy-start(bf16[256,2048]{1,0:T(8,128)(2,1)} %result.1) | copy-start | bytes 3145732
  48.3 32.2 %copy-start.15 = (bf16[256]{0:T(256)(128)(2,1)S(1)}, bf16[256]{0:T(256)(128)(2,1)}, u32[]{:S(2)}) copy-start(bf16[256]{0:T(256)(128)(2,1)} %param.33) | copy-start | bytes 1540
  48.3 12.7 %collective-permute-start.1 = (bf16[32,48,128]{2,1,0:T(8,128)(2,1)S(1)}, bf16[32,48,128]{2,1,0:T(8,128)(2,1)S(1)}, u32[]{:S(2)}, u32[]{:S(2)}) collective-permute-start(bf16[32,48,128]{2,1,0:T(8,128)(2,1)S(1)} %slice.4.refs_0_), channel_id=1, source_target_pairs={{0,2},{2,4},{4,6},{6,8},{8,10},{10,12},{12,14},{14,0},{1,3},{3,5},... | collective-permute-start | bytes 1179656 | tf_op jit(solution)/shard_map/ppermute | solution.py:497
  51.6 10.6 %collective-permute-start.2 = (bf16[32,48,128]{2,1,0:T(8,128)(2,1)S(1)}, bf16[32,48,128]{2,1,0:T(8,128)(2,1)S(1)}, u32[]{:S(2)}, u32[]{:S(2)}) collective-permute-start(bf16[32,48,128]{2,1,0:T(8,128)(2,1)S(1)} %slice.4.refs_0_), channel_id=1, source_target_pairs={{0,14},{2,0},{4,2},{6,4},{8,6},{10,8},{12,10},{14,12},{1,15},{3,1}... | collective-permute-start | bytes 1179656 | tf_op jit(solution)/shard_map/ppermute | solution.py:497
  55.5 18.4 %collective-permute-start.3 = (bf16[32,48,128]{2,1,0:T(8,128)(2,1)S(1)}, bf16[32,48,128]{2,1,0:T(8,128)(2,1)S(1)}, u32[]{:S(2)}, u32[]{:S(2)}) collective-permute-start(bf16[32,48,128]{2,1,0:T(8,128)(2,1)S(1)} %slice.4.refs_0_), channel_id=1, source_target_pairs={{0,4},{1,13},{2,6},{3,15},{4,8},{5,1},{6,10},{7,3},{8,12},{9,5},{1... | collective-permute-start | bytes 1179656 | tf_op jit(solution)/shard_map/ppermute | solution.py:497
  62.3 13.9 %copy-start.3 = (bf16[32,48,128]{2,1,0:T(8,128)(2,1)}, bf16[32,48,128]{2,1,0:T(8,128)(2,1)S(1)}, u32[]{:S(2)}) copy-start(bf16[32,48,128]{2,1,0:T(8,128)(2,1)S(1)} %collective-permute-done.2.refs_2_) | copy-start | bytes 1179652
  73.8 2.4 %copy-start.5 = (bf16[32,48,128]{2,1,0:T(8,128)(2,1)}, bf16[32,48,128]{2,1,0:T(8,128)(2,1)S(1)}, u32[]{:S(2)}) copy-start(bf16[32,48,128]{2,1,0:T(8,128)(2,1)S(1)} %collective-permute-done.3.refs_3_) | copy-start | bytes 1179652
  76.2 22.9 %collective-permute-start.5 = (bf16[768,512]{1,0:T(8,128)(2,1)}, bf16[768,512]{1,0:T(8,128)(2,1)}, u32[]{:S(2)}, u32[]{:S(2)}) collective-permute-start(bf16[768,512]{1,0:T(8,128)(2,1)} %shard_map.216), channel_id=1, source_target_pairs={{0,1},{1,0},{2,3},{3,2},{4,5},{5,4},{6,7},{7,6},{8,9},{9,8},{10,11... | collective-permute-start | bytes 2359304 | tf_op jit(solution)/shard_map/ppermute | solution.py:497
  78.1 28.7 %collective-permute-start.7 = (bf16[256,2048]{1,0:T(8,128)(2,1)S(1)}, bf16[256,2048]{1,0:T(8,128)(2,1)}, u32[]{:S(2)}, u32[]{:S(2)}) collective-permute-start(bf16[256,2048]{1,0:T(8,128)(2,1)S(1)} %copy-done), channel_id=1, source_target_pairs={{0,1},{1,0},{2,3},{3,2},{4,5},{5,4},{6,7},{7,6},{8,9},{9,8},{10,11... | collective-permute-start | bytes 3145736 | tf_op jit(solution)/shard_map/ppermute | solution.py:497
  81.9 14.0 %all-to-all-start.1 = ((bf16[32,8,128]{2,1,0:T(8,128)(2,1)}), bf16[32,8,128]{2,1,0:T(8,128)(2,1)S(1)}, u32[]{:S(2)}, u32[]{:S(2)}) async-start(bf16[32,8,128]{2,1,0:T(8,128)(2,1)} %shard_map.218), calls=%async_computation.1 | async-start | bytes 131072 | tf_op jit(solution)/shard_map/all_to_all | solution.py:513
  86.9 9.0 %copy-start.11 = (bf16[256,128]{1,0:T(8,128)(2,1)S(1)}, bf16[256,128]{1,0:T(8,128)(2,1)}, u32[]{:S(2)}) copy-start(bf16[256,128]{1,0:T(8,128)(2,1)} %get-tuple-element.40.c.refs_1_) | copy-start | bytes 196612
  95.9 0.9 copy-start.7
  96.8 0.9 copy-start.10
  97.7 0.9 copy-start.12
  98.6 1.2 copy-start.1
  98.6 1.5 copy-start.2
  98.6 1.6 copy-start.4
  98.7 1.7 %copy-start.6 = (bf16[32,48,128]{2,1,0:T(8,128)(2,1)S(1)}, bf16[32,48,128]{2,1,0:T(8,128)(2,1)}, u32[]{:S(2)}) copy-start(bf16[32,48,128]{2,1,0:T(8,128)(2,1)} %copy-done.5) | copy-start | bytes 1179652
  103.1 4.8 %copy-start.9 = (bf16[1024,256]{1,0:T(8,128)(2,1)S(1)}, bf16[1024,256]{1,0:T(8,128)(2,1)}, u32[]{:S(2)}) copy-start(bf16[1024,256]{1,0:T(8,128)(2,1)} %get-tuple-element.44.keep) | copy-start | bytes 1572868
  103.1 4.8 %collective-permute-start.6 = (bf16[896,256]{1,0:T(8,128)(2,1)S(1)}, bf16[896,256]{1,0:T(8,128)(2,1)S(1)}, u32[]{:S(2)}, u32[]{:S(2)}) collective-permute-start(bf16[896,256]{1,0:T(8,128)(2,1)S(1)} %shard_map.220.own), channel_id=1, source_target_pairs={{0,1},{1,0},{2,3},{3,2},{4,5},{5,4},{6,7},{7,6},{8,9},{9,8},{10,11... | collective-permute-start | bytes 1376264 | tf_op jit(solution)/shard_map/ppermute | solution.py:497
  110.1 19.0 %collective-permute-start.10 = (bf16[1024,128]{1,0:T(8,128)(2,1)S(1)}, bf16[1024,128]{1,0:T(8,128)(2,1)S(1)}, u32[]{:S(2)}, u32[]{:S(2)}) collective-permute-start(bf16[1024,128]{1,0:T(8,128)(2,1)S(1)} %get-tuple-element.50), channel_id=1, source_target_pairs={{0,2},{2,4},{4,6},{6,8},{8,10},{10,12},{12,14},{14,0},{1,3},{3,5},... | collective-permute-start | bytes 786440 | tf_op jit(solution)/shard_map/ppermute | solution.py:497
  112.1 17.1 %collective-permute-start.11 = (bf16[1024,128]{1,0:T(8,128)(2,1)S(1)}, bf16[1024,128]{1,0:T(8,128)(2,1)S(1)}, u32[]{:S(2)}, u32[]{:S(2)}) collective-permute-start(bf16[1024,128]{1,0:T(8,128)(2,1)S(1)} %get-tuple-element.51), channel_id=1, source_target_pairs={{0,14},{2,0},{4,2},{6,4},{8,6},{10,8},{12,10},{14,12},{1,15},{3,1}... | collective-permute-start | bytes 786440 | tf_op jit(solution)/shard_map/ppermute | solution.py:497
  116.7 16.0 %collective-permute-start.12 = (bf16[1024,128]{1,0:T(8,128)(2,1)S(1)}, bf16[1024,128]{1,0:T(8,128)(2,1)S(1)}, u32[]{:S(2)}, u32[]{:S(2)}) collective-permute-start(bf16[1024,128]{1,0:T(8,128)(2,1)S(1)} %get-tuple-element.52), channel_id=1, source_target_pairs={{0,4},{1,13},{2,6},{3,15},{4,8},{5,1},{6,10},{7,3},{8,12},{9,5},{1... | collective-permute-start | bytes 786440 | tf_op jit(solution)/shard_map/ppermute | solution.py:497
  122.6 17.7 %collective-permute-start.8 = (bf16[1024,128]{1,0:T(8,128)(2,1)S(1)}, bf16[1024,128]{1,0:T(8,128)(2,1)S(1)}, u32[]{:S(2)}, u32[]{:S(2)}) collective-permute-start(bf16[1024,128]{1,0:T(8,128)(2,1)S(1)} %get-tuple-element.46), channel_id=1, source_target_pairs={{0,2},{2,4},{4,6},{6,8},{8,10},{10,12},{12,14},{14,0},{1,3},{3,5},... | collective-permute-start | bytes 786440 | tf_op jit(solution)/shard_map/ppermute | solution.py:497
  125.1 15.2 %collective-permute-start.9 = (bf16[1024,128]{1,0:T(8,128)(2,1)S(1)}, bf16[1024,128]{1,0:T(8,128)(2,1)S(1)}, u32[]{:S(2)}, u32[]{:S(2)}) collective-permute-start(bf16[1024,128]{1,0:T(8,128)(2,1)S(1)} %get-tuple-element.47), channel_id=1, source_target_pairs={{0,14},{2,0},{4,2},{6,4},{8,6},{10,8},{12,10},{14,12},{1,15},{3,1}... | collective-permute-start | bytes 786440 | tf_op jit(solution)/shard_map/ppermute | solution.py:497
  132.9 31.9 %copy-start.8 = (f32[256,2]{0,1:T(2,128)S(1)}, f32[256,2]{0,1:T(2,128)}, u32[]{:S(2)}) copy-start(f32[256,2]{0,1:T(2,128)} %param.41) | copy-start | bytes 6148
  132.9 31.9 %copy-start.13 = (s32[2,256]{1,0:T(2,128)S(1)}, s32[2,256]{1,0:T(2,128)}, u32[]{:S(2)}) copy-start(s32[2,256]{1,0:T(2,128)} %get-tuple-element.57.slots) | copy-start | bytes 6148
  132.9 15.9 %collective-permute-start.13 = (bf16[1024,128]{1,0:T(8,128)(2,1)S(1)}, bf16[1024,128]{1,0:T(8,128)(2,1)S(1)}, u32[]{:S(2)}, u32[]{:S(2)}) collective-permute-start(bf16[1024,128]{1,0:T(8,128)(2,1)S(1)} %get-tuple-element.53), channel_id=1, source_target_pairs={{0,4},{2,6},{4,8},{6,10},{8,12},{10,14},{12,0},{14,2},{1,5},{3,7},... | collective-permute-start | bytes 786440 | tf_op jit(solution)/shard_map/ppermute | solution.py:497
  135.3 15.4 %collective-permute-start.14 = (bf16[1024,128]{1,0:T(8,128)(2,1)S(1)}, bf16[1024,128]{1,0:T(8,128)(2,1)S(1)}, u32[]{:S(2)}, u32[]{:S(2)}) collective-permute-start(bf16[1024,128]{1,0:T(8,128)(2,1)S(1)} %get-tuple-element.54), channel_id=1, source_target_pairs={{0,12},{2,14},{4,0},{6,2},{8,4},{10,6},{12,8},{14,10},{1,13},{3,15... | collective-permute-start | bytes 786440 | tf_op jit(solution)/shard_map/ppermute | solution.py:497

commit v6 on v5

--- a/solution.py
+++ b/solution.py
@@ -338,12 +338,15 @@
     out[sources * capacity :, :] = rows[...]
 
 
-def split_body(place, valve, expand, contract, keep, give):
-    half = valve.shape[0] // 2
+def split_body(place, valve, expand, contract, result, keep, give):
+    half, width = valve.shape[0] // 2, valve.shape[1]
     theirs = pl.ds(pl.multiple_of((1 - place[0]) * half, half), half)
     give[0:half, :] = valve[theirs, :]
     give[half : 2 * half, :] = expand[theirs, :]
     depth = contract.shape[0]
+    for k in range(result.shape[1] // width):
+        row = 3 * half + k * depth
+        give[row : row + depth, :] = result[:, k * width : (k + 1) * width]
     for k, home in enumerate(HOMES):
         base = 2 * ((place[1] + home) % len(HOMES))
         row, lane = k // 2 * depth, k % 2 * 128
@@ -360,11 +363,11 @@
         out[:, columns] = dot(rows[...], result[:, columns])
 
 
-def down_body(start, own, far, rows, keep, weights, result_far, *outs):
+def down_body(start, own, far, rows, keep, weights, *outs):
     depth = own.shape[1]
     each = rows.shape[0] // len(HOMES)
     total = own.shape[0] - rows.shape[0]
-    far_first = weights.shape[0] - keep.shape[0]
+    far_first = 2 * keep.shape[0]
     block = total // 2
 
     def step(i, _):
@@ -382,10 +385,12 @@
     lax.fori_loop(0, total // block, step, 0)
     first, last = start * each, (start + len(outs)) * each
     beyond = far[total + first : total + last, :]
-    wide = 512
+    wide = weights.shape[1]
     for column in range(0, rows.shape[1], wide):
-        columns = slice(column, column + wide)
-        product = rows[first:last, columns] + dot(beyond, result_far[:, columns])
+        row = far_first + keep.shape[0] + column // wide * depth
+        product = rows[first:last, column : column + wide] + dot(
+            beyond, weights[row : row + depth, :]
+        )
         product = product.astype(BF16)
         for k, out in enumerate(outs):
             for j in range(wide // 128):
@@ -563,14 +568,13 @@
     half = model_width // 2
     keep, give = call(
         placed(split_body),
-        (shaped(half, hidden_width), shaped(3 * half, hidden_width)),
-        (*place, valve, expand, contract),
+        (shaped(half, hidden_width), shaped(5 * half, hidden_width)),
+        (*place, valve, expand, contract, blender_result_matrix),
         1 << 30,
         None,
         smem=2,
     )
     weights_far = partner(give)
-    result_far = partner(blender_result_matrix)
 
     own = got[:, 0 : 2 * capacity, :]
     beyond = across(own)
@@ -629,7 +633,7 @@
         return call(
             functools.partial(down_body, start),
             (shaped(all_rows, lanes),) * 4,
-            (ours, ours_far, projected, keep, weights_far, result_far),
+            (ours, ours_far, projected, keep, weights_far),
             1 << 31,
             12,
         )

time: 168 us -> 163 us (0.970)
  starting transfers between devices: 58.1 us -> 55.9 us
  Pallas kernels: 27.1 us -> 25.4 us
    ppermute x15 -> x14, starting transfers between devices: 53.1 us -> 51.1 us  [permuted(): return lax.ppermute(x, axis, pairs)]
    ppermute x15 -> x14, waiting for transfers between devices: 29.1 us -> 29.1 us  [permuted(): return lax.ppermute(x, axis, pairs)]
  transfers between devices with their start and end apart: 16 -> 15, of which waited for: 8 -> 8; matrix products, arithmetic and copies ran while one was open for 0% -> 0% of each run, Pallas kernels for 12% -> 8%
where the time goes in v6:
time: 163 us; the launch traced here: 161 us
  starting transfers between devices  55.9 us (34%)
  blocking collectives  38.7 us (24%)
  waiting for transfers between devices  35.3 us (22%)
  Pallas kernels  25.4 us (16%)
  local copies, waits for them, and re-layouts  4.75 us (3%)
    ppermute x14, starting transfers between devices, permuted(): return lax.ppermute(x, axis, pairs)  51.1 us
    all_to_all x2, blocking collectives, exchanged(): return lax.all_to_all(x, axis, 0, 0, tiled=True)  38.7 us
    ppermute x14, waiting for transfers between devices, permuted(): return lax.ppermute(x, axis, pairs)  29.1 us
    pallas_call x14, Pallas kernels, call(): pl.pallas_call(body, out_shape=outs, in_specs=[SMEM] * smem + [pl.BlockSp...  24 us
    all_to_all x1, waiting for transfers between devices, exchanged(): return lax.all_to_all(x, axis, 0, 0, tiled=True)  6.26 us
    all_to_all x1, starting transfers between devices, exchanged(): return lax.all_to_all(x, axis, 0, 0, tiled=True)  4.82 us
    unnamed x32, local copies, waits for them, and re-layouts  4.72 us
  transfers between devices with their start and end apart: 15, of which 8 were waited for; matrix products, arithmetic and copies ran while one was open for 0% of the time, Pallas kernels for 8%

profile of v6, /device:TPU:1, one launch (start us, length us, event | category | flops | bytes accessed | tf_op | source)
XLA Modules:
  0.0 161.0 jit_solution(17646229081528569773)
XLA Ops:
  0.6 4.2 %shard_map.215 = (bf16[1024,256]{1,0:T(8,128)(2,1)}, bf16[5120,256]{1,0:T(8,128)(2,1)}) custom-call(s32[1]{0:T(128)} %bitcast.core, s32[1]{0:T(128)} %bitcast.1.chip, bf16[2048,256]{1,0:T(8,128)(2,1)} %bitcast.15, bf16[2048,256]{1,0:T(8,128)(2,1)} %bitcast.17, bf16[256,2048]{1,0:T(8,128)(2,1)} %bitcast.22, bf16[256,2048]{1,0:T(8,128)(2,1)} %result.1), custom_call_target="tpu_custom_call" | custom-call | flops 1073741824 | bytes 1048576 | tf_op jit(solution)/shard_map/pallas_call | solution.py:29
  4.9 8.7 %collective-permute-start.4 = (bf16[5120,256]{1,0:T(8,128)(2,1)}, bf16[5120,256]{1,0:T(8,128)(2,1)S(1)}, u32[]{:S(2)}, u32[]{:S(2)}) collective-permute-start(bf16[5120,256]{1,0:T(8,128)(2,1)} %get-tuple-element.37), channel_id=1, source_target_pairs={{0,1},{1,0},{2,3},{3,2},{4,5},{5,4},{6,7},{7,6},{8,9},{9,8},{10,11... | collective-permute-start | bytes 7864328 | tf_op jit(solution)/shard_map/ppermute | solution.py:502
  13.6 1.3 shard_map.213
  15.0 1.3 collective-permute-start
  16.3 3.4 %shard_map.212 = (bf16[768,256]{1,0:T(8,128)(2,1)}, s32[2,256]{1,0:T(2,128)}, f32[256,256]{1,0:T(8,128)}, bf16[256,128]{1,0:T(8,128)(2,1)}, bf16[256,128]{1,0:T(...) custom-call(s32[1]{0:T(128)} %bitcast.2.place, f32[4]{0:T(128)} %offset.1, f32[4]{0:T(128)} %speed.1, ...), custom_call_target="tpu_custom_call" | custom-call | flops 1073741824 | bytes 1048576 | tf_op jit(solution)/shard_map/pallas_call | solution.py:29
  20.2 2.6 %shard_map.214 = (bf16[32,64,128]{2,1,0:T(8,128)(2,1)}, f32[256,256]{1,0:T(8,128)}, bf16[256,128]{1,0:T(8,128)(2,1)}, bf16[256,128]{1,0:T(8,128)(2,1)}) custom-call(bf16[768,256]{1,0:T(8,128)(2,1)} %get-tuple-element.30.routed, f32[256,256]{1,0:T(8,128)} %get-tuple-element.31.x_in, bf16[256,128]{1,0:T(8,128)(2,1)} %get-tuple-element.32.b_in, ...), custom_call_target="tpu_custom_call" | custom-call | flops 1073741824 | bytes 1048576 | tf_op jit(solution)/shard_map/pallas_call | solution.py:29
  22.8 25.7 %all_to_all.15.got = bf16[32,64,128]{2,1,0:T(8,128)(2,1)S(1)} all-to-all(bf16[32,64,128]{2,1,0:T(8,128)(2,1)} %get-tuple-element.36), channel_id=1, replica_groups=mesh['ep_0'=8,'ep_1'=4,'tp_0'=8,'tp_1'=2] {'ep_0','ep_1'}, dimensions={0} | all-to-all | bytes 1048576 | tf_op jit(solution)/shard_map/all_to_all | solution.py:518
  48.5 3.2 %collective-permute-start.1 = (bf16[32,48,128]{2,1,0:T(8,128)(2,1)S(1)}, bf16[32,48,128]{2,1,0:T(8,128)(2,1)S(1)}, u32[]{:S(2)}, u32[]{:S(2)}) collective-permute-start(bf16[32,48,128]{2,1,0:T(8,128)(2,1)S(1)} %slice.4.refs_0_), channel_id=1, source_target_pairs={{0,2},{2,4},{4,6},{6,8},{8,10},{10,12},{12,14},{14,0},{1,3},{3,5},... | collective-permute-start | bytes 1179656 | tf_op jit(solution)/shard_map/ppermute | solution.py:502
  51.7 3.8 %collective-permute-start.2 = (bf16[32,48,128]{2,1,0:T(8,128)(2,1)S(1)}, bf16[32,48,128]{2,1,0:T(8,128)(2,1)S(1)}, u32[]{:S(2)}, u32[]{:S(2)}) collective-permute-start(bf16[32,48,128]{2,1,0:T(8,128)(2,1)S(1)} %slice.4.refs_0_), channel_id=1, source_target_pairs={{0,14},{2,0},{4,2},{6,4},{8,6},{10,8},{12,10},{14,12},{1,15},{3,1}... | collective-permute-start | bytes 1179656 | tf_op jit(solution)/shard_map/ppermute | solution.py:502
  55.6 4.1 %collective-permute-start.3 = (bf16[32,48,128]{2,1,0:T(8,128)(2,1)S(1)}, bf16[32,48,128]{2,1,0:T(8,128)(2,1)S(1)}, u32[]{:S(2)}, u32[]{:S(2)}) collective-permute-start(bf16[32,48,128]{2,1,0:T(8,128)(2,1)S(1)} %slice.4.refs_0_), channel_id=1, source_target_pairs={{0,4},{1,13},{2,6},{3,15},{4,8},{5,1},{6,10},{7,3},{8,12},{9,5},{1... | collective-permute-start | bytes 1179656 | tf_op jit(solution)/shard_map/ppermute | solution.py:502
  59.7 1.2 collective-permute-done.1.refs_1_
  61.0 1.3 collective-permute-done.2.refs_2_
  62.3 11.6 %collective-permute-done.3.refs_3_ = bf16[32,48,128]{2,1,0:T(8,128)(2,1)S(1)} collective-permute-done((bf16[32,48,128]{2,1,0:T(8,128)(2,1)S(1)}, bf16[32,48,128]{2,1,0:T(8,128)(2,1)S(1)}, u32[]{:S(2)}, u32[]{:S(2)}) %collective-permute-start.3) | collective-permute-done | bytes 393248 | tf_op jit(solution)/shard_map/ppermute | solution.py:502
  73.9 2.4 %shard_map.216 = bf16[768,512]{1,0:T(8,128)(2,1)} custom-call(s32[1]{0:T(128)} %bitcast.core, s32[1]{0:T(128)} %bitcast.1.chip, bf16[32,48,128]{2,1,0:T(8,128)(2,1)S(1)} %slice.4.refs_0_, bf16[32,48,128]{2,1,0:T(8,128)(2,1)S(1)} %collective-permute-done.1.refs_1_, bf16[32,48,128]{2,1,0:T(8,128)(2,1)S(1)} %collective-permute-done.2.refs_2_, ...), custom_call_target="tpu_custom_call" | custom-call | flops 2147483648 | bytes 1048576 | tf_op jit(solution)/shard_map/pallas_call | solution.py:29
  76.3 2.0 %collective-permute-start.5 = (bf16[768,512]{1,0:T(8,128)(2,1)}, bf16[768,512]{1,0:T(8,128)(2,1)}, u32[]{:S(2)}, u32[]{:S(2)}) collective-permute-start(bf16[768,512]{1,0:T(8,128)(2,1)} %shard_map.216), channel_id=1, source_target_pairs={{0,1},{1,0},{2,3},{3,2},{4,5},{5,4},{6,7},{7,6},{8,9},{9,8},{10,11... | collective-permute-start | bytes 2359304 | tf_op jit(solution)/shard_map/ppermute | solution.py:502
  78.4 1.3 shard_map.218
  79.7 4.8 %all-to-all-start.1 = ((bf16[32,8,128]{2,1,0:T(8,128)(2,1)}), bf16[32,8,128]{2,1,0:T(8,128)(2,1)S(1)}, u32[]{:S(2)}, u32[]{:S(2)}) async-start(bf16[32,8,128]{2,1,0:T(8,128)(2,1)} %shard_map.218), calls=%async_computation.1 | async-start | bytes 131072 | tf_op jit(solution)/shard_map/all_to_all | solution.py:518
  84.5 2.5 %shard_map.217.refs_0_ = f32[256,256]{1,0:T(8,128)} custom-call(f32[4]{0:T(128)} %bypass.1, f32[256,256]{1,0:T(8,128)} %get-tuple-element.38.x, bf16[256,128]{1,0:T(8,128)(2,1)} %get-tuple-element.39.b, bf16[256,128]{1,0:T(8,128)(2,1)} %get-tuple-element.40.c.refs_1_, f32[256,8]{1,0:T(8,128)} %get-tuple-element.35.columns_in.columns.refs_2_, ...), custom_call_target="tpu_custom_call" | custom-call | flops 2147483648 | bytes 1048576 | tf_op jit(solution)/shard_map/pallas_call | solution.py:29
  87.1 6.3 %all-to-all-done.1 = bf16[32,8,128]{2,1,0:T(8,128)(2,1)S(1)} async-done(((bf16[32,8,128]{2,1,0:T(8,128)(2,1)}), bf16[32,8,128]{2,1,0:T(8,128)(2,1)S(1)}, u32[]{:S(2)}, u32[]{:S(2)}) %all-to-all-start.1) | async-done | bytes 65568 | tf_op jit(solution)/shard_map/all_to_all | solution.py:518
  97.9 2.8 %shard_map.220.own = bf16[896,256]{1,0:T(8,128)(2,1)S(1)} custom-call(s32[1]{0:T(128)} %bitcast.core, s32[1]{0:T(128)} %bitcast.1.chip, bf16[32,48,128]{2,1,0:T(8,128)(2,1)S(1)} %slice.4.refs_0_, bf16[32,48,128]{2,1,0:T(8,128)(2,1)S(1)} %collective-permute-done.1.refs_1_, bf16[32,48,128]{2,1,0:T(8,128)(2,1)S(1)} %copy-done.5, ...), custom_call_target="tpu_custom_call" | custom-call | flops 2147483648 | bytes 1048576 | tf_op jit(solution)/shard_map/pallas_call | solution.py:29
  100.7 3.8 %collective-permute-start.6 = (bf16[896,256]{1,0:T(8,128)(2,1)S(1)}, bf16[896,256]{1,0:T(8,128)(2,1)S(1)}, u32[]{:S(2)}, u32[]{:S(2)}) collective-permute-start(bf16[896,256]{1,0:T(8,128)(2,1)S(1)} %shard_map.220.own), channel_id=1, source_target_pairs={{0,1},{1,0},{2,3},{3,2},{4,5},{5,4},{6,7},{7,6},{8,9},{9,8},{10,11... | collective-permute-start | bytes 1376264 | tf_op jit(solution)/shard_map/ppermute | solution.py:502
  107.0 1.9 %collective-permute-start.9 = (bf16[1024,128]{1,0:T(8,128)(2,1)S(1)}, bf16[1024,128]{1,0:T(8,128)(2,1)S(1)}, u32[]{:S(2)}, u32[]{:S(2)}) collective-permute-start(bf16[1024,128]{1,0:T(8,128)(2,1)S(1)} %get-tuple-element.50), channel_id=1, source_target_pairs={{0,2},{2,4},{4,6},{6,8},{8,10},{10,12},{12,14},{14,0},{1,3},{3,5},... | collective-permute-start | bytes 786440 | tf_op jit(solution)/shard_map/ppermute | solution.py:502
  108.9 4.6 %collective-permute-start.10 = (bf16[1024,128]{1,0:T(8,128)(2,1)S(1)}, bf16[1024,128]{1,0:T(8,128)(2,1)S(1)}, u32[]{:S(2)}, u32[]{:S(2)}) collective-permute-start(bf16[1024,128]{1,0:T(8,128)(2,1)S(1)} %get-tuple-element.51), channel_id=1, source_target_pairs={{0,14},{2,0},{4,2},{6,4},{8,6},{10,8},{12,10},{14,12},{1,15},{3,1}... | collective-permute-start | bytes 786440 | tf_op jit(solution)/shard_map/ppermute | solution.py:502
  113.5 3.7 %collective-permute-start.11 = (bf16[1024,128]{1,0:T(8,128)(2,1)S(1)}, bf16[1024,128]{1,0:T(8,128)(2,1)S(1)}, u32[]{:S(2)}, u32[]{:S(2)}) collective-permute-start(bf16[1024,128]{1,0:T(8,128)(2,1)S(1)} %get-tuple-element.52), channel_id=1, source_target_pairs={{0,4},{1,13},{2,6},{3,15},{4,8},{5,1},{6,10},{7,3},{8,12},{9,5},{1... | collective-permute-start | bytes 786440 | tf_op jit(solution)/shard_map/ppermute | solution.py:502
  118.3 2.5 %collective-permute-start.7 = (bf16[1024,128]{1,0:T(8,128)(2,1)S(1)}, bf16[1024,128]{1,0:T(8,128)(2,1)S(1)}, u32[]{:S(2)}, u32[]{:S(2)}) collective-permute-start(bf16[1024,128]{1,0:T(8,128)(2,1)S(1)} %get-tuple-element.46), channel_id=1, source_target_pairs={{0,2},{2,4},{4,6},{6,8},{8,10},{10,12},{12,14},{14,0},{1,3},{3,5},... | collective-permute-start | bytes 786440 | tf_op jit(solution)/shard_map/ppermute | solution.py:502
  120.7 4.0 %collective-permute-start.8 = (bf16[1024,128]{1,0:T(8,128)(2,1)S(1)}, bf16[1024,128]{1,0:T(8,128)(2,1)S(1)}, u32[]{:S(2)}, u32[]{:S(2)}) collective-permute-start(bf16[1024,128]{1,0:T(8,128)(2,1)S(1)} %get-tuple-element.47), channel_id=1, source_target_pairs={{0,14},{2,0},{4,2},{6,4},{8,6},{10,8},{12,10},{14,12},{1,15},{3,1}... | collective-permute-start | bytes 786440 | tf_op jit(solution)/shard_map/ppermute | solution.py:502
  124.8 5.0 %collective-permute-done.11.refs_4_ = bf16[1024,128]{1,0:T(8,128)(2,1)S(1)} collective-permute-done((bf16[1024,128]{1,0:T(8,128)(2,1)S(1)}, bf16[1024,128]{1,0:T(8,128)(2,1)S(1)}, u32[]{:S(2)}, u32[]{:S(2)}) %collective-permute-start.11) | collective-permute-done | bytes 262176 | tf_op jit(solution)/shard_map/ppermute | solution.py:502
  130.0 2.1 %collective-permute-start.12 = (bf16[1024,128]{1,0:T(8,128)(2,1)S(1)}, bf16[1024,128]{1,0:T(8,128)(2,1)S(1)}, u32[]{:S(2)}, u32[]{:S(2)}) collective-permute-start(bf16[1024,128]{1,0:T(8,128)(2,1)S(1)} %get-tuple-element.53), channel_id=1, source_target_pairs={{0,4},{2,6},{4,8},{6,10},{8,12},{10,14},{12,0},{14,2},{1,5},{3,7},... | collective-permute-start | bytes 786440 | tf_op jit(solution)/shard_map/ppermute | solution.py:502
  132.2 5.3 %collective-permute-start.13 = (bf16[1024,128]{1,0:T(8,128)(2,1)S(1)}, bf16[1024,128]{1,0:T(8,128)(2,1)S(1)}, u32[]{:S(2)}, u32[]{:S(2)}) collective-permute-start(bf16[1024,128]{1,0:T(8,128)(2,1)S(1)} %get-tuple-element.54), channel_id=1, source_target_pairs={{0,12},{2,14},{4,0},{6,2},{8,4},{10,6},{12,8},{14,10},{1,13},{3,15... | collective-permute-start | bytes 786440 | tf_op jit(solution)/shard_map/ppermute | solution.py:502
  137.5 8.1 %collective-permute-done.12.up = bf16[1024,128]{1,0:T(8,128)(2,1)S(1)} collective-permute-done((bf16[1024,128]{1,0:T(8,128)(2,1)S(1)}, bf16[1024,128]{1,0:T(8,128)(2,1)S(1)}, u32[]{:S(2)}, u32[]{:S(2)}) %collective-permute-start.12) | collective-permute-done | bytes 262176 | tf_op jit(solution)/shard_map/ppermute | solution.py:502
  146.9 13.0 %all_to_all.16.got = bf16[32,24,128]{2,1,0:T(8,128)(2,1)S(1)} all-to-all(bf16[32,24,128]{2,1,0:T(8,128)(2,1)S(1)} %bitcast.19), channel_id=1, replica_groups=mesh['ep_0'=8,'ep_1'=4,'tp_0'=8,'tp_1'=2] {'ep_0','ep_1'}, dimensions={0} | all-to-all | bytes 393216 | tf_op jit(solution)/shard_map/all_to_all | solution.py:518
  159.9 1.1 shard_map.226
  (49 shorter events, 10.2 us)
Async XLA Ops:
  4.9 69.0 %collective-permute-start.4 = (bf16[5120,256]{1,0:T(8,128)(2,1)}, bf16[5120,256]{1,0:T(8,128)(2,1)S(1)}, u32[]{:S(2)}, u32[]{:S(2)}) collective-permute-start(bf16[5120,256]{1,0:T(8,128)(2,1)} %get-tuple-element.37), channel_id=1, source_target_pairs={{0,1},{1,0},{2,3},{3,2},{4,5},{5,4},{6,7},{7,6},{8,9},{9,8},{10,11... | collective-permute-start | bytes 7864328 | tf_op jit(solution)/shard_map/ppermute | solution.py:502
  15.0 4.7 %collective-permute-start = (bf16[8,512]{1,0:T(8,128)(2,1)}, bf16[8,512]{1,0:T(8,128)(2,1)S(1)}, u32[]{:S(2)}, u32[]{:S(2)}) collective-permute-start(bf16[8,512]{1,0:T(8,128)(2,1)} %shard_map.213), channel_id=1, source_target_pairs={{0,16},{16,32},{32,48},{48,64},{64,80},{80,96},{96,112},{112,128},... | collective-permute-start | bytes 24584 | tf_op jit(solution)/shard_map/ppermute | solution.py:502
  19.7 0.6 copy-start.14
  48.5 29.8 %copy-start.15 = (bf16[256]{0:T(256)(128)(2,1)S(1)}, bf16[256]{0:T(256)(128)(2,1)}, u32[]{:S(2)}) copy-start(bf16[256]{0:T(256)(128)(2,1)} %param.33) | copy-start | bytes 1540
  48.5 12.4 %collective-permute-start.1 = (bf16[32,48,128]{2,1,0:T(8,128)(2,1)S(1)}, bf16[32,48,128]{2,1,0:T(8,128)(2,1)S(1)}, u32[]{:S(2)}, u32[]{:S(2)}) collective-permute-start(bf16[32,48,128]{2,1,0:T(8,128)(2,1)S(1)} %slice.4.refs_0_), channel_id=1, source_target_pairs={{0,2},{2,4},{4,6},{6,8},{8,10},{10,12},{12,14},{14,0},{1,3},{3,5},... | collective-permute-start | bytes 1179656 | tf_op jit(solution)/shard_map/ppermute | solution.py:502
  51.7 10.5 %collective-permute-start.2 = (bf16[32,48,128]{2,1,0:T(8,128)(2,1)S(1)}, bf16[32,48,128]{2,1,0:T(8,128)(2,1)S(1)}, u32[]{:S(2)}, u32[]{:S(2)}) collective-permute-start(bf16[32,48,128]{2,1,0:T(8,128)(2,1)S(1)} %slice.4.refs_0_), channel_id=1, source_target_pairs={{0,14},{2,0},{4,2},{6,4},{8,6},{10,8},{12,10},{14,12},{1,15},{3,1}... | collective-permute-start | bytes 1179656 | tf_op jit(solution)/shard_map/ppermute | solution.py:502
  55.6 18.4 %collective-permute-start.3 = (bf16[32,48,128]{2,1,0:T(8,128)(2,1)S(1)}, bf16[32,48,128]{2,1,0:T(8,128)(2,1)S(1)}, u32[]{:S(2)}, u32[]{:S(2)}) collective-permute-start(bf16[32,48,128]{2,1,0:T(8,128)(2,1)S(1)} %slice.4.refs_0_), channel_id=1, source_target_pairs={{0,4},{1,13},{2,6},{3,15},{4,8},{5,1},{6,10},{7,3},{8,12},{9,5},{1... | collective-permute-start | bytes 1179656 | tf_op jit(solution)/shard_map/ppermute | solution.py:502
  62.3 14.1 %copy-start.4 = (bf16[32,48,128]{2,1,0:T(8,128)(2,1)}, bf16[32,48,128]{2,1,0:T(8,128)(2,1)S(1)}, u32[]{:S(2)}) copy-start(bf16[32,48,128]{2,1,0:T(8,128)(2,1)S(1)} %collective-permute-done.2.refs_2_) | copy-start | bytes 1179652
  73.9 2.4 %copy-start.6 = (bf16[32,48,128]{2,1,0:T(8,128)(2,1)}, bf16[32,48,128]{2,1,0:T(8,128)(2,1)S(1)}, u32[]{:S(2)}) copy-start(bf16[32,48,128]{2,1,0:T(8,128)(2,1)S(1)} %collective-permute-done.3.refs_3_) | copy-start | bytes 1179652
  76.3 20.2 %collective-permute-start.5 = (bf16[768,512]{1,0:T(8,128)(2,1)}, bf16[768,512]{1,0:T(8,128)(2,1)}, u32[]{:S(2)}, u32[]{:S(2)}) collective-permute-start(bf16[768,512]{1,0:T(8,128)(2,1)} %shard_map.216), channel_id=1, source_target_pairs={{0,1},{1,0},{2,3},{3,2},{4,5},{5,4},{6,7},{7,6},{8,9},{9,8},{10,11... | collective-permute-start | bytes 2359304 | tf_op jit(solution)/shard_map/ppermute | solution.py:502
  79.7 13.6 %all-to-all-start.1 = ((bf16[32,8,128]{2,1,0:T(8,128)(2,1)}), bf16[32,8,128]{2,1,0:T(8,128)(2,1)S(1)}, u32[]{:S(2)}, u32[]{:S(2)}) async-start(bf16[32,8,128]{2,1,0:T(8,128)(2,1)} %shard_map.218), calls=%async_computation.1 | async-start | bytes 131072 | tf_op jit(solution)/shard_map/all_to_all | solution.py:518
  84.5 8.8 %copy-start.11 = (bf16[256,128]{1,0:T(8,128)(2,1)S(1)}, bf16[256,128]{1,0:T(8,128)(2,1)}, u32[]{:S(2)}) copy-start(bf16[256,128]{1,0:T(8,128)(2,1)} %get-tuple-element.40.c.refs_1_) | copy-start | bytes 196612
  93.4 0.9 copy-start.8
  94.3 0.9 copy-start.10
  95.2 0.9 copy-start.12
  96.1 1.2 copy-start.1
  96.1 1.5 copy-start.2
  96.1 1.6 %copy-start.5 = (bf16[32,48,128]{2,1,0:T(8,128)(2,1)S(1)}, bf16[32,48,128]{2,1,0:T(8,128)(2,1)}, u32[]{:S(2)}) copy-start(bf16[32,48,128]{2,1,0:T(8,128)(2,1)} %copy-done.4) | copy-start | bytes 1179652
  96.1 1.7 %copy-start.7 = (bf16[32,48,128]{2,1,0:T(8,128)(2,1)S(1)}, bf16[32,48,128]{2,1,0:T(8,128)(2,1)}, u32[]{:S(2)}) copy-start(bf16[32,48,128]{2,1,0:T(8,128)(2,1)} %copy-done.6) | copy-start | bytes 1179652
  97.9 6.7 %copy-start = (bf16[256,2048]{1,0:T(8,128)(2,1)S(1)}, bf16[256,2048]{1,0:T(8,128)(2,1)}, u32[]{:S(2)}) copy-start(bf16[256,2048]{1,0:T(8,128)(2,1)} %result.1) | copy-start | bytes 3145732
  97.9 8.1 %copy-start.3 = (bf16[1024,256]{1,0:T(8,128)(2,1)S(1)}, bf16[1024,256]{1,0:T(8,128)(2,1)}, u32[]{:S(2)}) copy-start(bf16[1024,256]{1,0:T(8,128)(2,1)} %get-tuple-element.44.keep) | copy-start | bytes 1572868
  100.7 5.3 %collective-permute-start.6 = (bf16[896,256]{1,0:T(8,128)(2,1)S(1)}, bf16[896,256]{1,0:T(8,128)(2,1)S(1)}, u32[]{:S(2)}, u32[]{:S(2)}) collective-permute-start(bf16[896,256]{1,0:T(8,128)(2,1)S(1)} %shard_map.220.own), channel_id=1, source_target_pairs={{0,1},{1,0},{2,3},{3,2},{4,5},{5,4},{6,7},{7,6},{8,9},{9,8},{10,11... | collective-permute-start | bytes 1376264 | tf_op jit(solution)/shard_map/ppermute | solution.py:502
  107.0 17.8 %collective-permute-start.9 = (bf16[1024,128]{1,0:T(8,128)(2,1)S(1)}, bf16[1024,128]{1,0:T(8,128)(2,1)S(1)}, u32[]{:S(2)}, u32[]{:S(2)}) collective-permute-start(bf16[1024,128]{1,0:T(8,128)(2,1)S(1)} %get-tuple-element.50), channel_id=1, source_target_pairs={{0,2},{2,4},{4,6},{6,8},{8,10},{10,12},{12,14},{14,0},{1,3},{3,5},... | collective-permute-start | bytes 786440 | tf_op jit(solution)/shard_map/ppermute | solution.py:502
  108.9 15.9 %collective-permute-start.10 = (bf16[1024,128]{1,0:T(8,128)(2,1)S(1)}, bf16[1024,128]{1,0:T(8,128)(2,1)S(1)}, u32[]{:S(2)}, u32[]{:S(2)}) collective-permute-start(bf16[1024,128]{1,0:T(8,128)(2,1)S(1)} %get-tuple-element.51), channel_id=1, source_target_pairs={{0,14},{2,0},{4,2},{6,4},{8,6},{10,8},{12,10},{14,12},{1,15},{3,1}... | collective-permute-start | bytes 786440 | tf_op jit(solution)/shard_map/ppermute | solution.py:502
  113.5 16.3 %collective-permute-start.11 = (bf16[1024,128]{1,0:T(8,128)(2,1)S(1)}, bf16[1024,128]{1,0:T(8,128)(2,1)S(1)}, u32[]{:S(2)}, u32[]{:S(2)}) collective-permute-start(bf16[1024,128]{1,0:T(8,128)(2,1)S(1)} %get-tuple-element.52), channel_id=1, source_target_pairs={{0,4},{1,13},{2,6},{3,15},{4,8},{5,1},{6,10},{7,3},{8,12},{9,5},{1... | collective-permute-start | bytes 786440 | tf_op jit(solution)/shard_map/ppermute | solution.py:502
  118.2 41.7 %copy-start.9 = (f32[256,2]{0,1:T(2,128)S(1)}, f32[256,2]{0,1:T(2,128)}, u32[]{:S(2)}) copy-start(f32[256,2]{0,1:T(2,128)} %param.41) | copy-start | bytes 6148
  118.2 41.7 %copy-start.13 = (s32[2,256]{1,0:T(2,128)S(1)}, s32[2,256]{1,0:T(2,128)}, u32[]{:S(2)}) copy-start(s32[2,256]{1,0:T(2,128)} %get-tuple-element.57.slots) | copy-start | bytes 6148
  118.3 19.2 %collective-permute-start.7 = (bf16[1024,128]{1,0:T(8,128)(2,1)S(1)}, bf16[1024,128]{1,0:T(8,128)(2,1)S(1)}, u32[]{:S(2)}, u32[]{:S(2)}) collective-permute-start(bf16[1024,128]{1,0:T(8,128)(2,1)S(1)} %get-tuple-element.46), channel_id=1, source_target_pairs={{0,2},{2,4},{4,6},{6,8},{8,10},{10,12},{12,14},{14,0},{1,3},{3,5},... | collective-permute-start | bytes 786440 | tf_op jit(solution)/shard_map/ppermute | solution.py:502
  120.7 16.7 %collective-permute-start.8 = (bf16[1024,128]{1,0:T(8,128)(2,1)S(1)}, bf16[1024,128]{1,0:T(8,128)(2,1)S(1)}, u32[]{:S(2)}, u32[]{:S(2)}) collective-permute-start(bf16[1024,128]{1,0:T(8,128)(2,1)S(1)} %get-tuple-element.47), channel_id=1, source_target_pairs={{0,14},{2,0},{4,2},{6,4},{8,6},{10,8},{12,10},{14,12},{1,15},{3,1}... | collective-permute-start | bytes 786440 | tf_op jit(solution)/shard_map/ppermute | solution.py:502
  130.0 15.5 %collective-permute-start.12 = (bf16[1024,128]{1,0:T(8,128)(2,1)S(1)}, bf16[1024,128]{1,0:T(8,128)(2,1)S(1)}, u32[]{:S(2)}, u32[]{:S(2)}) collective-permute-start(bf16[1024,128]{1,0:T(8,128)(2,1)S(1)} %get-tuple-element.53), channel_id=1, source_target_pairs={{0,4},{2,6},{4,8},{6,10},{8,12},{10,14},{12,0},{14,2},{1,5},{3,7},... | collective-permute-start | bytes 786440 | tf_op jit(solution)/shard_map/ppermute | solution.py:502
  132.2 14.0 %collective-permute-start.13 = (bf16[1024,128]{1,0:T(8,128)(2,1)S(1)}, bf16[1024,128]{1,0:T(8,128)(2,1)S(1)}, u32[]{:S(2)}, u32[]{:S(2)}) collective-permute-start(bf16[1024,128]{1,0:T(8,128)(2,1)S(1)} %get-tuple-element.54), channel_id=1, source_target_pairs={{0,12},{2,14},{4,0},{6,2},{8,4},{10,6},{12,8},{14,10},{1,13},{3,15... | collective-permute-start | bytes 786440 | tf_op jit(solution)/shard_map/ppermute | solution.py:502
